TPU v7x, 128 devices: a whole 4x4x4 slice. The times are simulated.
128 devices in a mesh: sp: 16 (over z, x), tp: 8 (over y, core).
Axes of the slice: x: 4, y: 4, z: 4, core: 2. Of those that a mesh axis runs over, the one named last changes fastest.
Arguments:
- tokens: bfloat16 [16384, 4096], P(('sp', 'tp')), may hold values from -6 to 6
- norm_gain: float32 [4096], replicated, may hold values from 0.1 to 1.9
- q_down: bfloat16 [4096, 768], replicated, may hold values from -0.09375 to 0.09375
- kv_down: bfloat16 [4096, 512], replicated, may hold values from -0.09375 to 0.09375
- rope_down: bfloat16 [4096, 32], replicated, may hold values from -8 to 8
- q_gain: float32 [768], replicated, may hold values from 0.1 to 1.9
- kv_gain: float32 [512], replicated, may hold values from 0.1 to 1.9
- q_up: bfloat16 [768, 1536], P(None, 'tp'), may hold values from -0.21875 to 0.21875
- kv_up: bfloat16 [512, 2048], P(None, 'tp'), may hold values from -0.25 to 0.25
- out_weight: bfloat16 [1024, 4096], replicated, may hold values from -0.1875 to 0.1875
- out_gain: float32 [4096], replicated, may hold values from 0.1 to 1.9
Outputs:
- mixed: bfloat16 [16384, 4096], P(('sp', 'tp'))
All inputs are finite; a program needn't handle non-finite values.
Results may differ from a plain program's by a relative error of at most 0.02.
The roundings to bfloat16 on the way count: a program that leaves them out, or rounds other values in their place, can miss the bound.
Values may be sent and summed in bfloat16 or wider, within the bound.
No kernel may reach another device: no remote copies, remote signals or barrier semaphores. Data moves between devices by JAX's collectives and lax.ppermute only.
A program may use at most 128 MiB of HBM per device.

v0:
```python
import jax
import jax.numpy as jnp
from jax import lax
from jax.sharding import PartitionSpec as P

NOPE = 64
ROPE = 32
VDIM = 64


EPS = 1e-06
THETA = 500000.0


def sent_together(arrays, axis, dim, along):
    ends, at = ([], 0)
    for a in arrays[:-1]:
        at += a.shape[along]
        ends.append(at)
    both = jnp.concatenate(arrays, axis=along)
    return tuple(jnp.split(lax.all_gather(both, axis, axis=dim, tiled=True), ends, axis=along))


def scaled_norm(values_in, gain):
    values_in = values_in.astype(jnp.float32)
    return (
        values_in * lax.rsqrt(jnp.mean(values_in * values_in, axis=-1, keepdims=True) + EPS) * gain
    )


def rotate(values_in, position):
    width = values_in.shape[-1]
    half_dim = width // 2
    inverse = 1.0 / THETA ** (jnp.arange(0, width, 2, dtype=jnp.float32) / width)
    angles = position[:, None] * inverse[None, :]
    angles = angles.reshape((angles.shape[0],) + (1,) * (values_in.ndim - 2) + (half_dim,))
    cosine = jnp.cos(angles)
    sine = jnp.sin(angles)
    left = values_in[..., :half_dim]
    right = values_in[..., half_dim:]
    return jnp.concatenate([left * cosine - right * sine, right * cosine + left * sine], axis=-1)


def local(
    tokens,
    norm_gain,
    q_down,
    kv_down,
    rope_down,
    q_gain,
    kv_gain,
    q_up,
    kv_up,
    out_weight,
    out_gain,
):
    row_count = tokens.shape[0]
    tp_count = lax.axis_size("tp")
    tp_place = lax.axis_index("tp")
    sp_place = lax.axis_index("sp")
    group_rows = row_count * tp_count
    row_first = (sp_place * tp_count + tp_place) * row_count
    own_position = (row_first + jnp.arange(row_count)).astype(jnp.float32)
    normed = scaled_norm(tokens, norm_gain).astype(jnp.bfloat16)
    q_lat = scaled_norm(jnp.dot(normed, q_down, preferred_element_type=jnp.float32), q_gain).astype(
        jnp.bfloat16
    )
    kv_lat = scaled_norm(
        jnp.dot(normed, kv_down, preferred_element_type=jnp.float32), kv_gain
    ).astype(jnp.bfloat16)
    key_rot = rotate(
        jnp.dot(normed, rope_down, preferred_element_type=jnp.float32), own_position
    ).astype(jnp.bfloat16)
    q_group, kv_group, rot_group = sent_together((q_lat, kv_lat, key_rot), "tp", 0, 1)
    query_first = sp_place * group_rows
    query_index = query_first + jnp.arange(group_rows)
    head_count = q_up.shape[1] // (NOPE + ROPE)
    query = jnp.dot(q_group, q_up, preferred_element_type=jnp.float32).reshape(
        group_rows, head_count, NOPE + ROPE
    )
    query = jnp.concatenate(
        [query[..., :NOPE], rotate(query[..., NOPE:], query_index.astype(jnp.float32))], axis=-1
    )
    query = query.astype(jnp.bfloat16)
    query_nope = query[..., :NOPE]
    query_rot = query[..., NOPE:]
    factor = (NOPE + ROPE) ** (-0.5)

    def attend_block(state, key_rows, rot_rows, block_first):

        def compute(state_in):
            top_score, total, summed = state_in
            keys_values = key_rows
            keys_values = keys_values.reshape(key_rows.shape[0], head_count, NOPE + VDIM)
            scores = jnp.einsum(
                "qhd,khd->hqk",
                query_nope,
                keys_values[..., :NOPE],
                preferred_element_type=jnp.float32,
            )
            scores = scores + jnp.einsum(
                "qhd,kd->hqk", query_rot, rot_rows, preferred_element_type=jnp.float32
            )
            scores = scores * factor
            key_index = block_first + jnp.arange(key_rows.shape[0])
            visible = (key_index[None, :] <= query_index[:, None])[None]
            scores = jnp.where(visible, scores, -1e30)
            new_top = jnp.maximum(top_score, jnp.max(scores, axis=-1))
            correction = jnp.exp(top_score - new_top)
            weights = jnp.where(visible, jnp.exp(scores - new_top[..., None]), 0.0)
            total_new = total * correction + jnp.sum(weights, axis=-1)
            product = jnp.einsum(
                "hqk,khd->hqd",
                weights.astype(jnp.bfloat16),
                keys_values[..., NOPE:],
                preferred_element_type=jnp.float32,
            )
            return (new_top, total_new, summed * correction[..., None] + product)

        return lax.cond(
            block_first <= query_first + group_rows - 1, compute, lambda state_in: state_in, state
        )

    start_state = (
        jnp.full((head_count, group_rows), -1e30, jnp.float32),
        jnp.zeros((head_count, group_rows), jnp.float32),
        jnp.zeros((head_count, group_rows, VDIM), jnp.float32),
    )
    expanded = jnp.dot(kv_group, kv_up, preferred_element_type=jnp.float32).astype(jnp.bfloat16)
    key_piece, rot_piece = sent_together((expanded, rot_group), "sp", 0, 1)
    piece_rows = rot_piece.shape[0]
    block_count = piece_rows // group_rows
    key_blocks = key_piece.reshape((block_count, group_rows) + key_piece.shape[1:])
    rot_blocks = rot_piece.reshape(block_count, group_rows, rot_piece.shape[1])

    def step(state_in, index):
        block_first = index * group_rows
        return (attend_block(state_in, key_blocks[index], rot_blocks[index], block_first), None)

    state_out, unused = lax.scan(step, start_state, jnp.arange(block_count))
    top_score, total, summed = state_out
    attended = (summed / total[..., None]).transpose(1, 0, 2).reshape(group_rows, head_count * VDIM)
    attended = attended.astype(jnp.bfloat16)
    own_heads = lax.all_to_all(attended, "tp", split_axis=0, concat_axis=1, tiled=True)
    projected = jnp.dot(own_heads, out_weight, preferred_element_type=jnp.float32)
    return scaled_norm(projected, out_gain).astype(jnp.bfloat16)


def solution(mesh):
    return jax.shard_map(
        local,
        mesh=mesh,
        in_specs=(
            P(("sp", "tp"), None),
            P(),
            P(),
            P(),
            P(),
            P(),
            P(),
            P(None, "tp"),
            P(None, "tp"),
            P(),
            P(),
        ),
        out_specs=P(("sp", "tp"), None),
        check_vma=False,
    )
```

profile of v0, /device:TPU:102, one launch (start us, length us, event | category | flops | bytes accessed | tf_op | source)
XLA Modules:
  0.0 364.7 jit_solution(10357704969036706414)
XLA Ops:
  10.4 3.4 multiply_reduce_fusion.2
  13.9 3.9 %multiply_reduce_fusion.1 = (f32[128]{0:T(128)S(1)}, f32[128,768]{1,0:T(8,128)S(1)}) fusion(bf16[4096,768]{1,0:T(8,128)(2,1)} %param.17, bf16[128,4096]{1,0:T(8,128)(2,1)S(1)} %copy-done.2, f32[4096]{0:T(1024)S(1)} %copy-done.7, f32[128]{0:T(128)S(1)} %add_rsqrt_fusion.3), kind=kOutput, calls=%fused_computation.40 | convolution fusion | flops 807600000 | bytes 7750656 | tf_op jit(solution)/shard_map/dot_general | solution.py:65
  19.1 27.8 %all-gather.3.cloned.1.call-done = bf16[1024,1312]{1,0:T(8,128)(2,1)} async-done(((bf16[128,1312]{1,0:T(8,128)(2,1)}), bf16[1024,1312]{1,0:T(8,128)(2,1)}) %all-gather.3.cloned.1.call-update) | async-done | bytes 2686992 | tf_op jit(solution)/shard_map/all_gather | solution.py:21
  51.9 73.0 %all-gather.5.cloned.1.call-done = bf16[16384,288]{0,1:T(8,128)(2,1)} async-done(((bf16[1024,288]{0,1:T(8,128)(2,1)}), bf16[16384,288]{0,1:T(8,128)(2,1)}) %all-gather.5.cloned.1.call-update) | async-done | bytes 9437200 | tf_op jit(solution)/shard_map/all_gather | solution.py:21
  124.8 7.6 %split.22 = bf16[16384,256]{0,1:T(8,128)(2,1)} slice(bf16[16384,288]{0,1:T(8,128)(2,1)} %all-gather.5.cloned.1.call-done), slice={[0:16384], [0:256]} | slice | bytes 16777216 | tf_op jit(solution)/shard_map/split | solution.py:21
  132.4 8.2 %copy.51 = bf16[32,16,8,1024]{3,2,0,1:T(8,128)(2,1)} copy(bf16[32,16,8,1024]{3,2,1,0:T(8,128)(2,1)} %bitcast.45) | data formatting | bytes 16777216 | tf_op jit(solution)/shard_map/reshape | solution.py:133
  140.8 199.3 %while.17 = (s32[]{:T(128)}, f32[2,1024]{1,0:T(2,128)S(1)}, f32[2,1024]{1,0:T(2,128)S(1)}, f32[2,1024,64]{1,2,0:T(8,128)S(1)}, s32[16]{0:T(128)S(1)}, /*index=5*...) while((s32[]{:T(128)}, f32[2,1024]{1,0:T(2,128)S(1)}, ...), condition=%wide.region_8.9_spmd.clone, body=%wide.region_3.8_spmd.clone.sunk | while | flops 693377024 | bytes 49373544 | solution.py:140
  142.0 11.2 %conditional.3 = ((f32[2,1024]{1,0:T(2,128)S(1)}, f32[2,1024]{1,0:T(2,128)S(1)}, f32[2,1024,64]{1,2,0:T(8,128)S(1)})) conditional(s32[]{:T(128)} %convert_element_type.102, (f32[2,1024]{1,0:T(2,128)S(1)}, f32[2,1024]{1,0:T(2,128)S(1)}, f32[2,1024,64]{1,2,0:T(8,128)S(1)}) %tuple.63, (s32[]{:T(128)}, s32[]{:T(128)}, s32[]{:T(128)}, ...), branch_computations={%region_4.4_spmd, %region_5.7_spmd} | conditional | flops 693377024 | bytes 49369168 | solution.py:120
  147.0 2.3 fusion.39
  151.1 2.1 fusion.9
  154.5 11.2 %conditional.3 = ((f32[2,1024]{1,0:T(2,128)S(1)}, f32[2,1024]{1,0:T(2,128)S(1)}, f32[2,1024,64]{1,2,0:T(8,128)S(1)})) conditional(s32[]{:T(128)} %convert_element_type.102, (f32[2,1024]{1,0:T(2,128)S(1)}, f32[2,1024]{1,0:T(2,128)S(1)}, f32[2,1024,64]{1,2,0:T(8,128)S(1)}) %tuple.63, (s32[]{:T(128)}, s32[]{:T(128)}, s32[]{:T(128)}, ...), branch_computations={%region_4.4_spmd, %region_5.7_spmd} | conditional | flops 693377024 | bytes 49369168 | solution.py:120
  159.5 2.3 fusion.39
  163.6 2.1 fusion.9
  166.9 11.2 %conditional.3 = ((f32[2,1024]{1,0:T(2,128)S(1)}, f32[2,1024]{1,0:T(2,128)S(1)}, f32[2,1024,64]{1,2,0:T(8,128)S(1)})) conditional(s32[]{:T(128)} %convert_element_type.102, (f32[2,1024]{1,0:T(2,128)S(1)}, f32[2,1024]{1,0:T(2,128)S(1)}, f32[2,1024,64]{1,2,0:T(8,128)S(1)}) %tuple.63, (s32[]{:T(128)}, s32[]{:T(128)}, s32[]{:T(128)}, ...), branch_computations={%region_4.4_spmd, %region_5.7_spmd} | conditional | flops 693377024 | bytes 49369168 | solution.py:120
  172.0 2.3 fusion.39
  176.0 2.1 fusion.9
  179.4 11.2 %conditional.3 = ((f32[2,1024]{1,0:T(2,128)S(1)}, f32[2,1024]{1,0:T(2,128)S(1)}, f32[2,1024,64]{1,2,0:T(8,128)S(1)})) conditional(s32[]{:T(128)} %convert_element_type.102, (f32[2,1024]{1,0:T(2,128)S(1)}, f32[2,1024]{1,0:T(2,128)S(1)}, f32[2,1024,64]{1,2,0:T(8,128)S(1)}) %tuple.63, (s32[]{:T(128)}, s32[]{:T(128)}, s32[]{:T(128)}, ...), branch_computations={%region_4.4_spmd, %region_5.7_spmd} | conditional | flops 693377024 | bytes 49369168 | solution.py:120
  184.4 2.3 fusion.39
  188.5 2.1 fusion.9
  191.8 11.2 %conditional.3 = ((f32[2,1024]{1,0:T(2,128)S(1)}, f32[2,1024]{1,0:T(2,128)S(1)}, f32[2,1024,64]{1,2,0:T(8,128)S(1)})) conditional(s32[]{:T(128)} %convert_element_type.102, (f32[2,1024]{1,0:T(2,128)S(1)}, f32[2,1024]{1,0:T(2,128)S(1)}, f32[2,1024,64]{1,2,0:T(8,128)S(1)}) %tuple.63, (s32[]{:T(128)}, s32[]{:T(128)}, s32[]{:T(128)}, ...), branch_computations={%region_4.4_spmd, %region_5.7_spmd} | conditional | flops 693377024 | bytes 49369168 | solution.py:120
  196.9 2.3 fusion.39
  204.3 11.2 %conditional.3 = ((f32[2,1024]{1,0:T(2,128)S(1)}, f32[2,1024]{1,0:T(2,128)S(1)}, f32[2,1024,64]{1,2,0:T(8,128)S(1)})) conditional(s32[]{:T(128)} %convert_element_type.102, (f32[2,1024]{1,0:T(2,128)S(1)}, f32[2,1024]{1,0:T(2,128)S(1)}, f32[2,1024,64]{1,2,0:T(8,128)S(1)}) %tuple.63, (s32[]{:T(128)}, s32[]{:T(128)}, s32[]{:T(128)}, ...), branch_computations={%region_4.4_spmd, %region_5.7_spmd} | conditional | flops 693377024 | bytes 49369168 | solution.py:120
  209.3 2.3 fusion.39
  216.8 11.2 %conditional.3 = ((f32[2,1024]{1,0:T(2,128)S(1)}, f32[2,1024]{1,0:T(2,128)S(1)}, f32[2,1024,64]{1,2,0:T(8,128)S(1)})) conditional(s32[]{:T(128)} %convert_element_type.102, (f32[2,1024]{1,0:T(2,128)S(1)}, f32[2,1024]{1,0:T(2,128)S(1)}, f32[2,1024,64]{1,2,0:T(8,128)S(1)}) %tuple.63, (s32[]{:T(128)}, s32[]{:T(128)}, s32[]{:T(128)}, ...), branch_computations={%region_4.4_spmd, %region_5.7_spmd} | conditional | flops 693377024 | bytes 49369168 | solution.py:120
  221.8 2.3 fusion.39
  229.2 11.2 %conditional.3 = ((f32[2,1024]{1,0:T(2,128)S(1)}, f32[2,1024]{1,0:T(2,128)S(1)}, f32[2,1024,64]{1,2,0:T(8,128)S(1)})) conditional(s32[]{:T(128)} %convert_element_type.102, (f32[2,1024]{1,0:T(2,128)S(1)}, f32[2,1024]{1,0:T(2,128)S(1)}, f32[2,1024,64]{1,2,0:T(8,128)S(1)}) %tuple.63, (s32[]{:T(128)}, s32[]{:T(128)}, s32[]{:T(128)}, ...), branch_computations={%region_4.4_spmd, %region_5.7_spmd} | conditional | flops 693377024 | bytes 49369168 | solution.py:120
  234.2 2.3 fusion.39
  241.7 11.2 %conditional.3 = ((f32[2,1024]{1,0:T(2,128)S(1)}, f32[2,1024]{1,0:T(2,128)S(1)}, f32[2,1024,64]{1,2,0:T(8,128)S(1)})) conditional(s32[]{:T(128)} %convert_element_type.102, (f32[2,1024]{1,0:T(2,128)S(1)}, f32[2,1024]{1,0:T(2,128)S(1)}, f32[2,1024,64]{1,2,0:T(8,128)S(1)}) %tuple.63, (s32[]{:T(128)}, s32[]{:T(128)}, s32[]{:T(128)}, ...), branch_computations={%region_4.4_spmd, %region_5.7_spmd} | conditional | flops 693377024 | bytes 49369168 | solution.py:120
  246.7 2.3 fusion.39
  250.7 2.1 fusion.9
  254.1 11.2 %conditional.3 = ((f32[2,1024]{1,0:T(2,128)S(1)}, f32[2,1024]{1,0:T(2,128)S(1)}, f32[2,1024,64]{1,2,0:T(8,128)S(1)})) conditional(s32[]{:T(128)} %convert_element_type.102, (f32[2,1024]{1,0:T(2,128)S(1)}, f32[2,1024]{1,0:T(2,128)S(1)}, f32[2,1024,64]{1,2,0:T(8,128)S(1)}) %tuple.63, (s32[]{:T(128)}, s32[]{:T(128)}, s32[]{:T(128)}, ...), branch_computations={%region_4.4_spmd, %region_5.7_spmd} | conditional | flops 693377024 | bytes 49369168 | solution.py:120
  259.1 2.3 fusion.39
  266.6 11.2 %conditional.3 = ((f32[2,1024]{1,0:T(2,128)S(1)}, f32[2,1024]{1,0:T(2,128)S(1)}, f32[2,1024,64]{1,2,0:T(8,128)S(1)})) conditional(s32[]{:T(128)} %convert_element_type.102, (f32[2,1024]{1,0:T(2,128)S(1)}, f32[2,1024]{1,0:T(2,128)S(1)}, f32[2,1024,64]{1,2,0:T(8,128)S(1)}) %tuple.63, (s32[]{:T(128)}, s32[]{:T(128)}, s32[]{:T(128)}, ...), branch_computations={%region_4.4_spmd, %region_5.7_spmd} | conditional | flops 693377024 | bytes 49369168 | solution.py:120
  271.6 2.3 fusion.39
  279.0 11.2 %conditional.3 = ((f32[2,1024]{1,0:T(2,128)S(1)}, f32[2,1024]{1,0:T(2,128)S(1)}, f32[2,1024,64]{1,2,0:T(8,128)S(1)})) conditional(s32[]{:T(128)} %convert_element_type.102, (f32[2,1024]{1,0:T(2,128)S(1)}, f32[2,1024]{1,0:T(2,128)S(1)}, f32[2,1024,64]{1,2,0:T(8,128)S(1)}) %tuple.63, (s32[]{:T(128)}, s32[]{:T(128)}, s32[]{:T(128)}, ...), branch_computations={%region_4.4_spmd, %region_5.7_spmd} | conditional | flops 693377024 | bytes 49369168 | solution.py:120
  284.0 2.3 fusion.39
  291.5 11.2 %conditional.3 = ((f32[2,1024]{1,0:T(2,128)S(1)}, f32[2,1024]{1,0:T(2,128)S(1)}, f32[2,1024,64]{1,2,0:T(8,128)S(1)})) conditional(s32[]{:T(128)} %convert_element_type.102, (f32[2,1024]{1,0:T(2,128)S(1)}, f32[2,1024]{1,0:T(2,128)S(1)}, f32[2,1024,64]{1,2,0:T(8,128)S(1)}) %tuple.63, (s32[]{:T(128)}, s32[]{:T(128)}, s32[]{:T(128)}, ...), branch_computations={%region_4.4_spmd, %region_5.7_spmd} | conditional | flops 693377024 | bytes 49369168 | solution.py:120
  296.5 2.3 fusion.39
  303.9 11.2 %conditional.3 = ((f32[2,1024]{1,0:T(2,128)S(1)}, f32[2,1024]{1,0:T(2,128)S(1)}, f32[2,1024,64]{1,2,0:T(8,128)S(1)})) conditional(s32[]{:T(128)} %convert_element_type.102, (f32[2,1024]{1,0:T(2,128)S(1)}, f32[2,1024]{1,0:T(2,128)S(1)}, f32[2,1024,64]{1,2,0:T(8,128)S(1)}) %tuple.63, (s32[]{:T(128)}, s32[]{:T(128)}, s32[]{:T(128)}, ...), branch_computations={%region_4.4_spmd, %region_5.7_spmd} | conditional | flops 693377024 | bytes 49369168 | solution.py:120
  309.0 2.3 fusion.39
  316.4 11.2 %conditional.3 = ((f32[2,1024]{1,0:T(2,128)S(1)}, f32[2,1024]{1,0:T(2,128)S(1)}, f32[2,1024,64]{1,2,0:T(8,128)S(1)})) conditional(s32[]{:T(128)} %convert_element_type.102, (f32[2,1024]{1,0:T(2,128)S(1)}, f32[2,1024]{1,0:T(2,128)S(1)}, f32[2,1024,64]{1,2,0:T(8,128)S(1)}) %tuple.63, (s32[]{:T(128)}, s32[]{:T(128)}, s32[]{:T(128)}, ...), branch_computations={%region_4.4_spmd, %region_5.7_spmd} | conditional | flops 693377024 | bytes 49369168 | solution.py:120
  321.4 2.3 fusion.39
  325.5 2.1 fusion.9
  328.8 11.2 %conditional.3 = ((f32[2,1024]{1,0:T(2,128)S(1)}, f32[2,1024]{1,0:T(2,128)S(1)}, f32[2,1024,64]{1,2,0:T(8,128)S(1)})) conditional(s32[]{:T(128)} %convert_element_type.102, (f32[2,1024]{1,0:T(2,128)S(1)}, f32[2,1024]{1,0:T(2,128)S(1)}, f32[2,1024,64]{1,2,0:T(8,128)S(1)}) %tuple.63, (s32[]{:T(128)}, s32[]{:T(128)}, s32[]{:T(128)}, ...), branch_computations={%region_4.4_spmd, %region_5.7_spmd} | conditional | flops 693377024 | bytes 49369168 | solution.py:120
  333.9 2.3 fusion.39
  337.9 2.1 fusion.9
  340.2 11.6 %all_to_all.16 = bf16[8,128,128]{1,2,0:T(8,128)(2,1)S(1)} all-to-all(bf16[8,128,128]{1,2,0:T(8,128)(2,1)S(1)} %copy.44), channel_id=1, replica_groups=mesh['sp'=16,'tp'=8] {'tp'}, dimensions={0} | all-to-all | bytes 524288 | tf_op jit(solution)/shard_map/all_to_all | solution.py:144
  351.8 4.8 %multiply_reduce_fusion = (f32[128]{0:T(128)S(1)}, f32[128,4096]{1,0:T(8,128)S(1)}) fusion(bf16[128,1024]{0,1:T(8,128)(2,1)S(1)} %bitcast.51, bf16[1024,4096]{1,0:T(8,128)(2,1)} %param.24), kind=kOutput, calls=%fused_computation.30 | convolution fusion | flops 1074790272 | bytes 10748416 | tf_op jit(solution)/shard_map/dot_general | solution.py:145
  (224 shorter events, 116.4 us)
Async XLA Ops:
  6.5 44.5 %copy-start = (bf16[768,192]{0,1:T(8,128)(2,1)S(1)}, bf16[768,192]{0,1:T(8,128)(2,1)}, u32[]{:S(2)}) copy-start(bf16[768,192]{0,1:T(8,128)(2,1)} %param.22) | copy-start | bytes 884740
  6.5 40.3 %all-gather.3.cloned.1.call-start = ((), (), s32[]{:S(2)}) async-start(), calls=%async_computation.1 | async-start | bytes 3244032 | tf_op jit(solution)/shard_map/all_gather | solution.py:21
  8.1 5.7 %copy-start.2 = (bf16[128,4096]{1,0:T(8,128)(2,1)S(1)}, bf16[128,4096]{1,0:T(8,128)(2,1)}, u32[]{:S(2)}) copy-start(bf16[128,4096]{1,0:T(8,128)(2,1)} %param.15) | copy-start | bytes 3145732
  8.1 5.7 %copy-start.7 = (f32[4096]{0:T(1024)S(1)}, f32[4096]{0:T(1024)}, u32[]{:S(2)}) copy-start(f32[4096]{0:T(1024)} %param.16) | copy-start | bytes 49156
  13.8 4.0 %copy-start.6 = (f32[512]{0:T(512)S(1)}, f32[512]{0:T(512)}, u32[]{:S(2)}) copy-start(f32[512]{0:T(512)} %param.21) | copy-start | bytes 6148
  13.8 4.1 %copy-start.5 = (f32[768]{0:T(1024)S(1)}, f32[768]{0:T(1024)}, u32[]{:S(2)}) copy-start(f32[768]{0:T(1024)} %param.20) | copy-start | bytes 9220
  18.9 106.0 %all-gather.5.cloned.1.call-start = ((), (), s32[]{:S(2)}) async-start(), calls=%async_computation.2 | async-start | bytes 10027008 | tf_op jit(solution)/shard_map/all_gather | solution.py:21
  46.9 4.2 %copy-start.3 = (bf16[1024,1312]{1,0:T(8,128)(2,1)S(1)}, bf16[1024,1312]{1,0:T(8,128)(2,1)}, u32[]{:S(2)}) copy-start(bf16[1024,1312]{1,0:T(8,128)(2,1)} %all-gather.3.cloned.1.call-done) | copy-start | bytes 8060932
  132.4 8.2 %slice-start = ((bf16[16384,288]{0,1:T(8,128)(2,1)}), bf16[16384,32]{0,1:T(8,128)(2,1)S(1)}, s32[]{:S(2)}) async-start(bf16[16384,288]{0,1:T(8,128)(2,1)} %all-gather.5.cloned.1.call-done), calls=%async_computation.3 | async-start | bytes 2097152 | tf_op jit(solution)/shard_map/split | solution.py:21
  351.8 4.8 %copy-start.4 = (f32[4096]{0:T(1024)S(1)}, f32[4096]{0:T(1024)}, u32[]{:S(2)}) copy-start(f32[4096]{0:T(1024)} %param.25) | copy-start | bytes 49156
  351.8 6.1 %copy-start.1 = (bf16[768,192]{0,1:T(8,128)(2,1)S(1)}, bf16[768,192]{0,1:T(8,128)(2,1)}, u32[]{:S(2)}) copy-start(bf16[768,192]{0,1:T(8,128)(2,1)} %param.22) | copy-start | bytes 884740
Sparse Core Ops, SparseCore 0:
  19.0 27.8 all-gather.2
  50.9 73.9 all-gather.4
where the time goes:
time: 366 us; the launch traced here: 365 us
  matrix products  107 us (29%)
  waiting for transfers between devices  101 us (28%)
  local copies, waits for them, and re-layouts  45.1 us (12%)
  loops' own time  43.2 us (12%)
  other arithmetic  42.9 us (12%)
  between operations  13.7 us (4%)
  blocking collectives  11.6 us (3%)
    all_gather x2, waiting for transfers between devices, sent_together(): lax.all_gather(both, axis, axis=dim, tiled=True)  101 us
    dot_general x16, matrix products, compute(): jnp.einsum('qhd,kd->hqk', query_rot, rot_rows, preferred_element_type=jnp...  36.7 us
    dot_general x16, matrix products, compute(): jnp.einsum('hqk,khd->hqd', weights.astype(jnp.bfloat16), keys_values[...,...  33.3 us
    another operation x16, loops' own time, attend_block(): lax.cond(block_first <= query_first + group_rows - 1, compute, lambda sta...  32.2 us
    reduce_sum x16, other arithmetic, compute(): total_new = total * correction + jnp.sum(weights, axis=-1)  27.4 us
    dot_general x16, matrix products, compute(): jnp.einsum('qhd,khd->hqk', query_nope, keys_values[..., :NOPE], preferred...  20.8 us
    dynamic_slice x16, local copies, waits for them, and re-layouts, step(): key_blocks[index]  17.3 us
    all_to_all x1, blocking collectives, local(): lax.all_to_all(attended, 'tp', split_axis=0, concat_axis=1, tiled=True)  11.6 us
  transfers between devices with their start and end apart: 2, of which 2 were waited for; matrix products, arithmetic and copies ran while one was open for 0% of the time, Pallas kernels for 0%

commit v1 on v0

v1 whole, which is shorter than its diff:
```python
import functools

import jax
import jax.numpy as jnp
from jax import lax
from jax.experimental import pallas as pl
from jax.experimental.pallas import tpu as pltpu
from jax.sharding import PartitionSpec as P


BF = jnp.bfloat16
F32 = jnp.float32
EPS = 1e-06
THETA = 500000.0
AXES = ("sp", "tp")
VM = pl.BlockSpec(memory_space=pltpu.VMEM)
SM = pl.BlockSpec(memory_space=pltpu.SMEM)


PER_US = 3e8


def small(mib):
    return pltpu.CompilerParams(vmem_limit_bytes=mib * 2**20)


def pairs(move):
    out = []
    for i in range(128):
        sp, tp = i // 8, i % 8
        z, x, y, c = move(sp // 4, sp % 4, tp // 2, tp % 2)
        out.append((i, ((z % 4) * 4 + x % 4) * 8 + (y % 4) * 2 + c % 2))
    return out


def back(perm):
    return [(b, a) for a, b in perm]


ALONG_Y = [pairs(lambda z, x, y, c, k=k: (z, x, y + k, c)) for k in range(4)]
ALONG_Z = [pairs(lambda z, x, y, c, k=k: (z + k, x, y, c)) for k in range(4)]
ALONG_X = [pairs(lambda z, x, y, c, k=k: (z, x + k, y, c)) for k in range(4)]
CORE = pairs(lambda z, x, y, c: (z, x, y, c + 1))


def send(a, perm):
    return lax.ppermute(a, AXES, perm)


def normed_rows(v, gain):
    return v * lax.rsqrt(jnp.mean(v * v, axis=-1, keepdims=True) + EPS) * gain


CHUNKS = 4


def down_kernel(
    tok, gain, kvd, rd, kvg, qd, qg, cos, sin, out,
    tok_v, gain_v, kvd_v, rd_v, kvg_v, qd_v, qg_v, normed, sems,
):
    step = kvd.shape[0] // CHUNKS
    copies = {}

    def fetch(name, src, dst):
        copies[name] = pltpu.make_async_copy(src, dst, sems.at[len(copies)])
        copies[name].start()

    fetch("tok", tok, tok_v)
    fetch("gain", gain, gain_v)
    fetch("rd", rd, rd_v)
    for n in range(CHUNKS):
        fetch(("kv", n), kvd.at[pl.ds(n * step, step)], kvd_v.at[n])
    fetch("kvg", kvg, kvg_v)
    for n in range(CHUNKS):
        fetch(("q", n), qd.at[pl.ds(n * step, step)], qd_v.at[n])
    fetch("qg", qg, qg_v)
    copies["tok"].wait()
    copies["gain"].wait()
    normed[...] = normed_rows(tok_v[...].astype(F32), gain_v[...]).astype(BF)
    copies["rd"].wait()
    r = lax.dot_general(
        rd_v[...], normed[...], (((1,), (1,)), ((), ())), preferred_element_type=F32
    )
    left, right = r[0:16], r[16:32]
    out[512:528, :] = (left * cos[...] - right * sin[...]).astype(BF)
    out[528:544, :] = (right * cos[...] + left * sin[...]).astype(BF)

    def product(name, weights):
        total = None
        for n in range(CHUNKS):
            copies[(name, n)].wait()
            part = jnp.dot(
                normed[:, n * step : n * step + step], weights[n], preferred_element_type=F32
            )
            total = part if total is None else total + part
        return total

    total = product("kv", kvd_v)
    copies["kvg"].wait()
    out[0:512, :] = normed_rows(total, kvg_v[...]).T.astype(BF)
    total = product("q", qd_v)
    copies["qg"].wait()
    gain_q = jnp.concatenate([qg_v[n : n + 1, :] for n in range(6)], axis=1)
    out[544:1312, :] = normed_rows(total, gain_q).T.astype(BF)


def down_call(tok, gain, kvd, rd, kvg, qd, qg, cos, sin):
    rows, d = tok.shape
    step = d // CHUNKS
    return pl.pallas_call(
        down_kernel,
        out_shape=jax.ShapeDtypeStruct((1312, rows), BF),
        in_specs=[pl.BlockSpec(memory_space=pl.ANY)] * 7 + [VM] * 2,
        out_specs=VM,
        scratch_shapes=[
            pltpu.VMEM((rows, d), BF),
            pltpu.VMEM((1, d), F32),
            pltpu.VMEM((CHUNKS, step, 512), BF),
            pltpu.VMEM((32, d), BF),
            pltpu.VMEM((1, 512), F32),
            pltpu.VMEM((CHUNKS, step, 768), BF),
            pltpu.VMEM((6, 128), F32),
            pltpu.VMEM((rows, d), BF),
            pltpu.SemaphoreType.DMA((5 + 2 * CHUNKS,)),
        ],
        name="down",
    )(tok, gain, kvd, rd, kvg, qd, qg, cos, sin)


def up_kernel(
    s, p0, p1, p2, p3, kv_own, kv_other, q_own, q_other, cos, sin,
    near, q0, m1, m2, m3, kv_w, q_w, kv, q,
):
    z, c = s[1], s[4]
    parts = (p0, p1, p2, p3)
    kv_w[0:256, :] = kv_own[...].T
    kv_w[256:512, :] = kv_other[...].T
    q_w[0:192, :] = q_own[...]
    q_w[192:384, :] = q_other[...]
    lat = jnp.concatenate([p[0:512, :] for p in parts], axis=1)
    rot = jnp.concatenate([p[512:544, :] for p in parts], axis=1)
    kv[...] = jnp.dot(kv_w[...], lat, preferred_element_type=F32).astype(BF)
    lat = jnp.concatenate([p[544:1312, :] for p in parts], axis=1)
    q[...] = jnp.dot(q_w[...], lat, preferred_element_type=F32)
    for k, out in enumerate((None, m1, m2, m3)):
        head = (z + k - 2 * c + 4) & 3
        at = head * 128
        to = near if k == 0 else out
        to[0:64, :] = kv[pl.ds(pl.multiple_of(at, 128), 64), :]
        to[64:96, :] = rot
        to[96:160, :] = kv[pl.ds(pl.multiple_of(at + 64, 64), 64), :]
        to, low = (q0, 0) if k == 0 else (out, 160)
        at = head * 96
        left = q[pl.ds(pl.multiple_of(at + 64, 32), 16), :]
        right = q[pl.ds(pl.multiple_of(at + 80, 16), 16), :]
        to[low : low + 64, :] = q[pl.ds(pl.multiple_of(at, 32), 64), :].astype(BF)
        to[low + 64 : low + 80, :] = (left * cos[...] - right * sin[...]).astype(BF)
        to[low + 80 : low + 96, :] = (right * cos[...] + left * sin[...]).astype(BF)


def up_call(s, parts, *rest):
    piece = lambda rows: jax.ShapeDtypeStruct((rows, 512), BF)
    return pl.pallas_call(
        up_kernel,
        out_shape=[piece(160), piece(96)] + [piece(256)] * 3,
        in_specs=[SM] + [VM] * 10,
        out_specs=[VM] * 5,
        scratch_shapes=[
            pltpu.VMEM((512, 512), BF),
            pltpu.VMEM((384, 768), BF),
            pltpu.VMEM((512, 512), BF),
            pltpu.VMEM((384, 512), F32),
        ],
        compiler_params=small(16),
        name="up",
    )(s, *parts, *rest)


def gather_kernel(q0, m1, m2, m3, far, q):
    q[0:96, :] = q0[...]
    for n, m in enumerate((m1, m2, m3)):
        far[160 * n : 160 * n + 160, :] = m[0:160, :]
        q[96 * n + 96 : 96 * n + 192, :] = m[160:256, :]


def gather_call(*pieces):
    return pl.pallas_call(
        gather_kernel,
        out_shape=[jax.ShapeDtypeStruct((480, 512), BF), jax.ShapeDtypeStruct((384, 512), BF)],
        in_specs=[VM] * 4,
        out_specs=[VM] * 2,
        compiler_params=small(8),
        name="gather",
    )(*pieces)


def regroup_kernel(r0, r1, r2, r3, *outs):
    for j, o in enumerate(outs):
        for k, r in enumerate((r0, r1, r2, r3)):
            o[64 * k : 64 * k + 64, :] = r[:, 128 * j : 128 * j + 128]


def regroup_call(*pieces):
    return pl.pallas_call(
        regroup_kernel,
        out_shape=[jax.ShapeDtypeStruct((256, 128), BF)] * 4,
        in_specs=[VM] * 4,
        out_specs=[VM] * 4,
        compiler_params=small(8),
        name="regroup",
    )(*pieces)


SCALE = 1.4426950408889634 / 96**0.5
LIMIT = 60.0


def attn_kernel(first, last, s_ref, *refs):
    outs = ()
    if first:
        own, other, near, far, acc_ref, qs, ks, vs, top, m_ref = refs
    elif last:
        qs, near, far, acc_in, *outs, ks, vs, top, m_ref, acc_ref = refs
    else:
        qs, near, far, acc_in, acc_ref, ks, vs, top, m_ref = refs
    xk, z, x, y, c = (s_ref[i] for i in range(5))

    def reset():
        top[...] = jnp.full(top.shape, -1e30, F32)
        if first:
            m_ref[...] = jnp.full(m_ref.shape, -1e30, F32)
            acc_ref[...] = jnp.zeros(acc_ref.shape, F32)
        else:
            acc_ref[...] = acc_in[...]
            m_ref[...] = acc_in[:, 80:81, :]

    row = lax.broadcasted_iota(jnp.int32, (16, 512), 0)
    ones = jnp.where(row == 0, 1.0, 0.0).astype(BF)
    for k in range(4):
        if first:
            for h, v in enumerate((own, other)):
                q = v[96 * k : 96 * k + 96, :].astype(F32) * SCALE
                high = q.astype(BF)
                qs[k, 0:96, 512 * h : 512 * h + 512] = high
                qs[k, 96:192, 512 * h : 512 * h + 512] = (q - high.astype(F32)).astype(BF)
        r, at = (near, 0) if k == 0 else (far, 160 * (k - 1))
        kt = r[at : at + 96, :]
        ks[k] = jnp.concatenate([kt, kt], axis=0).T
        vs[k, 0:64, :] = r[at + 96 : at + 160, :]
        vs[k, 64:80, :] = ones

    def exact(kq, kk, free):
        m_old = m_ref[kq]
        s = jnp.dot(ks[kk], qs[kq], preferred_element_type=F32)
        kr = lax.broadcasted_iota(jnp.int32, (512, 1024), 0)
        qr = lax.broadcasted_iota(jnp.int32, (512, 1024), 1)
        kpos = ((y - (kr >> 7)) & 3) * 256 + c * 128 + (kr & 127)
        par = jnp.where(qr < 512, c, 1 - c)
        qpos = ((y - (qr >> 7)) & 3) * 256 + par * 128 + (qr & 127)
        s = jnp.where(kpos <= qpos + free, s, -1e30)
        m_new = jnp.maximum(m_old, jnp.max(s, axis=0, keepdims=True))
        p = jnp.exp2(s - m_new).astype(BF)
        o = jnp.dot(vs[kk], p, preferred_element_type=F32)
        acc_ref[kq, 0:80] = acc_ref[kq, 0:80] * jnp.exp2(m_old - m_new) + o
        m_ref[kq] = m_new

    def fast(kq, keys):
        m = m_ref[kq]
        q = qs[kq]
        peak, o = None, None
        for kk in keys:
            s = jnp.dot(ks[kk], q, preferred_element_type=F32)
            high = jnp.max(s.reshape(64, 8, 1024), axis=0)
            peak = high if peak is None else jnp.maximum(peak, high)
            p = jnp.exp2(s - m).astype(BF)
            d = jnp.dot(vs[kk], p, preferred_element_type=F32)
            o = d if o is None else o + d
        acc_ref[kq, 0:80] += o
        top[...] = jnp.maximum(top[...], peak - m)

    def walk(quick):
        @pl.loop(0, 4)
        def _(kq):
            zq = (z - kq + 4) & 3
            full = zq + jnp.where(xk < x, 1, 0)

            diag = jnp.where(xk == x, 1, 0)
            some = 1 if first else jnp.where(zq == 0, 1, 0)
            start = jnp.minimum(jnp.where(quick, some, full), full)

            @pl.loop(1 - diag, start + 1)
            def _(j):
                at = jnp.where(j == 0, zq, j - 1)
                exact(kq, (z - at + 4) & 3, jnp.where(j == 0, 0, 2048))

            count = full - start

            @pl.loop(0, count // 2)
            def _(j):
                fast(kq, [(z - start - 2 * j - n + 8) & 3 for n in (0, 1)])

            @pl.when(count % 2 == 1)
            def _():
                fast(kq, [(z - full + 5) & 3])

    def attempt(turn):
        reset()
        walk(turn == 0)
        over = jnp.logical_not(jnp.max(top[...]) <= LIMIT)
        return jnp.where(jnp.logical_and(over, turn == 0), 1, 2)

    lax.while_loop(lambda turn: turn < 2, attempt, jnp.int32(0))

    @pl.when(jnp.logical_not(jnp.max(top[...]) <= LIMIT))
    def _():
        reset()
        walk(False)

    if outs:
        for k in range(4):
            for h, o in enumerate(outs):
                o[k, 0:80, :] = acc_ref[k, 0:80, 512 * h : 512 * h + 512]
                o[k, 80:81, :] = m_ref[k, :, 512 * h : 512 * h + 512]
    else:
        acc_ref[:, 80:81, :] = m_ref[...]


def attention(scal, near, far, queries=None, state=None, last=False):
    first = state is None
    outs = [jax.ShapeDtypeStruct((4, 88, 1024), F32)]
    scratch = [
        pltpu.VMEM((4, 512, 192), BF),
        pltpu.VMEM((4, 80, 512), BF),
        pltpu.VMEM((8, 1024), F32),
        pltpu.VMEM((4, 1, 1024), F32),
    ]
    if first:
        outs.append(jax.ShapeDtypeStruct((4, 192, 1024), BF))
        args = (scal, *queries, near, far)
    else:
        args = (scal, queries, near, far, state)
    if last:
        outs = [jax.ShapeDtypeStruct((4, 88, 512), F32)] * 2
        scratch.append(pltpu.VMEM((4, 88, 1024), F32))
    return pl.pallas_call(
        functools.partial(attn_kernel, first, last),
        out_shape=outs,
        in_specs=[SM] + [VM] * (len(args) - 1),
        out_specs=[VM] * len(outs),
        scratch_shapes=scratch,
        compiler_params=small(28),
        cost_estimate=pl.CostEstimate(flops=int(5 * PER_US), transcendentals=0, bytes_accessed=2**20),
        name="attn",
    )(*args)


def merge_kernel(mine, theirs, *outs):
    for k in range(4):
        m1, m2 = mine[k, 80:81, :], theirs[k, 80:81, :]
        m = jnp.maximum(m1, m2)
        a = mine[k, 0:72, :] * jnp.exp2(m1 - m) + theirs[k, 0:72, :] * jnp.exp2(m2 - m)
        outs[k][...] = (a[0:64] / a[64:65]).astype(BF)


def merge_call(mine, theirs):
    return pl.pallas_call(
        merge_kernel,
        out_shape=[jax.ShapeDtypeStruct((64, 512), BF)] * 4,
        in_specs=[VM] * 2,
        out_specs=[VM] * 4,
        compiler_params=small(8),
        name="merge",
    )(mine, theirs)


def out_kernel(s, t0, t1, t2, t3, w, gain, out, heads):
    z, y = s[1], s[3]
    for j, t in enumerate((t0, t1, t2, t3)):
        for k in range(4):
            at = (4 * ((y + j) & 3) + ((z + k) & 3)) * 64
            heads[pl.ds(pl.multiple_of(at, 64), 64), :] = t[64 * k : 64 * k + 64, :]
    rows = heads[...].T
    proj = jnp.dot(rows, w[...], preferred_element_type=F32)
    out[...] = normed_rows(proj, gain[...]).astype(BF)


def out_call(s, parts, w, gain):
    return pl.pallas_call(
        out_kernel,
        out_shape=jax.ShapeDtypeStruct((128, w.shape[1]), BF),
        in_specs=[SM] + [VM] * 6,
        out_specs=VM,
        scratch_shapes=[pltpu.VMEM((w.shape[0], 128), BF)],
        compiler_params=small(24),
        name="out_proj",
    )(s, *parts, w, gain)


def turns(position):
    inverse = 1.0 / THETA ** (jnp.arange(0, 32, 2, dtype=F32) / 32)
    angles = inverse[:, None] * position.astype(F32)[None, :]
    return jnp.cos(angles), jnp.sin(angles)


def local(tokens, norm_gain, q_down, kv_down, rope_down, q_gain, kv_gain, q_up, kv_up, out_weight, out_gain):
    sp, tp = lax.axis_index("sp"), lax.axis_index("tp")
    z, x, y, c = sp // 4, sp % 4, tp // 2, tp % 2
    scal = lambda xk: jnp.stack([xk, z, x, y, c]).astype(jnp.int32)
    here = scal(x)
    lane = jnp.arange(128)
    cos_own, sin_own = turns((sp * 8 + tp) * 128 + lane)
    block = (y - jnp.arange(4)) % 4
    cos_q, sin_q = turns((sp * 1024 + block[:, None] * 256 + c * 128 + lane[None, :]).reshape(-1))

    def sends(arrays, perms):
        out = []
        for a, perm in zip(arrays, perms):
            out.append(send(a, perm))
        return out

    q_up = q_up.T
    kv_up_other, q_up_other = sends([kv_up, q_up], [CORE] * 2)
    lat = down_call(
        tokens, norm_gain[None], kv_down, rope_down.T, kv_gain[None], q_down,
        q_gain.reshape(6, 128), cos_own, sin_own,
    )
    lats = [lat] + sends([lat] * 3, ALONG_Y[1:])
    near, q0, *moved = up_call(here, lats, kv_up, kv_up_other, q_up, q_up_other, cos_q, sin_q)
    moved = sends(moved, ALONG_Z[1:])
    turn = [ALONG_X[1], ALONG_X[3], ALONG_X[2]]
    near = [near] + sends([near] * 3, turn)
    far, queries = gather_call(q0, *moved)
    (other,) = sends([queries], [CORE])
    far = [far] + sends([far] * 3, turn)

    acc, qs = attention(here, near[0], far[0], (queries, other))
    for n, k in ((1, 1), (2, 3)):
        (acc,) = attention(scal((x - k) % 4), near[n], far[n], qs, acc)
    mine, theirs = attention(scal((x - 2) % 4), near[3], far[3], qs, acc, last=True)
    (theirs,) = sends([theirs], [CORE])
    result = merge_call(mine, theirs)
    ret = [result[0]] + sends(result[1:], [back(p) for p in ALONG_Z[1:]])
    parts = regroup_call(*ret)
    parts = [parts[0]] + sends(parts[1:], [back(p) for p in ALONG_Y[1:]])
    return out_call(here, parts, out_weight, out_gain[None])


def solution(mesh):
    return jax.shard_map(
        local,
        mesh=mesh,
        in_specs=(
            P(AXES, None),
            P(),
            P(),
            P(),
            P(),
            P(),
            P(),
            P(None, "tp"),
            P(None, "tp"),
            P(),
            P(),
        ),
        out_specs=P(AXES, None),
        check_vma=False,
    )
```

time: 366 us -> 152 us (0.42)
  the two profiles are of different devices: /device:TPU:102 before, /device:TPU:6 now
where the time goes in v1:
time: 152 us
  Pallas kernels  84.1 us (55%)
  waiting for transfers between devices  37.2 us (24%)
  starting transfers between devices  28.3 us (19%)
    pallas_call x4, Pallas kernels, attention(): pl.pallas_call(functools.partial(attn_kernel, first, last), out_shape=out...  71.4 us
    ppermute x22, waiting for transfers between devices, send(): return lax.ppermute(a, AXES, perm)  37.2 us
    ppermute x22, starting transfers between devices, send(): return lax.ppermute(a, AXES, perm)  28.3 us
    pallas_call x1, Pallas kernels, down_call(): pl.pallas_call(down_kernel, out_shape=jax.ShapeDtypeStruct((1312, rows),...  7.78 us
    pallas_call x1, Pallas kernels, out_call(): pl.pallas_call(out_kernel, out_shape=jax.ShapeDtypeStruct((128, w.shape[1...  3.18 us
  transfers between devices with their start and end apart: 22, of which 13 were waited for; matrix products, arithmetic and copies ran while one was open for 0% of the time, Pallas kernels for 36%

profile of v1, /device:TPU:6, one launch (start us, length us, event | category | flops | bytes accessed | tf_op | source)
XLA Modules:
  0.0 152.1 jit_solution(6589383845274363879)
XLA Ops:
  0.0 0.7 multiply_sine_fusion.1
  0.8 7.8 %down.1.p0 = bf16[1312,128]{1,0:T(8,128)(2,1)} custom-call(bf16[128,4096]{1,0:T(8,128)(2,1)} %tok.1, f32[1,4096]{1,0:T(1,128)} %bitcast.21, bf16[4096,512]{1,0:T(8,128)(2,1)} %kvd.1, bf16[32,4096]{1,0:T(8,128)(2,1)} %bitcast.20, f32[1,512]{1,0:T(1,128)} %bitcast.23, bf16[4096,768]{1,0:T(8,128)(2,1)} %qd.1, f32[6,128]{1,0:T(8,128)} %bitcast.22, ...), custom_call_target="tpu_custom_call" | custom-call | tf_op jit(solution)/shard_map/down/pallas_call | solution.py:110
  8.5 1.6 %collective-permute-start = (bf16[1312,128]{1,0:T(8,128)(2,1)}, bf16[1312,128]{1,0:T(8,128)(2,1)S(1)}, u32[]{:S(2)}, u32[]{:S(2)}) collective-permute-start(bf16[1312,128]{1,0:T(8,128)(2,1)} %down.1.p0), channel_id=1, source_target_pairs={{0,2},{1,3},{2,4},{3,5},{4,6},{5,7},{6,0},{7,1},{8,10},{9,11},{10,... | collective-permute-start | bytes 1007624 | tf_op jit(solution)/shard_map/ppermute | solution.py:47
  10.2 2.9 %collective-permute-start.1 = (bf16[1312,128]{1,0:T(8,128)(2,1)}, bf16[1312,128]{1,0:T(8,128)(2,1)S(1)}, u32[]{:S(2)}, u32[]{:S(2)}) collective-permute-start(bf16[1312,128]{1,0:T(8,128)(2,1)} %down.1.p0), channel_id=1, source_target_pairs={{0,4},{1,5},{2,6},{3,7},{4,0},{5,1},{6,2},{7,3},{8,12},{9,13},{10,... | collective-permute-start | bytes 1007624 | tf_op jit(solution)/shard_map/ppermute | solution.py:47
  13.1 1.3 collective-permute-start.2
  14.4 0.5 collective-permute-start.3
  15.0 0.1 stack.50.s.s_ref
  15.1 0.2 multiply_sine_fusion
  15.3 1.1 collective-permute-done.3.kv_other
  16.4 3.3 %collective-permute-done.p1 = bf16[1312,128]{1,0:T(8,128)(2,1)S(1)} collective-permute-done((bf16[1312,128]{1,0:T(8,128)(2,1)}, bf16[1312,128]{1,0:T(8,128)(2,1)S(1)}, u32[]{:S(2)}, u32[]{:S(2)}) %collective-permute-start) | collective-permute-done | bytes 335904 | tf_op jit(solution)/shard_map/ppermute | solution.py:47
  19.7 8.4 %collective-permute-done.1.p2 = bf16[1312,128]{1,0:T(8,128)(2,1)S(1)} collective-permute-done((bf16[1312,128]{1,0:T(8,128)(2,1)}, bf16[1312,128]{1,0:T(8,128)(2,1)S(1)}, u32[]{:S(2)}, u32[]{:S(2)}) %collective-permute-start.1) | collective-permute-done | bytes 335904 | tf_op jit(solution)/shard_map/ppermute | solution.py:47
  28.1 1.0 copy-done
  29.1 1.5 up.1
  30.5 2.0 %collective-permute-start.5 = (bf16[256,512]{1,0:T(8,128)(2,1)S(1)}, bf16[256,512]{1,0:T(8,128)(2,1)S(1)}, u32[]{:S(2)}, u32[]{:S(2)}) collective-permute-start(bf16[256,512]{1,0:T(8,128)(2,1)S(1)} %get-tuple-element.25), channel_id=1, source_target_pairs={{0,32},{1,33},{2,34},{3,35},{4,36},{5,37},{6,38},{7,39},{8,40},{9,... | collective-permute-start | bytes 786440 | tf_op jit(solution)/shard_map/ppermute | solution.py:47
  32.5 3.6 %collective-permute-start.6 = (bf16[256,512]{1,0:T(8,128)(2,1)S(1)}, bf16[256,512]{1,0:T(8,128)(2,1)S(1)}, u32[]{:S(2)}, u32[]{:S(2)}) collective-permute-start(bf16[256,512]{1,0:T(8,128)(2,1)S(1)} %get-tuple-element.26), channel_id=1, source_target_pairs={{0,64},{1,65},{2,66},{3,67},{4,68},{5,69},{6,70},{7,71},{8,72},{9,... | collective-permute-start | bytes 786440 | tf_op jit(solution)/shard_map/ppermute | solution.py:47
  36.1 1.0 collective-permute-start.7
  37.1 3.8 %collective-permute-done.5.m1 = bf16[256,512]{1,0:T(8,128)(2,1)S(1)} collective-permute-done((bf16[256,512]{1,0:T(8,128)(2,1)S(1)}, bf16[256,512]{1,0:T(8,128)(2,1)S(1)}, u32[]{:S(2)}, u32[]{:S(2)}) %collective-permute-start.5) | collective-permute-done | bytes 262176 | tf_op jit(solution)/shard_map/ppermute | solution.py:47
  40.9 6.0 %collective-permute-done.6.m2 = bf16[256,512]{1,0:T(8,128)(2,1)S(1)} collective-permute-done((bf16[256,512]{1,0:T(8,128)(2,1)S(1)}, bf16[256,512]{1,0:T(8,128)(2,1)S(1)}, u32[]{:S(2)}, u32[]{:S(2)}) %collective-permute-start.6) | collective-permute-done | bytes 262176 | tf_op jit(solution)/shard_map/ppermute | solution.py:47
  46.9 0.1 collective-permute-start.8
  47.0 0.5 collective-permute-start.14
  47.6 1.5 %collective-permute-start.12 = (bf16[480,512]{1,0:T(8,128)(2,1)S(1)}, bf16[480,512]{1,0:T(8,128)(2,1)S(1)}, u32[]{:S(2)}, u32[]{:S(2)}) collective-permute-start(bf16[480,512]{1,0:T(8,128)(2,1)S(1)} %get-tuple-element.30.refs_3_), channel_id=1, source_target_pairs={{0,24},{1,25},{2,26},{3,27},{4,28},{5,29},{6,30},{7,31},{8,0},{9,1... | collective-permute-start | bytes 1474568 | tf_op jit(solution)/shard_map/ppermute | solution.py:47
  49.1 1.4 collective-permute-start.10
  50.5 2.1 %collective-permute-start.13 = (bf16[160,512]{1,0:T(8,128)(2,1)S(1)}, bf16[160,512]{1,0:T(8,128)(2,1)S(1)}, u32[]{:S(2)}, u32[]{:S(2)}) collective-permute-start(bf16[160,512]{1,0:T(8,128)(2,1)S(1)} %get-tuple-element.29.refs_2_), channel_id=1, source_target_pairs={{0,8},{1,9},{2,10},{3,11},{4,12},{5,13},{6,14},{7,15},{8,16},{9,17... | collective-permute-start | bytes 491528 | tf_op jit(solution)/shard_map/ppermute | solution.py:47
  52.6 0.1 stack.56.s_ref
  52.7 0.1 stack.54.s_ref
  52.9 0.2 collective-permute-start.11
  53.1 20.0 %attn.4 = (f32[4,88,1024]{2,1,0:T(8,128)S(1)}, bf16[4,192,1024]{2,1,0:T(8,128)(2,1)S(1)}) custom-call(s32[5]{0:T(128)S(1)} %stack.50.s.s_ref, bf16[384,512]{1,0:T(8,128)(2,1)S(1)} %get-tuple-element.28.refs_0_, bf16[384,512]{1,0:T(8,128)(2,1)S(1)} %collective-permute-done.8.refs_1_, bf16[160,512]{1,0:T(8,128)(2,1)S(1)} %get-tuple-element.29.refs_2_, ...), custom_call_target="tpu_custom_call" | custom-call | flops 1500000000 | bytes 1048576 | tf_op jit(solution)/shard_map/attn/pallas_call | solution.py:345
  73.1 1.7 %collective-permute-done.13.refs_1_ = bf16[160,512]{1,0:T(8,128)(2,1)S(1)} collective-permute-done((bf16[160,512]{1,0:T(8,128)(2,1)S(1)}, bf16[160,512]{1,0:T(8,128)(2,1)S(1)}, u32[]{:S(2)}, u32[]{:S(2)}) %collective-permute-start.13) | collective-permute-done | bytes 163872 | tf_op jit(solution)/shard_map/ppermute | solution.py:47
  74.8 1.4 collective-permute-start.9
  76.2 17.1 %attn.5.refs_3_ = f32[4,88,1024]{2,1,0:T(8,128)S(1)} custom-call(s32[5]{0:T(128)S(1)} %stack.56.s_ref, bf16[4,192,1024]{2,1,0:T(8,128)(2,1)S(1)} %get-tuple-element.31.refs_0_, bf16[160,512]{1,0:T(8,128)(2,1)S(1)} %collective-permute-done.13.refs_1_, bf16[480,512]{1,0:T(8,128)(2,1)S(1)} %collective-permute-done.14.refs_2_, ...), custom_call_target="tpu_custom_call" | custom-call | flops 1500000000 | bytes 1048576 | tf_op jit(solution)/shard_map/attn/pallas_call | solution.py:345
  93.3 17.3 %attn.6.refs_3_ = f32[4,88,1024]{2,1,0:T(8,128)S(1)} custom-call(s32[5]{0:T(128)S(1)} %stack.54.s_ref, bf16[4,192,1024]{2,1,0:T(8,128)(2,1)S(1)} %get-tuple-element.31.refs_0_, bf16[160,512]{1,0:T(8,128)(2,1)S(1)} %collective-permute-done.11.refs_1_, bf16[480,512]{1,0:T(8,128)(2,1)S(1)} %collective-permute-done.12.refs_2_, f32[4,88,1024]{2,1,0:T(8,128)S(1)} %attn.5.refs_3_), custom_call_target="tpu_custom_call" | custom-call | flops 1500000000 | bytes 1048576 | tf_op jit(solution)/shard_map/attn/pallas_call | solution.py:345
  110.6 17.1 %attn.7 = (f32[4,88,512]{2,1,0:T(8,128)S(1)}, f32[4,88,512]{2,1,0:T(8,128)S(1)}) custom-call(s32[5]{0:T(128)S(1)} %stack.52.s_ref, bf16[4,192,1024]{2,1,0:T(8,128)(2,1)S(1)} %get-tuple-element.31.refs_0_, bf16[160,512]{1,0:T(8,128)(2,1)S(1)} %collective-permute-done.9.refs_1_, bf16[480,512]{1,0:T(8,128)(2,1)S(1)} %collective-permute-done.10.refs_2_, ...), custom_call_target="tpu_custom_call" | custom-call | flops 1500000000 | bytes 1048576 | tf_op jit(solution)/shard_map/attn/pallas_call | solution.py:345
  127.7 0.1 collective-permute-start.15
  127.8 2.2 %collective-permute-done.15.theirs = f32[4,88,512]{2,1,0:T(8,128)S(1)} collective-permute-done((f32[4,88,512]{2,1,0:T(8,128)S(1)}, f32[4,88,512]{2,1,0:T(8,128)S(1)}, u32[]{:S(2)}, u32[]{:S(2)}) %collective-permute-start.15) | collective-permute-done | bytes 720928 | tf_op jit(solution)/shard_map/ppermute | solution.py:47
  130.0 0.1 merge.1
  130.1 2.2 %collective-permute-start.16 = (bf16[64,512]{1,0:T(8,128)(2,1)S(1)}, bf16[64,512]{1,0:T(8,128)(2,1)S(1)}, u32[]{:S(2)}, u32[]{:S(2)}) collective-permute-start(bf16[64,512]{1,0:T(8,128)(2,1)S(1)} %get-tuple-element.36), channel_id=1, source_target_pairs={{32,0},{33,1},{34,2},{35,3},{36,4},{37,5},{38,6},{39,7},{40,8},{41... | collective-permute-start | bytes 196616 | tf_op jit(solution)/shard_map/ppermute | solution.py:47
  132.3 1.2 collective-permute-start.17
  133.5 0.3 collective-permute-start.18
  133.8 1.6 %collective-permute-done.16.r1 = bf16[64,512]{1,0:T(8,128)(2,1)S(1)} collective-permute-done((bf16[64,512]{1,0:T(8,128)(2,1)S(1)}, bf16[64,512]{1,0:T(8,128)(2,1)S(1)}, u32[]{:S(2)}, u32[]{:S(2)}) %collective-permute-start.16) | collective-permute-done | bytes 65568 | tf_op jit(solution)/shard_map/ppermute | solution.py:47
  135.5 2.9 %collective-permute-done.17.r2 = bf16[64,512]{1,0:T(8,128)(2,1)S(1)} collective-permute-done((bf16[64,512]{1,0:T(8,128)(2,1)S(1)}, bf16[64,512]{1,0:T(8,128)(2,1)S(1)}, u32[]{:S(2)}, u32[]{:S(2)}) %collective-permute-start.17) | collective-permute-done | bytes 65568 | tf_op jit(solution)/shard_map/ppermute | solution.py:47
  138.4 0.7 collective-permute-done.18.r3
  139.1 3.3 %collective-permute-start.19 = (bf16[256,128]{1,0:T(8,128)(2,1)S(1)}, bf16[256,128]{1,0:T(8,128)(2,1)S(1)}, u32[]{:S(2)}, u32[]{:S(2)}) collective-permute-start(bf16[256,128]{1,0:T(8,128)(2,1)S(1)} %get-tuple-element.40), channel_id=1, source_target_pairs={{2,0},{3,1},{4,2},{5,3},{6,4},{7,5},{0,6},{1,7},{10,8},{11,9},{12,... | collective-permute-start | bytes 196616 | tf_op jit(solution)/shard_map/ppermute | solution.py:47
  142.4 0.4 collective-permute-start.20
  142.8 0.5 collective-permute-start.21
  143.3 1.6 %collective-permute-done.19.t1 = bf16[256,128]{1,0:T(8,128)(2,1)S(1)} collective-permute-done((bf16[256,128]{1,0:T(8,128)(2,1)S(1)}, bf16[256,128]{1,0:T(8,128)(2,1)S(1)}, u32[]{:S(2)}, u32[]{:S(2)}) %collective-permute-start.19) | collective-permute-done | bytes 65568 | tf_op jit(solution)/shard_map/ppermute | solution.py:47
  144.9 3.3 %collective-permute-done.20.t2 = bf16[256,128]{1,0:T(8,128)(2,1)S(1)} collective-permute-done((bf16[256,128]{1,0:T(8,128)(2,1)S(1)}, bf16[256,128]{1,0:T(8,128)(2,1)S(1)}, u32[]{:S(2)}, u32[]{:S(2)}) %collective-permute-start.20) | collective-permute-done | bytes 65568 | tf_op jit(solution)/shard_map/ppermute | solution.py:47
  148.2 0.6 collective-permute-done.21.t3
  148.9 3.2 %out_proj.1 = bf16[128,4096]{1,0:T(8,128)(2,1)} custom-call(s32[5]{0:T(128)S(1)} %stack.50.s.s_ref, bf16[256,128]{1,0:T(8,128)(2,1)S(1)} %get-tuple-element.39.t0, bf16[256,128]{1,0:T(8,128)(2,1)S(1)} %collective-permute-done.19.t1, bf16[256,128]{1,0:T(8,128)(2,1)S(1)} %collective-permute-done.20.t2, bf16[256,128]{1,0:T(8,128)(2,1)S(1)} %collective-permute-done.21.t3, ...), custom_call_target="tpu_custom_call" | custom-call | tf_op jit(solution)/shard_map/out_proj/pallas_call | solution.py:388
  (29 shorter events, 0.3 us)
Async XLA Ops:
  0.7 13.7 %copy-start.1 = (bf16[768,192]{0,1:T(8,128)(2,1)S(1)}, bf16[768,192]{0,1:T(8,128)(2,1)}, u32[]{:S(2)}) copy-start(bf16[768,192]{0,1:T(8,128)(2,1)} %param.18) | copy-start | bytes 884740
  0.7 13.7 %copy-start.2 = (bf16[512,256]{1,0:T(8,128)(2,1)S(1)}, bf16[512,256]{1,0:T(8,128)(2,1)}, u32[]{:S(2)}) copy-start(bf16[512,256]{1,0:T(8,128)(2,1)} %kv_own.1) | copy-start | bytes 786436
  8.5 11.2 %collective-permute-start = (bf16[1312,128]{1,0:T(8,128)(2,1)}, bf16[1312,128]{1,0:T(8,128)(2,1)S(1)}, u32[]{:S(2)}, u32[]{:S(2)}) collective-permute-start(bf16[1312,128]{1,0:T(8,128)(2,1)} %down.1.p0), channel_id=1, source_target_pairs={{0,2},{1,3},{2,4},{3,5},{4,6},{5,7},{6,0},{7,1},{8,10},{9,11},{10,... | collective-permute-start | bytes 1007624 | tf_op jit(solution)/shard_map/ppermute | solution.py:47
  10.2 17.9 %collective-permute-start.1 = (bf16[1312,128]{1,0:T(8,128)(2,1)}, bf16[1312,128]{1,0:T(8,128)(2,1)S(1)}, u32[]{:S(2)}, u32[]{:S(2)}) collective-permute-start(bf16[1312,128]{1,0:T(8,128)(2,1)} %down.1.p0), channel_id=1, source_target_pairs={{0,4},{1,5},{2,6},{3,7},{4,0},{5,1},{6,2},{7,3},{8,12},{9,13},{10,... | collective-permute-start | bytes 1007624 | tf_op jit(solution)/shard_map/ppermute | solution.py:47
  13.1 15.0 %collective-permute-start.2 = (bf16[1312,128]{1,0:T(8,128)(2,1)}, bf16[1312,128]{1,0:T(8,128)(2,1)S(1)}, u32[]{:S(2)}, u32[]{:S(2)}) collective-permute-start(bf16[1312,128]{1,0:T(8,128)(2,1)} %down.1.p0), channel_id=1, source_target_pairs={{0,6},{1,7},{2,0},{3,1},{4,2},{5,3},{6,4},{7,5},{8,14},{9,15},{10,... | collective-permute-start | bytes 1007624 | tf_op jit(solution)/shard_map/ppermute | solution.py:47
  14.4 2.0 %collective-permute-start.4 = (bf16[192,768]{1,0:T(8,128)(2,1)S(1)}, bf16[192,768]{1,0:T(8,128)(2,1)S(1)}, u32[]{:S(2)}, u32[]{:S(2)}) collective-permute-start(bf16[192,768]{1,0:T(8,128)(2,1)S(1)} %bitcast.17), channel_id=1, source_target_pairs={{0,1},{1,0},{2,3},{3,2},{4,5},{5,4},{6,7},{7,6},{8,9},{9,8},{10,11... | collective-permute-start | bytes 884744 | tf_op jit(solution)/shard_map/ppermute | solution.py:47
  14.4 1.9 %collective-permute-start.3 = (bf16[512,256]{1,0:T(8,128)(2,1)S(1)}, bf16[512,256]{1,0:T(8,128)(2,1)S(1)}, u32[]{:S(2)}, u32[]{:S(2)}) collective-permute-start(bf16[512,256]{1,0:T(8,128)(2,1)S(1)} %copy-done.2), channel_id=1, source_target_pairs={{0,1},{1,0},{2,3},{3,2},{4,5},{5,4},{6,7},{7,6},{8,9},{9,8},{10,11... | collective-permute-start | bytes 786440 | tf_op jit(solution)/shard_map/ppermute | solution.py:47
  28.1 1.0 copy-start
  30.5 10.4 %collective-permute-start.5 = (bf16[256,512]{1,0:T(8,128)(2,1)S(1)}, bf16[256,512]{1,0:T(8,128)(2,1)S(1)}, u32[]{:S(2)}, u32[]{:S(2)}) collective-permute-start(bf16[256,512]{1,0:T(8,128)(2,1)S(1)} %get-tuple-element.25), channel_id=1, source_target_pairs={{0,32},{1,33},{2,34},{3,35},{4,36},{5,37},{6,38},{7,39},{8,40},{9,... | collective-permute-start | bytes 786440 | tf_op jit(solution)/shard_map/ppermute | solution.py:47
  32.5 14.4 %collective-permute-start.6 = (bf16[256,512]{1,0:T(8,128)(2,1)S(1)}, bf16[256,512]{1,0:T(8,128)(2,1)S(1)}, u32[]{:S(2)}, u32[]{:S(2)}) collective-permute-start(bf16[256,512]{1,0:T(8,128)(2,1)S(1)} %get-tuple-element.26), channel_id=1, source_target_pairs={{0,64},{1,65},{2,66},{3,67},{4,68},{5,69},{6,70},{7,71},{8,72},{9,... | collective-permute-start | bytes 786440 | tf_op jit(solution)/shard_map/ppermute | solution.py:47
  36.1 10.8 %collective-permute-start.7 = (bf16[256,512]{1,0:T(8,128)(2,1)S(1)}, bf16[256,512]{1,0:T(8,128)(2,1)S(1)}, u32[]{:S(2)}, u32[]{:S(2)}) collective-permute-start(bf16[256,512]{1,0:T(8,128)(2,1)S(1)} %get-tuple-element.27), channel_id=1, source_target_pairs={{0,96},{1,97},{2,98},{3,99},{4,100},{5,101},{6,102},{7,103},{8,104... | collective-permute-start | bytes 786440 | tf_op jit(solution)/shard_map/ppermute | solution.py:47
  46.9 6.0 %collective-permute-start.8 = (bf16[384,512]{1,0:T(8,128)(2,1)S(1)}, bf16[384,512]{1,0:T(8,128)(2,1)S(1)}, u32[]{:S(2)}, u32[]{:S(2)}) collective-permute-start(bf16[384,512]{1,0:T(8,128)(2,1)S(1)} %get-tuple-element.28.refs_0_), channel_id=1, source_target_pairs={{0,1},{1,0},{2,3},{3,2},{4,5},{5,4},{6,7},{7,6},{8,9},{9,8},{10,11... | collective-permute-start | bytes 1179656 | tf_op jit(solution)/shard_map/ppermute | solution.py:47
  47.0 29.1 %collective-permute-start.14 = (bf16[480,512]{1,0:T(8,128)(2,1)S(1)}, bf16[480,512]{1,0:T(8,128)(2,1)S(1)}, u32[]{:S(2)}, u32[]{:S(2)}) collective-permute-start(bf16[480,512]{1,0:T(8,128)(2,1)S(1)} %get-tuple-element.30.refs_3_), channel_id=1, source_target_pairs={{0,8},{1,9},{2,10},{3,11},{4,12},{5,13},{6,14},{7,15},{8,16},{9,17... | collective-permute-start | bytes 1474568 | tf_op jit(solution)/shard_map/ppermute | solution.py:47
  47.6 45.7 %collective-permute-start.12 = (bf16[480,512]{1,0:T(8,128)(2,1)S(1)}, bf16[480,512]{1,0:T(8,128)(2,1)S(1)}, u32[]{:S(2)}, u32[]{:S(2)}) collective-permute-start(bf16[480,512]{1,0:T(8,128)(2,1)S(1)} %get-tuple-element.30.refs_3_), channel_id=1, source_target_pairs={{0,24},{1,25},{2,26},{3,27},{4,28},{5,29},{6,30},{7,31},{8,0},{9,1... | collective-permute-start | bytes 1474568 | tf_op jit(solution)/shard_map/ppermute | solution.py:47
  49.1 61.4 %collective-permute-start.10 = (bf16[480,512]{1,0:T(8,128)(2,1)S(1)}, bf16[480,512]{1,0:T(8,128)(2,1)S(1)}, u32[]{:S(2)}, u32[]{:S(2)}) collective-permute-start(bf16[480,512]{1,0:T(8,128)(2,1)S(1)} %get-tuple-element.30.refs_3_), channel_id=1, source_target_pairs={{0,16},{1,17},{2,18},{3,19},{4,20},{5,21},{6,22},{7,23},{8,24},{9,... | collective-permute-start | bytes 1474568 | tf_op jit(solution)/shard_map/ppermute | solution.py:47
  50.5 24.2 %collective-permute-start.13 = (bf16[160,512]{1,0:T(8,128)(2,1)S(1)}, bf16[160,512]{1,0:T(8,128)(2,1)S(1)}, u32[]{:S(2)}, u32[]{:S(2)}) collective-permute-start(bf16[160,512]{1,0:T(8,128)(2,1)S(1)} %get-tuple-element.29.refs_2_), channel_id=1, source_target_pairs={{0,8},{1,9},{2,10},{3,11},{4,12},{5,13},{6,14},{7,15},{8,16},{9,17... | collective-permute-start | bytes 491528 | tf_op jit(solution)/shard_map/ppermute | solution.py:47
  52.9 40.4 %collective-permute-start.11 = (bf16[160,512]{1,0:T(8,128)(2,1)S(1)}, bf16[160,512]{1,0:T(8,128)(2,1)S(1)}, u32[]{:S(2)}, u32[]{:S(2)}) collective-permute-start(bf16[160,512]{1,0:T(8,128)(2,1)S(1)} %get-tuple-element.29.refs_2_), channel_id=1, source_target_pairs={{0,24},{1,25},{2,26},{3,27},{4,28},{5,29},{6,30},{7,31},{8,0},{9,1... | collective-permute-start | bytes 491528 | tf_op jit(solution)/shard_map/ppermute | solution.py:47
  74.8 35.8 %collective-permute-start.9 = (bf16[160,512]{1,0:T(8,128)(2,1)S(1)}, bf16[160,512]{1,0:T(8,128)(2,1)S(1)}, u32[]{:S(2)}, u32[]{:S(2)}) collective-permute-start(bf16[160,512]{1,0:T(8,128)(2,1)S(1)} %get-tuple-element.29.refs_2_), channel_id=1, source_target_pairs={{0,16},{1,17},{2,18},{3,19},{4,20},{5,21},{6,22},{7,23},{8,24},{9,... | collective-permute-start | bytes 491528 | tf_op jit(solution)/shard_map/ppermute | solution.py:47
  76.2 72.7 %slice-start = ((s8[8388608]{0:T(1024)(128)(4,1)}), s8[4194304]{0:T(1024)(128)(4,1)S(1)}, s32[]{:S(2)}) async-start(s8[8388608]{0:T(1024)(128)(4,1)} %bitcast.15), calls=%async_computation | async-start | bytes 8388608
  93.2 55.6 %slice-start.1 = ((s8[8388608]{0:T(1024)(128)(4,1)}), s8[4194304]{0:T(1024)(128)(4,1)S(1)}, s32[]{:S(2)}) async-start(s8[8388608]{0:T(1024)(128)(4,1)} %bitcast.15), calls=%async_computation.1 | async-start | bytes 8388608
  127.7 21.2 %copy-start.3 = (f32[4096]{0:T(1024)S(1)}, f32[4096]{0:T(1024)}, u32[]{:S(2)}) copy-start(f32[4096]{0:T(1024)} %param.21) | copy-start | bytes 49156
  127.7 2.3 %collective-permute-start.15 = (f32[4,88,512]{2,1,0:T(8,128)S(1)}, f32[4,88,512]{2,1,0:T(8,128)S(1)}, u32[]{:S(2)}, u32[]{:S(2)}) collective-permute-start(f32[4,88,512]{2,1,0:T(8,128)S(1)} %get-tuple-element.34), channel_id=1, source_target_pairs={{0,1},{1,0},{2,3},{3,2},{4,5},{5,4},{6,7},{7,6},{8,9},{9,8},{10,11... | collective-permute-start | bytes 2162696 | tf_op jit(solution)/shard_map/ppermute | solution.py:47
  130.1 5.3 %collective-permute-start.16 = (bf16[64,512]{1,0:T(8,128)(2,1)S(1)}, bf16[64,512]{1,0:T(8,128)(2,1)S(1)}, u32[]{:S(2)}, u32[]{:S(2)}) collective-permute-start(bf16[64,512]{1,0:T(8,128)(2,1)S(1)} %get-tuple-element.36), channel_id=1, source_target_pairs={{32,0},{33,1},{34,2},{35,3},{36,4},{37,5},{38,6},{39,7},{40,8},{41... | collective-permute-start | bytes 196616 | tf_op jit(solution)/shard_map/ppermute | solution.py:47
  132.3 6.1 %collective-permute-start.17 = (bf16[64,512]{1,0:T(8,128)(2,1)S(1)}, bf16[64,512]{1,0:T(8,128)(2,1)S(1)}, u32[]{:S(2)}, u32[]{:S(2)}) collective-permute-start(bf16[64,512]{1,0:T(8,128)(2,1)S(1)} %get-tuple-element.37), channel_id=1, source_target_pairs={{64,0},{65,1},{66,2},{67,3},{68,4},{69,5},{70,6},{71,7},{72,8},{73... | collective-permute-start | bytes 196616 | tf_op jit(solution)/shard_map/ppermute | solution.py:47
  133.5 5.6 %collective-permute-start.18 = (bf16[64,512]{1,0:T(8,128)(2,1)S(1)}, bf16[64,512]{1,0:T(8,128)(2,1)S(1)}, u32[]{:S(2)}, u32[]{:S(2)}) collective-permute-start(bf16[64,512]{1,0:T(8,128)(2,1)S(1)} %get-tuple-element.38), channel_id=1, source_target_pairs={{96,0},{97,1},{98,2},{99,3},{100,4},{101,5},{102,6},{103,7},{104,8... | collective-permute-start | bytes 196616 | tf_op jit(solution)/shard_map/ppermute | solution.py:47
  139.1 5.8 %collective-permute-start.19 = (bf16[256,128]{1,0:T(8,128)(2,1)S(1)}, bf16[256,128]{1,0:T(8,128)(2,1)S(1)}, u32[]{:S(2)}, u32[]{:S(2)}) collective-permute-start(bf16[256,128]{1,0:T(8,128)(2,1)S(1)} %get-tuple-element.40), channel_id=1, source_target_pairs={{2,0},{3,1},{4,2},{5,3},{6,4},{7,5},{0,6},{1,7},{10,8},{11,9},{12,... | collective-permute-start | bytes 196616 | tf_op jit(solution)/shard_map/ppermute | solution.py:47
  142.4 5.8 %collective-permute-start.20 = (bf16[256,128]{1,0:T(8,128)(2,1)S(1)}, bf16[256,128]{1,0:T(8,128)(2,1)S(1)}, u32[]{:S(2)}, u32[]{:S(2)}) collective-permute-start(bf16[256,128]{1,0:T(8,128)(2,1)S(1)} %get-tuple-element.41), channel_id=1, source_target_pairs={{4,0},{5,1},{6,2},{7,3},{0,4},{1,5},{2,6},{3,7},{12,8},{13,9},{14,... | collective-permute-start | bytes 196616 | tf_op jit(solution)/shard_map/ppermute | solution.py:47
  142.8 6.0 %collective-permute-start.21 = (bf16[256,128]{1,0:T(8,128)(2,1)S(1)}, bf16[256,128]{1,0:T(8,128)(2,1)S(1)}, u32[]{:S(2)}, u32[]{:S(2)}) collective-permute-start(bf16[256,128]{1,0:T(8,128)(2,1)S(1)} %get-tuple-element.42), channel_id=1, source_target_pairs={{6,0},{7,1},{0,2},{1,3},{2,4},{3,5},{4,6},{5,7},{14,8},{15,9},{8,1... | collective-permute-start | bytes 196616 | tf_op jit(solution)/shard_map/ppermute | solution.py:47

commit v2 on v1

--- a/solution.py
+++ b/solution.py
@@ -55,7 +55,7 @@
 
 
 def down_kernel(
-    tok, gain, kvd, rd, kvg, qd, qg, cos, sin, out,
+    tok, gain, kvd, rd, kvg, qd, qg, cos, sin, out, q_out,
     tok_v, gain_v, kvd_v, rd_v, kvg_v, qd_v, qg_v, normed, sems,
 ):
     step = kvd.shape[0] // CHUNKS
@@ -101,7 +101,7 @@
     total = product("q", qd_v)
     copies["qg"].wait()
     gain_q = jnp.concatenate([qg_v[n : n + 1, :] for n in range(6)], axis=1)
-    out[544:1312, :] = normed_rows(total, gain_q).T.astype(BF)
+    q_out[...] = normed_rows(total, gain_q).T.astype(BF)
 
 
 def down_call(tok, gain, kvd, rd, kvg, qd, qg, cos, sin):
@@ -109,9 +109,9 @@
     step = d // CHUNKS
     return pl.pallas_call(
         down_kernel,
-        out_shape=jax.ShapeDtypeStruct((1312, rows), BF),
+        out_shape=[jax.ShapeDtypeStruct((544, rows), BF), jax.ShapeDtypeStruct((768, rows), BF)],
         in_specs=[pl.BlockSpec(memory_space=pl.ANY)] * 7 + [VM] * 2,
-        out_specs=VM,
+        out_specs=[VM] * 2,
         scratch_shapes=[
             pltpu.VMEM((rows, d), BF),
             pltpu.VMEM((1, d), F32),
@@ -127,70 +127,76 @@
     )(tok, gain, kvd, rd, kvg, qd, qg, cos, sin)
 
 
-def up_kernel(
-    s, p0, p1, p2, p3, kv_own, kv_other, q_own, q_other, cos, sin,
-    near, q0, m1, m2, m3, kv_w, q_w, kv, q,
-):
+def kv_up_kernel(s, p0, p1, p2, p3, own, other, o0, o1, o2, o3, w, kv):
     z, c = s[1], s[4]
     parts = (p0, p1, p2, p3)
-    kv_w[0:256, :] = kv_own[...].T
-    kv_w[256:512, :] = kv_other[...].T
-    q_w[0:192, :] = q_own[...]
-    q_w[192:384, :] = q_other[...]
+    w[0:256, :] = own[...].T
+    w[256:512, :] = other[...].T
     lat = jnp.concatenate([p[0:512, :] for p in parts], axis=1)
     rot = jnp.concatenate([p[512:544, :] for p in parts], axis=1)
-    kv[...] = jnp.dot(kv_w[...], lat, preferred_element_type=F32).astype(BF)
-    lat = jnp.concatenate([p[544:1312, :] for p in parts], axis=1)
-    q[...] = jnp.dot(q_w[...], lat, preferred_element_type=F32)
-    for k, out in enumerate((None, m1, m2, m3)):
-        head = (z + k - 2 * c + 4) & 3
-        at = head * 128
-        to = near if k == 0 else out
+    kv[...] = jnp.dot(w[...], lat, preferred_element_type=F32).astype(BF)
+    for k, to in enumerate((o0, o1, o2, o3)):
+        at = ((z + k - 2 * c + 4) & 3) * 128
         to[0:64, :] = kv[pl.ds(pl.multiple_of(at, 128), 64), :]
         to[64:96, :] = rot
         to[96:160, :] = kv[pl.ds(pl.multiple_of(at + 64, 64), 64), :]
-        to, low = (q0, 0) if k == 0 else (out, 160)
-        at = head * 96
+
+
+def kv_up_call(s, parts, own, other):
+    return pl.pallas_call(
+        kv_up_kernel,
+        out_shape=[jax.ShapeDtypeStruct((160, 512), BF)] * 4,
+        in_specs=[SM] + [VM] * 6,
+        out_specs=[VM] * 4,
+        scratch_shapes=[pltpu.VMEM((512, 512), BF)] * 2,
+        compiler_params=small(8),
+        name="kv_up",
+    )(s, *parts, own, other)
+
+
+def q_up_kernel(s, p0, p1, p2, p3, own, other, cos, sin, o0, o1, o2, o3, w, q):
+    z, c = s[1], s[4]
+    w[0:192, :] = own[...]
+    w[192:384, :] = other[...]
+    lat = jnp.concatenate([p[...] for p in (p0, p1, p2, p3)], axis=1)
+    q[...] = jnp.dot(w[...], lat, preferred_element_type=F32)
+    for k, to in enumerate((o0, o1, o2, o3)):
+        at = ((z + k - 2 * c + 4) & 3) * 96
         left = q[pl.ds(pl.multiple_of(at + 64, 32), 16), :]
         right = q[pl.ds(pl.multiple_of(at + 80, 16), 16), :]
-        to[low : low + 64, :] = q[pl.ds(pl.multiple_of(at, 32), 64), :].astype(BF)
-        to[low + 64 : low + 80, :] = (left * cos[...] - right * sin[...]).astype(BF)
-        to[low + 80 : low + 96, :] = (right * cos[...] + left * sin[...]).astype(BF)
-
-
-def up_call(s, parts, *rest):
-    piece = lambda rows: jax.ShapeDtypeStruct((rows, 512), BF)
-    return pl.pallas_call(
-        up_kernel,
-        out_shape=[piece(160), piece(96)] + [piece(256)] * 3,
-        in_specs=[SM] + [VM] * 10,
-        out_specs=[VM] * 5,
-        scratch_shapes=[
-            pltpu.VMEM((512, 512), BF),
-            pltpu.VMEM((384, 768), BF),
-            pltpu.VMEM((512, 512), BF),
-            pltpu.VMEM((384, 512), F32),
-        ],
-        compiler_params=small(16),
-        name="up",
-    )(s, *parts, *rest)
-
-
-def gather_kernel(q0, m1, m2, m3, far, q):
-    q[0:96, :] = q0[...]
-    for n, m in enumerate((m1, m2, m3)):
-        far[160 * n : 160 * n + 160, :] = m[0:160, :]
-        q[96 * n + 96 : 96 * n + 192, :] = m[160:256, :]
-
-
-def gather_call(*pieces):
-    return pl.pallas_call(
-        gather_kernel,
-        out_shape=[jax.ShapeDtypeStruct((480, 512), BF), jax.ShapeDtypeStruct((384, 512), BF)],
-        in_specs=[VM] * 4,
-        out_specs=[VM] * 2,
+        to[0:64, :] = q[pl.ds(pl.multiple_of(at, 32), 64), :].astype(BF)
+        to[64:80, :] = (left * cos[...] - right * sin[...]).astype(BF)
+        to[80:96, :] = (right * cos[...] + left * sin[...]).astype(BF)
+
+
+def q_up_call(s, parts, own, other, cos, sin):
+    return pl.pallas_call(
+        q_up_kernel,
+        out_shape=[jax.ShapeDtypeStruct((96, 512), BF)] * 4,
+        in_specs=[SM] + [VM] * 8,
+        out_specs=[VM] * 4,
+        scratch_shapes=[pltpu.VMEM((384, 768), BF), pltpu.VMEM((384, 512), F32)],
+        compiler_params=small(10),
+        name="q_up",
+    )(s, *parts, own, other, cos, sin)
+
+
+def join_kernel(*refs):
+    at = 0
+    for r in refs[:-1]:
+        refs[-1][at : at + r.shape[0], :] = r[...]
+        at += r.shape[0]
+
+
+def join_call(*pieces):
+    rows = sum(p.shape[0] for p in pieces)
+    return pl.pallas_call(
+        join_kernel,
+        out_shape=jax.ShapeDtypeStruct((rows, 512), BF),
+        in_specs=[VM] * len(pieces),
+        out_specs=VM,
         compiler_params=small(8),
-        name="gather",
+        name="join",
     )(*pieces)
 
 
@@ -239,19 +245,16 @@
     for k in range(4):
         if first:
             for h, v in enumerate((own, other)):
-                q = v[96 * k : 96 * k + 96, :].astype(F32) * SCALE
-                high = q.astype(BF)
-                qs[k, 0:96, 512 * h : 512 * h + 512] = high
-                qs[k, 96:192, 512 * h : 512 * h + 512] = (q - high.astype(F32)).astype(BF)
+                qs[k, :, 512 * h : 512 * h + 512] = v[96 * k : 96 * k + 96, :]
         r, at = (near, 0) if k == 0 else (far, 160 * (k - 1))
         kt = r[at : at + 96, :]
-        ks[k] = jnp.concatenate([kt, kt], axis=0).T
+        ks[k] = kt.T
         vs[k, 0:64, :] = r[at + 96 : at + 160, :]
         vs[k, 64:80, :] = ones
 
     def exact(kq, kk, free):
         m_old = m_ref[kq]
-        s = jnp.dot(ks[kk], qs[kq], preferred_element_type=F32)
+        s = jnp.dot(ks[kk], qs[kq], preferred_element_type=F32) * SCALE
         kr = lax.broadcasted_iota(jnp.int32, (512, 1024), 0)
         qr = lax.broadcasted_iota(jnp.int32, (512, 1024), 1)
         kpos = ((y - (kr >> 7)) & 3) * 256 + c * 128 + (kr & 127)
@@ -272,11 +275,11 @@
             s = jnp.dot(ks[kk], q, preferred_element_type=F32)
             high = jnp.max(s.reshape(64, 8, 1024), axis=0)
             peak = high if peak is None else jnp.maximum(peak, high)
-            p = jnp.exp2(s - m).astype(BF)
+            p = jnp.exp2(s * SCALE - m).astype(BF)
             d = jnp.dot(vs[kk], p, preferred_element_type=F32)
             o = d if o is None else o + d
         acc_ref[kq, 0:80] += o
-        top[...] = jnp.maximum(top[...], peak - m)
+        top[...] = jnp.maximum(top[...], peak * SCALE - m)
 
     def walk(quick):
         @pl.loop(0, 4)
@@ -285,7 +288,14 @@
             full = zq + jnp.where(xk < x, 1, 0)
 
             diag = jnp.where(xk == x, 1, 0)
-            some = 1 if first else jnp.where(zq == 0, 1, 0)
+            some = 0 if first else jnp.where(zq == 0, 1, 0)
+            if first:
+
+                @pl.when(jnp.logical_and(quick, full > 0))
+                def _():
+                    s = jnp.dot(ks[z & 3, 0:128], qs[kq], preferred_element_type=F32) * SCALE
+                    m_ref[kq] = jnp.max(s, axis=0, keepdims=True)
+
             start = jnp.minimum(jnp.where(quick, some, full), full)
 
             @pl.loop(1 - diag, start + 1)
@@ -329,13 +339,13 @@
     first = state is None
     outs = [jax.ShapeDtypeStruct((4, 88, 1024), F32)]
     scratch = [
-        pltpu.VMEM((4, 512, 192), BF),
+        pltpu.VMEM((4, 512, 96), BF),
         pltpu.VMEM((4, 80, 512), BF),
         pltpu.VMEM((8, 1024), F32),
         pltpu.VMEM((4, 1, 1024), F32),
     ]
     if first:
-        outs.append(jax.ShapeDtypeStruct((4, 192, 1024), BF))
+        outs.append(jax.ShapeDtypeStruct((4, 96, 1024), BF))
         args = (scal, *queries, near, far)
     else:
         args = (scal, queries, near, far, state)
@@ -420,18 +430,22 @@
 
     q_up = q_up.T
     kv_up_other, q_up_other = sends([kv_up, q_up], [CORE] * 2)
-    lat = down_call(
+    lat, q_lat = down_call(
         tokens, norm_gain[None], kv_down, rope_down.T, kv_gain[None], q_down,
         q_gain.reshape(6, 128), cos_own, sin_own,
     )
     lats = [lat] + sends([lat] * 3, ALONG_Y[1:])
-    near, q0, *moved = up_call(here, lats, kv_up, kv_up_other, q_up, q_up_other, cos_q, sin_q)
+    q_lats = [q_lat] + sends([q_lat] * 3, ALONG_Y[1:])
+    near, *moved = kv_up_call(here, lats, kv_up, kv_up_other)
     moved = sends(moved, ALONG_Z[1:])
+    q0, *q_moved = q_up_call(here, q_lats, q_up, q_up_other, cos_q, sin_q)
+    q_moved = sends(q_moved, ALONG_Z[1:])
     turn = [ALONG_X[1], ALONG_X[3], ALONG_X[2]]
     near = [near] + sends([near] * 3, turn)
-    far, queries = gather_call(q0, *moved)
+    far = join_call(*moved)
+    far = [far] + sends([far] * 3, turn)
+    queries = join_call(q0, *q_moved)
     (other,) = sends([queries], [CORE])
-    far = [far] + sends([far] * 3, turn)
 
     acc, qs = attention(here, near[0], far[0], (queries, other))
     for n, k in ((1, 1), (2, 3)):

time: 152 us -> 151 us (level)
  waiting for transfers between devices: 37.2 us -> 27.4 us
  starting transfers between devices: 28.3 us -> 36.7 us
    ppermute x22 -> x28, waiting for transfers between devices: 37.2 us -> 27.4 us  [send(): return lax.ppermute(a, AXES, perm)]
    ppermute x22 -> x28, starting transfers between devices: 28.3 us -> 36.7 us  [send(): return lax.ppermute(a, AXES, perm)]
    pallas_call x3 -> x5, Pallas kernels: 9.29 us -> 9.93 us  [the longest x1 7.73 us: down_call(): pl.pallas_call(down_kernel, out_shape=[jax.ShapeDtypeStruct((544, rows),...]
  transfers between devices with their start and end apart: 22 -> 28, of which waited for: 13 -> 13; matrix products, arithmetic and copies ran while one was open for 0% -> 0% of each run, Pallas kernels for 36% -> 37%
where the time goes in v2:
time: 151 us
  Pallas kernels  83.6 us (55%)
  starting transfers between devices  36.7 us (24%)
  waiting for transfers between devices  27.4 us (18%)
  local copies, waits for them, and re-layouts  2.2 us (1%)
    pallas_call x4, Pallas kernels, attention(): pl.pallas_call(functools.partial(attn_kernel, first, last), out_shape=out...  70.3 us
    ppermute x28, starting transfers between devices, send(): return lax.ppermute(a, AXES, perm)  36.7 us
    ppermute x28, waiting for transfers between devices, send(): return lax.ppermute(a, AXES, perm)  27.4 us
    pallas_call x1, Pallas kernels, down_call(): pl.pallas_call(down_kernel, out_shape=[jax.ShapeDtypeStruct((544, rows),...  7.73 us
    pallas_call x1, Pallas kernels, out_call(): pl.pallas_call(out_kernel, out_shape=jax.ShapeDtypeStruct((128, w.shape[1...  3.21 us
  transfers between devices with their start and end apart: 28, of which 13 were waited for; matrix products, arithmetic and copies ran while one was open for 0% of the time, Pallas kernels for 37%

profile of v2, /device:TPU:6, one launch (start us, length us, event | category | flops | bytes accessed | tf_op | source)
XLA Modules:
  0.0 151.1 jit_solution(14961246054594326341)
XLA Ops:
  0.0 0.7 multiply_sine_fusion.1
  0.7 7.7 %down.1 = (bf16[544,128]{1,0:T(8,128)(2,1)}, bf16[768,128]{1,0:T(8,128)(2,1)}) custom-call(bf16[128,4096]{1,0:T(8,128)(2,1)} %tok.1, f32[1,4096]{1,0:T(1,128)} %bitcast.21, bf16[4096,512]{1,0:T(8,128)(2,1)} %kvd.1, bf16[32,4096]{1,0:T(8,128)(2,1)} %bitcast.20, f32[1,512]{1,0:T(1,128)} %bitcast.23, bf16[4096,768]{1,0:T(8,128)(2,1)} %qd.1, f32[6,128]{1,0:T(8,128)} %bitcast.22, ...), custom_call_target="tpu_custom_call" | custom-call | tf_op jit(solution)/shard_map/down/pallas_call | solution.py:110
  8.5 1.6 %collective-permute-start = (bf16[768,128]{1,0:T(8,128)(2,1)}, bf16[768,128]{1,0:T(8,128)(2,1)S(1)}, u32[]{:S(2)}, u32[]{:S(2)}) collective-permute-start(bf16[768,128]{1,0:T(8,128)(2,1)} %get-tuple-element.27.p0), channel_id=1, source_target_pairs={{0,2},{1,3},{2,4},{3,5},{4,6},{5,7},{6,0},{7,1},{8,10},{9,11},{10,... | collective-permute-start | bytes 589832 | tf_op jit(solution)/shard_map/ppermute | solution.py:47
  10.1 2.9 %collective-permute-start.1 = (bf16[768,128]{1,0:T(8,128)(2,1)}, bf16[768,128]{1,0:T(8,128)(2,1)S(1)}, u32[]{:S(2)}, u32[]{:S(2)}) collective-permute-start(bf16[768,128]{1,0:T(8,128)(2,1)} %get-tuple-element.27.p0), channel_id=1, source_target_pairs={{0,4},{1,5},{2,6},{3,7},{4,0},{5,1},{6,2},{7,3},{8,12},{9,13},{10,... | collective-permute-start | bytes 589832 | tf_op jit(solution)/shard_map/ppermute | solution.py:47
  13.0 1.3 collective-permute-start.2
  14.5 2.2 %collective-permute-done.p1 = bf16[768,128]{1,0:T(8,128)(2,1)S(1)} collective-permute-done((bf16[768,128]{1,0:T(8,128)(2,1)}, bf16[768,128]{1,0:T(8,128)(2,1)S(1)}, u32[]{:S(2)}, u32[]{:S(2)}) %collective-permute-start) | collective-permute-done | bytes 196640 | tf_op jit(solution)/shard_map/ppermute | solution.py:47
  16.7 1.4 collective-permute-start.8
  18.1 5.1 %collective-permute-done.1.p2 = bf16[768,128]{1,0:T(8,128)(2,1)S(1)} collective-permute-done((bf16[768,128]{1,0:T(8,128)(2,1)}, bf16[768,128]{1,0:T(8,128)(2,1)S(1)}, u32[]{:S(2)}, u32[]{:S(2)}) %collective-permute-start.1) | collective-permute-done | bytes 196640 | tf_op jit(solution)/shard_map/ppermute | solution.py:47
  23.2 0.7 collective-permute-start.9
  23.9 0.2 multiply_sine_fusion
  24.2 0.9 copy-done.2
  25.1 1.1 q_up.1
  26.2 2.0 %collective-permute-start.4 = (bf16[96,512]{1,0:T(8,128)(2,1)S(1)}, bf16[96,512]{1,0:T(8,128)(2,1)S(1)}, u32[]{:S(2)}, u32[]{:S(2)}) collective-permute-start(bf16[96,512]{1,0:T(8,128)(2,1)S(1)} %get-tuple-element.29), channel_id=1, source_target_pairs={{0,32},{1,33},{2,34},{3,35},{4,36},{5,37},{6,38},{7,39},{8,40},{9,... | collective-permute-start | bytes 294920 | tf_op jit(solution)/shard_map/ppermute | solution.py:47
  28.2 1.7 %collective-permute-done.9.p2 = bf16[544,128]{1,0:T(8,128)(2,1)S(1)} collective-permute-done((bf16[544,128]{1,0:T(8,128)(2,1)}, bf16[544,128]{1,0:T(8,128)(2,1)S(1)}, u32[]{:S(2)}, u32[]{:S(2)}) %collective-permute-start.9) | collective-permute-done | bytes 139296 | tf_op jit(solution)/shard_map/ppermute | solution.py:47
  30.0 0.9 copy-done.3
  30.9 1.0 kv_up.1
  31.9 2.0 %collective-permute-start.12 = (bf16[160,512]{1,0:T(8,128)(2,1)S(1)}, bf16[160,512]{1,0:T(8,128)(2,1)S(1)}, u32[]{:S(2)}, u32[]{:S(2)}) collective-permute-start(bf16[160,512]{1,0:T(8,128)(2,1)S(1)} %get-tuple-element.34), channel_id=1, source_target_pairs={{0,32},{1,33},{2,34},{3,35},{4,36},{5,37},{6,38},{7,39},{8,40},{9,... | collective-permute-start | bytes 491528 | tf_op jit(solution)/shard_map/ppermute | solution.py:47
  33.9 3.6 %collective-permute-start.13 = (bf16[160,512]{1,0:T(8,128)(2,1)S(1)}, bf16[160,512]{1,0:T(8,128)(2,1)S(1)}, u32[]{:S(2)}, u32[]{:S(2)}) collective-permute-start(bf16[160,512]{1,0:T(8,128)(2,1)S(1)} %get-tuple-element.35), channel_id=1, source_target_pairs={{0,64},{1,65},{2,66},{3,67},{4,68},{5,69},{6,70},{7,71},{8,72},{9,... | collective-permute-start | bytes 491528 | tf_op jit(solution)/shard_map/ppermute | solution.py:47
  37.5 1.0 collective-permute-start.14
  38.5 0.5 collective-permute-start.5
  39.1 3.1 %collective-permute-start.6 = (bf16[96,512]{1,0:T(8,128)(2,1)S(1)}, bf16[96,512]{1,0:T(8,128)(2,1)S(1)}, u32[]{:S(2)}, u32[]{:S(2)}) collective-permute-start(bf16[96,512]{1,0:T(8,128)(2,1)S(1)} %get-tuple-element.31), channel_id=1, source_target_pairs={{0,96},{1,97},{2,98},{3,99},{4,100},{5,101},{6,102},{7,103},{8,104... | collective-permute-start | bytes 294920 | tf_op jit(solution)/shard_map/ppermute | solution.py:47
  42.2 2.5 %collective-permute-done.5.refs_2_ = bf16[96,512]{1,0:T(8,128)(2,1)S(1)} collective-permute-done((bf16[96,512]{1,0:T(8,128)(2,1)S(1)}, bf16[96,512]{1,0:T(8,128)(2,1)S(1)}, u32[]{:S(2)}, u32[]{:S(2)}) %collective-permute-start.5) | collective-permute-done | bytes 98336 | tf_op jit(solution)/shard_map/ppermute | solution.py:47
  44.7 1.5 %collective-permute-done.6.refs_3_ = bf16[96,512]{1,0:T(8,128)(2,1)S(1)} collective-permute-done((bf16[96,512]{1,0:T(8,128)(2,1)S(1)}, bf16[96,512]{1,0:T(8,128)(2,1)S(1)}, u32[]{:S(2)}, u32[]{:S(2)}) %collective-permute-start.6) | collective-permute-done | bytes 98336 | tf_op jit(solution)/shard_map/ppermute | solution.py:47
  46.4 0.5 collective-permute-start.20
  46.9 1.5 %collective-permute-start.18 = (bf16[480,512]{1,0:T(8,128)(2,1)S(1)}, bf16[480,512]{1,0:T(8,128)(2,1)S(1)}, u32[]{:S(2)}, u32[]{:S(2)}) collective-permute-start(bf16[480,512]{1,0:T(8,128)(2,1)S(1)} %join.3.refs_3_), channel_id=1, source_target_pairs={{0,24},{1,25},{2,26},{3,27},{4,28},{5,29},{6,30},{7,31},{8,0},{9,1... | collective-permute-start | bytes 1474568 | tf_op jit(solution)/shard_map/ppermute | solution.py:47
  48.5 1.4 collective-permute-start.16
  49.9 2.1 %collective-permute-start.19 = (bf16[160,512]{1,0:T(8,128)(2,1)S(1)}, bf16[160,512]{1,0:T(8,128)(2,1)S(1)}, u32[]{:S(2)}, u32[]{:S(2)}) collective-permute-start(bf16[160,512]{1,0:T(8,128)(2,1)S(1)} %get-tuple-element.33.refs_2_), channel_id=1, source_target_pairs={{0,8},{1,9},{2,10},{3,11},{4,12},{5,13},{6,14},{7,15},{8,16},{9,17... | collective-permute-start | bytes 491528 | tf_op jit(solution)/shard_map/ppermute | solution.py:47
  52.3 0.2 collective-permute-start.17
  52.5 19.0 %attn.4 = (f32[4,88,1024]{2,1,0:T(8,128)S(1)}, bf16[4,96,1024]{2,1,0:T(8,128)(2,1)S(1)}) custom-call(s32[5]{0:T(128)S(1)} %stack.50.s.s_ref, bf16[384,512]{1,0:T(8,128)(2,1)S(1)} %join.2.refs_0_, bf16[384,512]{1,0:T(8,128)(2,1)S(1)} %collective-permute-done.7.refs_1_, bf16[160,512]{1,0:T(8,128)(2,1)S(1)} %get-tuple-element.33.refs_2_, ...), custom_call_target="tpu_custom_call" | custom-call | flops 1500000000 | bytes 1048576 | tf_op jit(solution)/shard_map/attn/pallas_call | solution.py:355
  71.5 2.7 %collective-permute-done.19.refs_1_ = bf16[160,512]{1,0:T(8,128)(2,1)S(1)} collective-permute-done((bf16[160,512]{1,0:T(8,128)(2,1)S(1)}, bf16[160,512]{1,0:T(8,128)(2,1)S(1)}, u32[]{:S(2)}, u32[]{:S(2)}) %collective-permute-start.19) | collective-permute-done | bytes 163872 | tf_op jit(solution)/shard_map/ppermute | solution.py:47
  74.2 1.4 collective-permute-start.15
  75.6 17.0 %attn.5.refs_3_ = f32[4,88,1024]{2,1,0:T(8,128)S(1)} custom-call(s32[5]{0:T(128)S(1)} %stack.56.s_ref, bf16[4,96,1024]{2,1,0:T(8,128)(2,1)S(1)} %get-tuple-element.37.refs_0_, bf16[160,512]{1,0:T(8,128)(2,1)S(1)} %collective-permute-done.19.refs_1_, bf16[480,512]{1,0:T(8,128)(2,1)S(1)} %collective-permute-done.20.refs_2_, ...), custom_call_target="tpu_custom_call" | custom-call | flops 1500000000 | bytes 1048576 | tf_op jit(solution)/shard_map/attn/pallas_call | solution.py:355
  92.6 17.2 %attn.6.refs_3_ = f32[4,88,1024]{2,1,0:T(8,128)S(1)} custom-call(s32[5]{0:T(128)S(1)} %stack.54.s_ref, bf16[4,96,1024]{2,1,0:T(8,128)(2,1)S(1)} %get-tuple-element.37.refs_0_, bf16[160,512]{1,0:T(8,128)(2,1)S(1)} %collective-permute-done.17.refs_1_, bf16[480,512]{1,0:T(8,128)(2,1)S(1)} %collective-permute-done.18.refs_2_, f32[4,88,1024]{2,1,0:T(8,128)S(1)} %attn.5.refs_3_), custom_call_target="tpu_custom_call" | custom-call | flops 1500000000 | bytes 1048576 | tf_op jit(solution)/shard_map/attn/pallas_call | solution.py:355
  109.8 17.0 %attn.7 = (f32[4,88,512]{2,1,0:T(8,128)S(1)}, f32[4,88,512]{2,1,0:T(8,128)S(1)}) custom-call(s32[5]{0:T(128)S(1)} %stack.52.s_ref, bf16[4,96,1024]{2,1,0:T(8,128)(2,1)S(1)} %get-tuple-element.37.refs_0_, bf16[160,512]{1,0:T(8,128)(2,1)S(1)} %collective-permute-done.15.refs_1_, bf16[480,512]{1,0:T(8,128)(2,1)S(1)} %collective-permute-done.16.refs_2_, ...), custom_call_target="tpu_custom_call" | custom-call | flops 1500000000 | bytes 1048576 | tf_op jit(solution)/shard_map/attn/pallas_call | solution.py:355
  127.0 2.2 %collective-permute-done.21.theirs = f32[4,88,512]{2,1,0:T(8,128)S(1)} collective-permute-done((f32[4,88,512]{2,1,0:T(8,128)S(1)}, f32[4,88,512]{2,1,0:T(8,128)S(1)}, u32[]{:S(2)}, u32[]{:S(2)}) %collective-permute-start.21) | collective-permute-done | bytes 720928 | tf_op jit(solution)/shard_map/ppermute | solution.py:47
  129.3 3.3 %collective-permute-start.22 = (bf16[64,512]{1,0:T(8,128)(2,1)S(1)}, bf16[64,512]{1,0:T(8,128)(2,1)S(1)}, u32[]{:S(2)}, u32[]{:S(2)}) collective-permute-start(bf16[64,512]{1,0:T(8,128)(2,1)S(1)} %get-tuple-element.42), channel_id=1, source_target_pairs={{32,0},{33,1},{34,2},{35,3},{36,4},{37,5},{38,6},{39,7},{40,8},{41... | collective-permute-start | bytes 196616 | tf_op jit(solution)/shard_map/ppermute | solution.py:47
  132.6 0.9 collective-permute-start.23
  133.5 0.9 collective-permute-start.24
  134.4 0.7 collective-permute-done.22.r1
  135.1 3.5 %collective-permute-done.23.r2 = bf16[64,512]{1,0:T(8,128)(2,1)S(1)} collective-permute-done((bf16[64,512]{1,0:T(8,128)(2,1)S(1)}, bf16[64,512]{1,0:T(8,128)(2,1)S(1)}, u32[]{:S(2)}, u32[]{:S(2)}) %collective-permute-start.23) | collective-permute-done | bytes 65568 | tf_op jit(solution)/shard_map/ppermute | solution.py:47
  138.6 0.7 collective-permute-done.24.r3
  139.4 1.2 collective-permute-start.25
  140.6 1.8 %collective-permute-start.26 = (bf16[256,128]{1,0:T(8,128)(2,1)S(1)}, bf16[256,128]{1,0:T(8,128)(2,1)S(1)}, u32[]{:S(2)}, u32[]{:S(2)}) collective-permute-start(bf16[256,128]{1,0:T(8,128)(2,1)S(1)} %get-tuple-element.47), channel_id=1, source_target_pairs={{4,0},{5,1},{6,2},{7,3},{0,4},{1,5},{2,6},{3,7},{12,8},{13,9},{14,... | collective-permute-start | bytes 196616 | tf_op jit(solution)/shard_map/ppermute | solution.py:47
  142.4 0.9 collective-permute-start.27
  143.3 0.7 collective-permute-done.25.t1
  144.0 2.4 %collective-permute-done.26.t2 = bf16[256,128]{1,0:T(8,128)(2,1)S(1)} collective-permute-done((bf16[256,128]{1,0:T(8,128)(2,1)S(1)}, bf16[256,128]{1,0:T(8,128)(2,1)S(1)}, u32[]{:S(2)}, u32[]{:S(2)}) %collective-permute-start.26) | collective-permute-done | bytes 65568 | tf_op jit(solution)/shard_map/ppermute | solution.py:47
  146.4 1.5 %collective-permute-done.27.t3 = bf16[256,128]{1,0:T(8,128)(2,1)S(1)} collective-permute-done((bf16[256,128]{1,0:T(8,128)(2,1)S(1)}, bf16[256,128]{1,0:T(8,128)(2,1)S(1)}, u32[]{:S(2)}, u32[]{:S(2)}) %collective-permute-start.27) | collective-permute-done | bytes 65568 | tf_op jit(solution)/shard_map/ppermute | solution.py:47
  147.9 3.2 %out_proj.1 = bf16[128,4096]{1,0:T(8,128)(2,1)} custom-call(s32[5]{0:T(128)S(1)} %stack.50.s.s_ref, bf16[256,128]{1,0:T(8,128)(2,1)S(1)} %get-tuple-element.45.t0, bf16[256,128]{1,0:T(8,128)(2,1)S(1)} %collective-permute-done.25.t1, bf16[256,128]{1,0:T(8,128)(2,1)S(1)} %collective-permute-done.26.t2, bf16[256,128]{1,0:T(8,128)(2,1)S(1)} %collective-permute-done.27.t3, ...), custom_call_target="tpu_custom_call" | custom-call | tf_op jit(solution)/shard_map/out_proj/pallas_call | solution.py:398
  (45 shorter events, 0.9 us)
Async XLA Ops:
  0.7 13.7 %copy-start = (bf16[768,192]{0,1:T(8,128)(2,1)S(1)}, bf16[768,192]{0,1:T(8,128)(2,1)}, u32[]{:S(2)}) copy-start(bf16[768,192]{0,1:T(8,128)(2,1)} %param.18) | copy-start | bytes 884740
  0.7 23.1 %copy-start.1 = (bf16[512,256]{1,0:T(8,128)(2,1)S(1)}, bf16[512,256]{1,0:T(8,128)(2,1)}, u32[]{:S(2)}) copy-start(bf16[512,256]{1,0:T(8,128)(2,1)} %own.1) | copy-start | bytes 786436
  8.5 8.2 %collective-permute-start = (bf16[768,128]{1,0:T(8,128)(2,1)}, bf16[768,128]{1,0:T(8,128)(2,1)S(1)}, u32[]{:S(2)}, u32[]{:S(2)}) collective-permute-start(bf16[768,128]{1,0:T(8,128)(2,1)} %get-tuple-element.27.p0), channel_id=1, source_target_pairs={{0,2},{1,3},{2,4},{3,5},{4,6},{5,7},{6,0},{7,1},{8,10},{9,11},{10,... | collective-permute-start | bytes 589832 | tf_op jit(solution)/shard_map/ppermute | solution.py:47
  10.1 13.1 %collective-permute-start.1 = (bf16[768,128]{1,0:T(8,128)(2,1)}, bf16[768,128]{1,0:T(8,128)(2,1)S(1)}, u32[]{:S(2)}, u32[]{:S(2)}) collective-permute-start(bf16[768,128]{1,0:T(8,128)(2,1)} %get-tuple-element.27.p0), channel_id=1, source_target_pairs={{0,4},{1,5},{2,6},{3,7},{4,0},{5,1},{6,2},{7,3},{8,12},{9,13},{10,... | collective-permute-start | bytes 589832 | tf_op jit(solution)/shard_map/ppermute | solution.py:47
  13.0 10.9 %collective-permute-start.2 = (bf16[768,128]{1,0:T(8,128)(2,1)}, bf16[768,128]{1,0:T(8,128)(2,1)S(1)}, u32[]{:S(2)}, u32[]{:S(2)}) collective-permute-start(bf16[768,128]{1,0:T(8,128)(2,1)} %get-tuple-element.27.p0), channel_id=1, source_target_pairs={{0,6},{1,7},{2,0},{3,1},{4,2},{5,3},{6,4},{7,5},{8,14},{9,15},{10,... | collective-permute-start | bytes 589832 | tf_op jit(solution)/shard_map/ppermute | solution.py:47
  14.4 13.8 %collective-permute-start.10 = (bf16[544,128]{1,0:T(8,128)(2,1)}, bf16[544,128]{1,0:T(8,128)(2,1)S(1)}, u32[]{:S(2)}, u32[]{:S(2)}) collective-permute-start(bf16[544,128]{1,0:T(8,128)(2,1)} %get-tuple-element.32.p0), channel_id=1, source_target_pairs={{0,6},{1,7},{2,0},{3,1},{4,2},{5,3},{6,4},{7,5},{8,14},{9,15},{10,... | collective-permute-start | bytes 417800 | tf_op jit(solution)/shard_map/ppermute | solution.py:47
  14.4 9.8 %collective-permute-start.3 = (bf16[192,768]{1,0:T(8,128)(2,1)S(1)}, bf16[192,768]{1,0:T(8,128)(2,1)S(1)}, u32[]{:S(2)}, u32[]{:S(2)}) collective-permute-start(bf16[192,768]{1,0:T(8,128)(2,1)S(1)} %bitcast.17), channel_id=1, source_target_pairs={{0,1},{1,0},{2,3},{3,2},{4,5},{5,4},{6,7},{7,6},{8,9},{9,8},{10,11... | collective-permute-start | bytes 884744 | tf_op jit(solution)/shard_map/ppermute | solution.py:47
  16.7 11.5 %collective-permute-start.8 = (bf16[544,128]{1,0:T(8,128)(2,1)}, bf16[544,128]{1,0:T(8,128)(2,1)S(1)}, u32[]{:S(2)}, u32[]{:S(2)}) collective-permute-start(bf16[544,128]{1,0:T(8,128)(2,1)} %get-tuple-element.32.p0), channel_id=1, source_target_pairs={{0,2},{1,3},{2,4},{3,5},{4,6},{5,7},{6,0},{7,1},{8,10},{9,11},{10,... | collective-permute-start | bytes 417800 | tf_op jit(solution)/shard_map/ppermute | solution.py:47
  23.2 6.8 %collective-permute-start.9 = (bf16[544,128]{1,0:T(8,128)(2,1)}, bf16[544,128]{1,0:T(8,128)(2,1)S(1)}, u32[]{:S(2)}, u32[]{:S(2)}) collective-permute-start(bf16[544,128]{1,0:T(8,128)(2,1)} %get-tuple-element.32.p0), channel_id=1, source_target_pairs={{0,4},{1,5},{2,6},{3,7},{4,0},{5,1},{6,2},{7,3},{8,12},{9,13},{10,... | collective-permute-start | bytes 417800 | tf_op jit(solution)/shard_map/ppermute | solution.py:47
  23.9 6.1 %collective-permute-start.11 = (bf16[512,256]{1,0:T(8,128)(2,1)S(1)}, bf16[512,256]{1,0:T(8,128)(2,1)S(1)}, u32[]{:S(2)}, u32[]{:S(2)}) collective-permute-start(bf16[512,256]{1,0:T(8,128)(2,1)S(1)} %copy-done.1), channel_id=1, source_target_pairs={{0,1},{1,0},{2,3},{3,2},{4,5},{5,4},{6,7},{7,6},{8,9},{9,8},{10,11... | collective-permute-start | bytes 786440 | tf_op jit(solution)/shard_map/ppermute | solution.py:47
  24.2 0.9 copy-start.2
  26.2 12.8 %collective-permute-start.4 = (bf16[96,512]{1,0:T(8,128)(2,1)S(1)}, bf16[96,512]{1,0:T(8,128)(2,1)S(1)}, u32[]{:S(2)}, u32[]{:S(2)}) collective-permute-start(bf16[96,512]{1,0:T(8,128)(2,1)S(1)} %get-tuple-element.29), channel_id=1, source_target_pairs={{0,32},{1,33},{2,34},{3,35},{4,36},{5,37},{6,38},{7,39},{8,40},{9,... | collective-permute-start | bytes 294920 | tf_op jit(solution)/shard_map/ppermute | solution.py:47
  30.0 0.9 copy-start.3
  31.9 14.4 %collective-permute-start.12 = (bf16[160,512]{1,0:T(8,128)(2,1)S(1)}, bf16[160,512]{1,0:T(8,128)(2,1)S(1)}, u32[]{:S(2)}, u32[]{:S(2)}) collective-permute-start(bf16[160,512]{1,0:T(8,128)(2,1)S(1)} %get-tuple-element.34), channel_id=1, source_target_pairs={{0,32},{1,33},{2,34},{3,35},{4,36},{5,37},{6,38},{7,39},{8,40},{9,... | collective-permute-start | bytes 491528 | tf_op jit(solution)/shard_map/ppermute | solution.py:47
  33.9 12.4 %collective-permute-start.13 = (bf16[160,512]{1,0:T(8,128)(2,1)S(1)}, bf16[160,512]{1,0:T(8,128)(2,1)S(1)}, u32[]{:S(2)}, u32[]{:S(2)}) collective-permute-start(bf16[160,512]{1,0:T(8,128)(2,1)S(1)} %get-tuple-element.35), channel_id=1, source_target_pairs={{0,64},{1,65},{2,66},{3,67},{4,68},{5,69},{6,70},{7,71},{8,72},{9,... | collective-permute-start | bytes 491528 | tf_op jit(solution)/shard_map/ppermute | solution.py:47
  37.5 8.8 %collective-permute-start.14 = (bf16[160,512]{1,0:T(8,128)(2,1)S(1)}, bf16[160,512]{1,0:T(8,128)(2,1)S(1)}, u32[]{:S(2)}, u32[]{:S(2)}) collective-permute-start(bf16[160,512]{1,0:T(8,128)(2,1)S(1)} %get-tuple-element.36), channel_id=1, source_target_pairs={{0,96},{1,97},{2,98},{3,99},{4,100},{5,101},{6,102},{7,103},{8,104... | collective-permute-start | bytes 491528 | tf_op jit(solution)/shard_map/ppermute | solution.py:47
  38.5 6.1 %collective-permute-start.5 = (bf16[96,512]{1,0:T(8,128)(2,1)S(1)}, bf16[96,512]{1,0:T(8,128)(2,1)S(1)}, u32[]{:S(2)}, u32[]{:S(2)}) collective-permute-start(bf16[96,512]{1,0:T(8,128)(2,1)S(1)} %get-tuple-element.30), channel_id=1, source_target_pairs={{0,64},{1,65},{2,66},{3,67},{4,68},{5,69},{6,70},{7,71},{8,72},{9,... | collective-permute-start | bytes 294920 | tf_op jit(solution)/shard_map/ppermute | solution.py:47
  39.1 7.1 %collective-permute-start.6 = (bf16[96,512]{1,0:T(8,128)(2,1)S(1)}, bf16[96,512]{1,0:T(8,128)(2,1)S(1)}, u32[]{:S(2)}, u32[]{:S(2)}) collective-permute-start(bf16[96,512]{1,0:T(8,128)(2,1)S(1)} %get-tuple-element.31), channel_id=1, source_target_pairs={{0,96},{1,97},{2,98},{3,99},{4,100},{5,101},{6,102},{7,103},{8,104... | collective-permute-start | bytes 294920 | tf_op jit(solution)/shard_map/ppermute | solution.py:47
  46.2 6.0 %collective-permute-start.7 = (bf16[384,512]{1,0:T(8,128)(2,1)S(1)}, bf16[384,512]{1,0:T(8,128)(2,1)S(1)}, u32[]{:S(2)}, u32[]{:S(2)}) collective-permute-start(bf16[384,512]{1,0:T(8,128)(2,1)S(1)} %join.2.refs_0_), channel_id=1, source_target_pairs={{0,1},{1,0},{2,3},{3,2},{4,5},{5,4},{6,7},{7,6},{8,9},{9,8},{10,11... | collective-permute-start | bytes 1179656 | tf_op jit(solution)/shard_map/ppermute | solution.py:47
  46.4 29.2 %collective-permute-start.20 = (bf16[480,512]{1,0:T(8,128)(2,1)S(1)}, bf16[480,512]{1,0:T(8,128)(2,1)S(1)}, u32[]{:S(2)}, u32[]{:S(2)}) collective-permute-start(bf16[480,512]{1,0:T(8,128)(2,1)S(1)} %join.3.refs_3_), channel_id=1, source_target_pairs={{0,8},{1,9},{2,10},{3,11},{4,12},{5,13},{6,14},{7,15},{8,16},{9,17... | collective-permute-start | bytes 1474568 | tf_op jit(solution)/shard_map/ppermute | solution.py:47
  46.9 45.6 %collective-permute-start.18 = (bf16[480,512]{1,0:T(8,128)(2,1)S(1)}, bf16[480,512]{1,0:T(8,128)(2,1)S(1)}, u32[]{:S(2)}, u32[]{:S(2)}) collective-permute-start(bf16[480,512]{1,0:T(8,128)(2,1)S(1)} %join.3.refs_3_), channel_id=1, source_target_pairs={{0,24},{1,25},{2,26},{3,27},{4,28},{5,29},{6,30},{7,31},{8,0},{9,1... | collective-permute-start | bytes 1474568 | tf_op jit(solution)/shard_map/ppermute | solution.py:47
  48.5 61.3 %collective-permute-start.16 = (bf16[480,512]{1,0:T(8,128)(2,1)S(1)}, bf16[480,512]{1,0:T(8,128)(2,1)S(1)}, u32[]{:S(2)}, u32[]{:S(2)}) collective-permute-start(bf16[480,512]{1,0:T(8,128)(2,1)S(1)} %join.3.refs_3_), channel_id=1, source_target_pairs={{0,16},{1,17},{2,18},{3,19},{4,20},{5,21},{6,22},{7,23},{8,24},{9,... | collective-permute-start | bytes 1474568 | tf_op jit(solution)/shard_map/ppermute | solution.py:47
  49.9 24.3 %collective-permute-start.19 = (bf16[160,512]{1,0:T(8,128)(2,1)S(1)}, bf16[160,512]{1,0:T(8,128)(2,1)S(1)}, u32[]{:S(2)}, u32[]{:S(2)}) collective-permute-start(bf16[160,512]{1,0:T(8,128)(2,1)S(1)} %get-tuple-element.33.refs_2_), channel_id=1, source_target_pairs={{0,8},{1,9},{2,10},{3,11},{4,12},{5,13},{6,14},{7,15},{8,16},{9,17... | collective-permute-start | bytes 491528 | tf_op jit(solution)/shard_map/ppermute | solution.py:47
  52.3 40.3 %collective-permute-start.17 = (bf16[160,512]{1,0:T(8,128)(2,1)S(1)}, bf16[160,512]{1,0:T(8,128)(2,1)S(1)}, u32[]{:S(2)}, u32[]{:S(2)}) collective-permute-start(bf16[160,512]{1,0:T(8,128)(2,1)S(1)} %get-tuple-element.33.refs_2_), channel_id=1, source_target_pairs={{0,24},{1,25},{2,26},{3,27},{4,28},{5,29},{6,30},{7,31},{8,0},{9,1... | collective-permute-start | bytes 491528 | tf_op jit(solution)/shard_map/ppermute | solution.py:47
  74.2 35.7 %collective-permute-start.15 = (bf16[160,512]{1,0:T(8,128)(2,1)S(1)}, bf16[160,512]{1,0:T(8,128)(2,1)S(1)}, u32[]{:S(2)}, u32[]{:S(2)}) collective-permute-start(bf16[160,512]{1,0:T(8,128)(2,1)S(1)} %get-tuple-element.33.refs_2_), channel_id=1, source_target_pairs={{0,16},{1,17},{2,18},{3,19},{4,20},{5,21},{6,22},{7,23},{8,24},{9,... | collective-permute-start | bytes 491528 | tf_op jit(solution)/shard_map/ppermute | solution.py:47
  75.6 72.3 %slice-start = ((s8[8388608]{0:T(1024)(128)(4,1)}), s8[4194304]{0:T(1024)(128)(4,1)S(1)}, s32[]{:S(2)}) async-start(s8[8388608]{0:T(1024)(128)(4,1)} %bitcast.15), calls=%async_computation | async-start | bytes 8388608
  92.5 55.4 %slice-start.1 = ((s8[8388608]{0:T(1024)(128)(4,1)}), s8[4194304]{0:T(1024)(128)(4,1)S(1)}, s32[]{:S(2)}) async-start(s8[8388608]{0:T(1024)(128)(4,1)} %bitcast.15), calls=%async_computation.1 | async-start | bytes 8388608
  109.8 38.1 %copy-start.4 = (f32[4096]{0:T(1024)S(1)}, f32[4096]{0:T(1024)}, u32[]{:S(2)}) copy-start(f32[4096]{0:T(1024)} %param.21) | copy-start | bytes 49156
  126.9 2.3 %collective-permute-start.21 = (f32[4,88,512]{2,1,0:T(8,128)S(1)}, f32[4,88,512]{2,1,0:T(8,128)S(1)}, u32[]{:S(2)}, u32[]{:S(2)}) collective-permute-start(f32[4,88,512]{2,1,0:T(8,128)S(1)} %get-tuple-element.40), channel_id=1, source_target_pairs={{0,1},{1,0},{2,3},{3,2},{4,5},{5,4},{6,7},{7,6},{8,9},{9,8},{10,11... | collective-permute-start | bytes 2162696 | tf_op jit(solution)/shard_map/ppermute | solution.py:47
  129.3 5.8 %collective-permute-start.22 = (bf16[64,512]{1,0:T(8,128)(2,1)S(1)}, bf16[64,512]{1,0:T(8,128)(2,1)S(1)}, u32[]{:S(2)}, u32[]{:S(2)}) collective-permute-start(bf16[64,512]{1,0:T(8,128)(2,1)S(1)} %get-tuple-element.42), channel_id=1, source_target_pairs={{32,0},{33,1},{34,2},{35,3},{36,4},{37,5},{38,6},{39,7},{40,8},{41... | collective-permute-start | bytes 196616 | tf_op jit(solution)/shard_map/ppermute | solution.py:47
  132.6 6.1 %collective-permute-start.23 = (bf16[64,512]{1,0:T(8,128)(2,1)S(1)}, bf16[64,512]{1,0:T(8,128)(2,1)S(1)}, u32[]{:S(2)}, u32[]{:S(2)}) collective-permute-start(bf16[64,512]{1,0:T(8,128)(2,1)S(1)} %get-tuple-element.43), channel_id=1, source_target_pairs={{64,0},{65,1},{66,2},{67,3},{68,4},{69,5},{70,6},{71,7},{72,8},{73... | collective-permute-start | bytes 196616 | tf_op jit(solution)/shard_map/ppermute | solution.py:47
  133.5 5.8 %collective-permute-start.24 = (bf16[64,512]{1,0:T(8,128)(2,1)S(1)}, bf16[64,512]{1,0:T(8,128)(2,1)S(1)}, u32[]{:S(2)}, u32[]{:S(2)}) collective-permute-start(bf16[64,512]{1,0:T(8,128)(2,1)S(1)} %get-tuple-element.44), channel_id=1, source_target_pairs={{96,0},{97,1},{98,2},{99,3},{100,4},{101,5},{102,6},{103,7},{104,8... | collective-permute-start | bytes 196616 | tf_op jit(solution)/shard_map/ppermute | solution.py:47
  139.4 4.6 %collective-permute-start.25 = (bf16[256,128]{1,0:T(8,128)(2,1)S(1)}, bf16[256,128]{1,0:T(8,128)(2,1)S(1)}, u32[]{:S(2)}, u32[]{:S(2)}) collective-permute-start(bf16[256,128]{1,0:T(8,128)(2,1)S(1)} %get-tuple-element.46), channel_id=1, source_target_pairs={{2,0},{3,1},{4,2},{5,3},{6,4},{7,5},{0,6},{1,7},{10,8},{11,9},{12,... | collective-permute-start | bytes 196616 | tf_op jit(solution)/shard_map/ppermute | solution.py:47
  140.6 5.8 %collective-permute-start.26 = (bf16[256,128]{1,0:T(8,128)(2,1)S(1)}, bf16[256,128]{1,0:T(8,128)(2,1)S(1)}, u32[]{:S(2)}, u32[]{:S(2)}) collective-permute-start(bf16[256,128]{1,0:T(8,128)(2,1)S(1)} %get-tuple-element.47), channel_id=1, source_target_pairs={{4,0},{5,1},{6,2},{7,3},{0,4},{1,5},{2,6},{3,7},{12,8},{13,9},{14,... | collective-permute-start | bytes 196616 | tf_op jit(solution)/shard_map/ppermute | solution.py:47
  142.4 5.5 %collective-permute-start.27 = (bf16[256,128]{1,0:T(8,128)(2,1)S(1)}, bf16[256,128]{1,0:T(8,128)(2,1)S(1)}, u32[]{:S(2)}, u32[]{:S(2)}) collective-permute-start(bf16[256,128]{1,0:T(8,128)(2,1)S(1)} %get-tuple-element.48), channel_id=1, source_target_pairs={{6,0},{7,1},{0,2},{1,3},{2,4},{3,5},{4,6},{5,7},{14,8},{15,9},{8,1... | collective-permute-start | bytes 196616 | tf_op jit(solution)/shard_map/ppermute | solution.py:47

commit v3 on v2

--- a/solution.py
+++ b/solution.py
@@ -54,29 +54,45 @@
 CHUNKS = 4
 
 
-def down_kernel(
-    tok, gain, kvd, rd, kvg, qd, qg, cos, sin, out, q_out,
-    tok_v, gain_v, kvd_v, rd_v, kvg_v, qd_v, qg_v, normed, sems,
-):
-    step = kvd.shape[0] // CHUNKS
+def fetcher(sems):
     copies = {}
 
     def fetch(name, src, dst):
         copies[name] = pltpu.make_async_copy(src, dst, sems.at[len(copies)])
         copies[name].start()
 
+    return copies, fetch
+
+
+def product(copies, normed, weights):
+    step = weights.shape[1]
+    total = None
+    for n in range(CHUNKS):
+        copies[n].wait()
+        part = jnp.dot(
+            normed[:, n * step : n * step + step], weights[n], preferred_element_type=F32
+        )
+        total = part if total is None else total + part
+    return total
+
+
+def kv_down_kernel(
+    tok, gain, kvd, rd, kvg, cos, sin, normed, out, tok_v, gain_v, kvd_v, rd_v, kvg_v, sems
+):
+    step = kvd.shape[0] // CHUNKS
+    copies, fetch = fetcher(sems)
     fetch("tok", tok, tok_v)
     fetch("gain", gain, gain_v)
+    for n in range(CHUNKS):
+        fetch(n, kvd.at[pl.ds(n * step, step)], kvd_v.at[n])
     fetch("rd", rd, rd_v)
-    for n in range(CHUNKS):
-        fetch(("kv", n), kvd.at[pl.ds(n * step, step)], kvd_v.at[n])
     fetch("kvg", kvg, kvg_v)
-    for n in range(CHUNKS):
-        fetch(("q", n), qd.at[pl.ds(n * step, step)], qd_v.at[n])
-    fetch("qg", qg, qg_v)
     copies["tok"].wait()
     copies["gain"].wait()
     normed[...] = normed_rows(tok_v[...].astype(F32), gain_v[...]).astype(BF)
+    total = product(copies, normed, kvd_v)
+    copies["kvg"].wait()
+    out[0:512, :] = normed_rows(total, kvg_v[...]).T.astype(BF)
     copies["rd"].wait()
     r = lax.dot_general(
         rd_v[...], normed[...], (((1,), (1,)), ((), ())), preferred_element_type=F32
@@ -85,46 +101,55 @@
     out[512:528, :] = (left * cos[...] - right * sin[...]).astype(BF)
     out[528:544, :] = (right * cos[...] + left * sin[...]).astype(BF)
 
-    def product(name, weights):
-        total = None
-        for n in range(CHUNKS):
-            copies[(name, n)].wait()
-            part = jnp.dot(
-                normed[:, n * step : n * step + step], weights[n], preferred_element_type=F32
-            )
-            total = part if total is None else total + part
-        return total
-
-    total = product("kv", kvd_v)
-    copies["kvg"].wait()
-    out[0:512, :] = normed_rows(total, kvg_v[...]).T.astype(BF)
-    total = product("q", qd_v)
-    copies["qg"].wait()
-    gain_q = jnp.concatenate([qg_v[n : n + 1, :] for n in range(6)], axis=1)
-    q_out[...] = normed_rows(total, gain_q).T.astype(BF)
-
-
-def down_call(tok, gain, kvd, rd, kvg, qd, qg, cos, sin):
+
+def kv_down_call(tok, gain, kvd, rd, kvg, cos, sin):
     rows, d = tok.shape
-    step = d // CHUNKS
-    return pl.pallas_call(
-        down_kernel,
-        out_shape=[jax.ShapeDtypeStruct((544, rows), BF), jax.ShapeDtypeStruct((768, rows), BF)],
-        in_specs=[pl.BlockSpec(memory_space=pl.ANY)] * 7 + [VM] * 2,
+    return pl.pallas_call(
+        kv_down_kernel,
+        out_shape=[jax.ShapeDtypeStruct((rows, d), BF), jax.ShapeDtypeStruct((544, rows), BF)],
+        in_specs=[pl.BlockSpec(memory_space=pl.ANY)] * 5 + [VM] * 2,
         out_specs=[VM] * 2,
         scratch_shapes=[
             pltpu.VMEM((rows, d), BF),
             pltpu.VMEM((1, d), F32),
-            pltpu.VMEM((CHUNKS, step, 512), BF),
+            pltpu.VMEM((CHUNKS, d // CHUNKS, 512), BF),
             pltpu.VMEM((32, d), BF),
             pltpu.VMEM((1, 512), F32),
-            pltpu.VMEM((CHUNKS, step, 768), BF),
+            pltpu.SemaphoreType.DMA((4 + CHUNKS,)),
+        ],
+        name="kv_down",
+    )(tok, gain, kvd, rd, kvg, cos, sin)
+
+
+def q_down_kernel(src, qd, qg, out, normed, qd_v, qg_v, sems):
+    step = qd.shape[0] // CHUNKS
+    copies, fetch = fetcher(sems)
+    fetch("in", src, normed)
+    for n in range(CHUNKS):
+        fetch(n, qd.at[pl.ds(n * step, step)], qd_v.at[n])
+    fetch("gain", qg, qg_v)
+    copies["in"].wait()
+    total = product(copies, normed, qd_v)
+    copies["gain"].wait()
+    gain = jnp.concatenate([qg_v[n : n + 1, :] for n in range(6)], axis=1)
+    out[...] = normed_rows(total, gain).T.astype(BF)
+
+
+def q_down_call(normed, qd, qg):
+    rows, d = normed.shape
+    return pl.pallas_call(
+        q_down_kernel,
+        out_shape=jax.ShapeDtypeStruct((768, rows), BF),
+        in_specs=[pl.BlockSpec(memory_space=pl.ANY)] * 3,
+        out_specs=VM,
+        scratch_shapes=[
+            pltpu.VMEM((rows, d), BF),
+            pltpu.VMEM((CHUNKS, d // CHUNKS, 768), BF),
             pltpu.VMEM((6, 128), F32),
-            pltpu.VMEM((rows, d), BF),
-            pltpu.SemaphoreType.DMA((5 + 2 * CHUNKS,)),
+            pltpu.SemaphoreType.DMA((2 + CHUNKS,)),
         ],
-        name="down",
-    )(tok, gain, kvd, rd, kvg, qd, qg, cos, sin)
+        name="q_down",
+    )(normed, qd, qg)
 
 
 def kv_up_kernel(s, p0, p1, p2, p3, own, other, o0, o1, o2, o3, w, kv):
@@ -430,11 +455,11 @@
 
     q_up = q_up.T
     kv_up_other, q_up_other = sends([kv_up, q_up], [CORE] * 2)
-    lat, q_lat = down_call(
-        tokens, norm_gain[None], kv_down, rope_down.T, kv_gain[None], q_down,
-        q_gain.reshape(6, 128), cos_own, sin_own,
+    normed, lat = kv_down_call(
+        tokens, norm_gain[None], kv_down, rope_down.T, kv_gain[None], cos_own, sin_own
     )
     lats = [lat] + sends([lat] * 3, ALONG_Y[1:])
+    q_lat = q_down_call(normed, q_down, q_gain.reshape(6, 128))
     q_lats = [q_lat] + sends([q_lat] * 3, ALONG_Y[1:])
     near, *moved = kv_up_call(here, lats, kv_up, kv_up_other)
     moved = sends(moved, ALONG_Z[1:])

time: 151 us -> 153 us (1.013)
  Pallas kernels: 83.6 us -> 85.9 us
    pallas_call x1 -> x2, Pallas kernels: 7.73 us -> 9.85 us  [the longest x1 5.26 us: kv_down_call(): pl.pallas_call(kv_down_kernel, out_shape=[jax.ShapeDtypeStruct((rows, d),...]
  transfers between devices with their start and end apart: 28 -> 28, of which waited for: 13 -> 13; matrix products, arithmetic and copies ran while one was open for 0% -> 0% of each run, Pallas kernels for 37% -> 36%
where the time goes in v3:
time: 153 us
  Pallas kernels  85.9 us (56%)
  starting transfers between devices  36.6 us (24%)
  waiting for transfers between devices  27.5 us (18%)
    pallas_call x4, Pallas kernels, attention(): pl.pallas_call(functools.partial(attn_kernel, first, last), out_shape=out...  70.5 us
    ppermute x28, starting transfers between devices, send(): return lax.ppermute(a, AXES, perm)  36.6 us
    ppermute x28, waiting for transfers between devices, send(): return lax.ppermute(a, AXES, perm)  27.5 us
    pallas_call x1, Pallas kernels, kv_down_call(): pl.pallas_call(kv_down_kernel, out_shape=[jax.ShapeDtypeStruct((rows, d),...  5.26 us
    pallas_call x1, Pallas kernels, q_down_call(): pl.pallas_call(q_down_kernel, out_shape=jax.ShapeDtypeStruct((768, rows),...  4.6 us
    pallas_call x1, Pallas kernels, out_call(): pl.pallas_call(out_kernel, out_shape=jax.ShapeDtypeStruct((128, w.shape[1...  3.18 us
  transfers between devices with their start and end apart: 28, of which 13 were waited for; matrix products, arithmetic and copies ran while one was open for 0% of the time, Pallas kernels for 36%

profile of v3, /device:TPU:6, one launch (start us, length us, event | category | flops | bytes accessed | tf_op | source)
XLA Modules:
  0.0 152.6 jit_solution(1668065415067345933)
XLA Ops:
  0.0 0.7 multiply_sine_fusion.1
  0.7 5.3 %kv_down.1 = (bf16[128,4096]{1,0:T(8,128)(2,1)}, bf16[544,128]{1,0:T(8,128)(2,1)}) custom-call(bf16[128,4096]{1,0:T(8,128)(2,1)} %tok.1, f32[1,4096]{1,0:T(1,128)} %bitcast.21, bf16[4096,512]{1,0:T(8,128)(2,1)} %kvd.1, bf16[32,4096]{1,0:T(8,128)(2,1)} %bitcast.20, f32[1,512]{1,0:T(1,128)} %bitcast.23, f32[16,128]{1,0:T(8,128)} %get-tuple-element.52.cos, ...), custom_call_target="tpu_custom_call" | custom-call | tf_op jit(solution)/shard_map/kv_down/pallas_call | solution.py:107
  6.0 4.6 %q_down.1.p0 = bf16[768,128]{1,0:T(8,128)(2,1)} custom-call(bf16[128,4096]{1,0:T(8,128)(2,1)} %get-tuple-element.27.src, bf16[4096,768]{1,0:T(8,128)(2,1)} %qd.1, f32[6,128]{1,0:T(8,128)} %bitcast.22), custom_call_target="tpu_custom_call" | custom-call | tf_op jit(solution)/shard_map/q_down/pallas_call | solution.py:140
  10.7 1.6 %collective-permute-start = (bf16[768,128]{1,0:T(8,128)(2,1)}, bf16[768,128]{1,0:T(8,128)(2,1)S(1)}, u32[]{:S(2)}, u32[]{:S(2)}) collective-permute-start(bf16[768,128]{1,0:T(8,128)(2,1)} %q_down.1.p0), channel_id=1, source_target_pairs={{0,2},{1,3},{2,4},{3,5},{4,6},{5,7},{6,0},{7,1},{8,10},{9,11},{10,... | collective-permute-start | bytes 589832 | tf_op jit(solution)/shard_map/ppermute | solution.py:47
  12.3 2.9 %collective-permute-start.1 = (bf16[768,128]{1,0:T(8,128)(2,1)}, bf16[768,128]{1,0:T(8,128)(2,1)S(1)}, u32[]{:S(2)}, u32[]{:S(2)}) collective-permute-start(bf16[768,128]{1,0:T(8,128)(2,1)} %q_down.1.p0), channel_id=1, source_target_pairs={{0,4},{1,5},{2,6},{3,7},{4,0},{5,1},{6,2},{7,3},{8,12},{9,13},{10,... | collective-permute-start | bytes 589832 | tf_op jit(solution)/shard_map/ppermute | solution.py:47
  15.2 1.3 collective-permute-start.2
  16.8 2.1 %collective-permute-done.p1 = bf16[768,128]{1,0:T(8,128)(2,1)S(1)} collective-permute-done((bf16[768,128]{1,0:T(8,128)(2,1)}, bf16[768,128]{1,0:T(8,128)(2,1)S(1)}, u32[]{:S(2)}, u32[]{:S(2)}) %collective-permute-start) | collective-permute-done | bytes 196640 | tf_op jit(solution)/shard_map/ppermute | solution.py:47
  18.9 1.4 collective-permute-start.8
  20.3 5.1 %collective-permute-done.1.p2 = bf16[768,128]{1,0:T(8,128)(2,1)S(1)} collective-permute-done((bf16[768,128]{1,0:T(8,128)(2,1)}, bf16[768,128]{1,0:T(8,128)(2,1)S(1)}, u32[]{:S(2)}, u32[]{:S(2)}) %collective-permute-start.1) | collective-permute-done | bytes 196640 | tf_op jit(solution)/shard_map/ppermute | solution.py:47
  25.4 0.7 collective-permute-start.9
  26.1 0.2 multiply_sine_fusion
  26.4 0.9 copy-done
  27.3 1.1 q_up.1
  28.4 2.0 %collective-permute-start.4 = (bf16[96,512]{1,0:T(8,128)(2,1)S(1)}, bf16[96,512]{1,0:T(8,128)(2,1)S(1)}, u32[]{:S(2)}, u32[]{:S(2)}) collective-permute-start(bf16[96,512]{1,0:T(8,128)(2,1)S(1)} %get-tuple-element.29), channel_id=1, source_target_pairs={{0,32},{1,33},{2,34},{3,35},{4,36},{5,37},{6,38},{7,39},{8,40},{9,... | collective-permute-start | bytes 294920 | tf_op jit(solution)/shard_map/ppermute | solution.py:47
  30.4 1.5 %collective-permute-done.9.p2 = bf16[544,128]{1,0:T(8,128)(2,1)S(1)} collective-permute-done((bf16[544,128]{1,0:T(8,128)(2,1)S(1)}, bf16[544,128]{1,0:T(8,128)(2,1)S(1)}, u32[]{:S(2)}, u32[]{:S(2)}) %collective-permute-start.9) | collective-permute-done | bytes 139296 | tf_op jit(solution)/shard_map/ppermute | solution.py:47
  31.9 1.0 kv_up.1
  33.0 2.0 %collective-permute-start.12 = (bf16[160,512]{1,0:T(8,128)(2,1)S(1)}, bf16[160,512]{1,0:T(8,128)(2,1)S(1)}, u32[]{:S(2)}, u32[]{:S(2)}) collective-permute-start(bf16[160,512]{1,0:T(8,128)(2,1)S(1)} %get-tuple-element.34), channel_id=1, source_target_pairs={{0,32},{1,33},{2,34},{3,35},{4,36},{5,37},{6,38},{7,39},{8,40},{9,... | collective-permute-start | bytes 491528 | tf_op jit(solution)/shard_map/ppermute | solution.py:47
  35.0 3.6 %collective-permute-start.13 = (bf16[160,512]{1,0:T(8,128)(2,1)S(1)}, bf16[160,512]{1,0:T(8,128)(2,1)S(1)}, u32[]{:S(2)}, u32[]{:S(2)}) collective-permute-start(bf16[160,512]{1,0:T(8,128)(2,1)S(1)} %get-tuple-element.35), channel_id=1, source_target_pairs={{0,64},{1,65},{2,66},{3,67},{4,68},{5,69},{6,70},{7,71},{8,72},{9,... | collective-permute-start | bytes 491528 | tf_op jit(solution)/shard_map/ppermute | solution.py:47
  38.6 1.0 collective-permute-start.14
  39.6 0.5 collective-permute-start.5
  40.1 3.1 %collective-permute-start.6 = (bf16[96,512]{1,0:T(8,128)(2,1)S(1)}, bf16[96,512]{1,0:T(8,128)(2,1)S(1)}, u32[]{:S(2)}, u32[]{:S(2)}) collective-permute-start(bf16[96,512]{1,0:T(8,128)(2,1)S(1)} %get-tuple-element.31), channel_id=1, source_target_pairs={{0,96},{1,97},{2,98},{3,99},{4,100},{5,101},{6,102},{7,103},{8,104... | collective-permute-start | bytes 294920 | tf_op jit(solution)/shard_map/ppermute | solution.py:47
  43.3 3.1 %collective-permute-done.5.refs_2_ = bf16[96,512]{1,0:T(8,128)(2,1)S(1)} collective-permute-done((bf16[96,512]{1,0:T(8,128)(2,1)S(1)}, bf16[96,512]{1,0:T(8,128)(2,1)S(1)}, u32[]{:S(2)}, u32[]{:S(2)}) %collective-permute-start.5) | collective-permute-done | bytes 98336 | tf_op jit(solution)/shard_map/ppermute | solution.py:47
  46.3 1.1 collective-permute-done.6.refs_3_
  47.7 0.6 collective-permute-start.20
  48.2 1.5 %collective-permute-start.18 = (bf16[480,512]{1,0:T(8,128)(2,1)S(1)}, bf16[480,512]{1,0:T(8,128)(2,1)S(1)}, u32[]{:S(2)}, u32[]{:S(2)}) collective-permute-start(bf16[480,512]{1,0:T(8,128)(2,1)S(1)} %join.3.refs_3_), channel_id=1, source_target_pairs={{0,24},{1,25},{2,26},{3,27},{4,28},{5,29},{6,30},{7,31},{8,0},{9,1... | collective-permute-start | bytes 1474568 | tf_op jit(solution)/shard_map/ppermute | solution.py:47
  49.8 1.4 collective-permute-start.16
  51.2 2.1 %collective-permute-start.19 = (bf16[160,512]{1,0:T(8,128)(2,1)S(1)}, bf16[160,512]{1,0:T(8,128)(2,1)S(1)}, u32[]{:S(2)}, u32[]{:S(2)}) collective-permute-start(bf16[160,512]{1,0:T(8,128)(2,1)S(1)} %get-tuple-element.33.refs_2_), channel_id=1, source_target_pairs={{0,8},{1,9},{2,10},{3,11},{4,12},{5,13},{6,14},{7,15},{8,16},{9,17... | collective-permute-start | bytes 491528 | tf_op jit(solution)/shard_map/ppermute | solution.py:47
  53.5 0.2 collective-permute-start.17
  53.7 19.1 %attn.4 = (f32[4,88,1024]{2,1,0:T(8,128)S(1)}, bf16[4,96,1024]{2,1,0:T(8,128)(2,1)S(1)}) custom-call(s32[5]{0:T(128)S(1)} %stack.50.s.s_ref, bf16[384,512]{1,0:T(8,128)(2,1)S(1)} %join.2.refs_0_, bf16[384,512]{1,0:T(8,128)(2,1)S(1)} %collective-permute-done.7.refs_1_, bf16[160,512]{1,0:T(8,128)(2,1)S(1)} %get-tuple-element.33.refs_2_, ...), custom_call_target="tpu_custom_call" | custom-call | flops 1500000000 | bytes 1048576 | tf_op jit(solution)/shard_map/attn/pallas_call | solution.py:380
  72.8 2.6 %collective-permute-done.19.refs_1_ = bf16[160,512]{1,0:T(8,128)(2,1)S(1)} collective-permute-done((bf16[160,512]{1,0:T(8,128)(2,1)S(1)}, bf16[160,512]{1,0:T(8,128)(2,1)S(1)}, u32[]{:S(2)}, u32[]{:S(2)}) %collective-permute-start.19) | collective-permute-done | bytes 163872 | tf_op jit(solution)/shard_map/ppermute | solution.py:47
  75.4 1.4 collective-permute-start.15
  76.9 17.1 %attn.5.refs_3_ = f32[4,88,1024]{2,1,0:T(8,128)S(1)} custom-call(s32[5]{0:T(128)S(1)} %stack.56.s_ref, bf16[4,96,1024]{2,1,0:T(8,128)(2,1)S(1)} %get-tuple-element.37.refs_0_, bf16[160,512]{1,0:T(8,128)(2,1)S(1)} %collective-permute-done.19.refs_1_, bf16[480,512]{1,0:T(8,128)(2,1)S(1)} %collective-permute-done.20.refs_2_, ...), custom_call_target="tpu_custom_call" | custom-call | flops 1500000000 | bytes 1048576 | tf_op jit(solution)/shard_map/attn/pallas_call | solution.py:380
  94.0 17.2 %attn.6.refs_3_ = f32[4,88,1024]{2,1,0:T(8,128)S(1)} custom-call(s32[5]{0:T(128)S(1)} %stack.54.s_ref, bf16[4,96,1024]{2,1,0:T(8,128)(2,1)S(1)} %get-tuple-element.37.refs_0_, bf16[160,512]{1,0:T(8,128)(2,1)S(1)} %collective-permute-done.17.refs_1_, bf16[480,512]{1,0:T(8,128)(2,1)S(1)} %collective-permute-done.18.refs_2_, f32[4,88,1024]{2,1,0:T(8,128)S(1)} %attn.5.refs_3_), custom_call_target="tpu_custom_call" | custom-call | flops 1500000000 | bytes 1048576 | tf_op jit(solution)/shard_map/attn/pallas_call | solution.py:380
  111.2 17.1 %attn.7 = (f32[4,88,512]{2,1,0:T(8,128)S(1)}, f32[4,88,512]{2,1,0:T(8,128)S(1)}) custom-call(s32[5]{0:T(128)S(1)} %stack.52.s_ref, bf16[4,96,1024]{2,1,0:T(8,128)(2,1)S(1)} %get-tuple-element.37.refs_0_, bf16[160,512]{1,0:T(8,128)(2,1)S(1)} %collective-permute-done.15.refs_1_, bf16[480,512]{1,0:T(8,128)(2,1)S(1)} %collective-permute-done.16.refs_2_, ...), custom_call_target="tpu_custom_call" | custom-call | flops 1500000000 | bytes 1048576 | tf_op jit(solution)/shard_map/attn/pallas_call | solution.py:380
  128.5 2.2 %collective-permute-done.21.theirs = f32[4,88,512]{2,1,0:T(8,128)S(1)} collective-permute-done((f32[4,88,512]{2,1,0:T(8,128)S(1)}, f32[4,88,512]{2,1,0:T(8,128)S(1)}, u32[]{:S(2)}, u32[]{:S(2)}) %collective-permute-start.21) | collective-permute-done | bytes 720928 | tf_op jit(solution)/shard_map/ppermute | solution.py:47
  130.8 3.4 %collective-permute-start.22 = (bf16[64,512]{1,0:T(8,128)(2,1)S(1)}, bf16[64,512]{1,0:T(8,128)(2,1)S(1)}, u32[]{:S(2)}, u32[]{:S(2)}) collective-permute-start(bf16[64,512]{1,0:T(8,128)(2,1)S(1)} %get-tuple-element.42), channel_id=1, source_target_pairs={{32,0},{33,1},{34,2},{35,3},{36,4},{37,5},{38,6},{39,7},{40,8},{41... | collective-permute-start | bytes 196616 | tf_op jit(solution)/shard_map/ppermute | solution.py:47
  134.2 0.5 collective-permute-start.23
  134.7 1.2 collective-permute-start.24
  135.9 1.5 collective-permute-done.22.r1
  137.4 2.8 %collective-permute-done.23.r2 = bf16[64,512]{1,0:T(8,128)(2,1)S(1)} collective-permute-done((bf16[64,512]{1,0:T(8,128)(2,1)S(1)}, bf16[64,512]{1,0:T(8,128)(2,1)S(1)}, u32[]{:S(2)}, u32[]{:S(2)}) %collective-permute-start.23) | collective-permute-done | bytes 65568 | tf_op jit(solution)/shard_map/ppermute | solution.py:47
  140.2 0.7 collective-permute-done.24.r3
  141.0 1.1 collective-permute-start.25
  142.1 1.8 %collective-permute-start.26 = (bf16[256,128]{1,0:T(8,128)(2,1)S(1)}, bf16[256,128]{1,0:T(8,128)(2,1)S(1)}, u32[]{:S(2)}, u32[]{:S(2)}) collective-permute-start(bf16[256,128]{1,0:T(8,128)(2,1)S(1)} %get-tuple-element.47), channel_id=1, source_target_pairs={{4,0},{5,1},{6,2},{7,3},{0,4},{1,5},{2,6},{3,7},{12,8},{13,9},{14,... | collective-permute-start | bytes 196616 | tf_op jit(solution)/shard_map/ppermute | solution.py:47
  144.0 0.8 collective-permute-start.27
  144.8 0.7 collective-permute-done.25.t1
  145.4 2.8 %collective-permute-done.26.t2 = bf16[256,128]{1,0:T(8,128)(2,1)S(1)} collective-permute-done((bf16[256,128]{1,0:T(8,128)(2,1)S(1)}, bf16[256,128]{1,0:T(8,128)(2,1)S(1)}, u32[]{:S(2)}, u32[]{:S(2)}) %collective-permute-start.26) | collective-permute-done | bytes 65568 | tf_op jit(solution)/shard_map/ppermute | solution.py:47
  148.2 1.2 collective-permute-done.27.t3
  149.4 3.2 %out_proj.1 = bf16[128,4096]{1,0:T(8,128)(2,1)} custom-call(s32[5]{0:T(128)S(1)} %stack.50.s.s_ref, bf16[256,128]{1,0:T(8,128)(2,1)S(1)} %get-tuple-element.45.t0, bf16[256,128]{1,0:T(8,128)(2,1)S(1)} %collective-permute-done.25.t1, bf16[256,128]{1,0:T(8,128)(2,1)S(1)} %collective-permute-done.26.t2, bf16[256,128]{1,0:T(8,128)(2,1)S(1)} %collective-permute-done.27.t3, ...), custom_call_target="tpu_custom_call" | custom-call | tf_op jit(solution)/shard_map/out_proj/pallas_call | solution.py:423
  (46 shorter events, 1.0 us)
Async XLA Ops:
  6.0 10.5 %copy-start.3 = (bf16[544,128]{1,0:T(8,128)(2,1)S(1)}, bf16[544,128]{1,0:T(8,128)(2,1)}, u32[]{:S(2)}) copy-start(bf16[544,128]{1,0:T(8,128)(2,1)} %get-tuple-element.32.p0) | copy-start | bytes 417796
  6.0 10.6 %copy-start.1 = (bf16[768,192]{0,1:T(8,128)(2,1)S(1)}, bf16[768,192]{0,1:T(8,128)(2,1)}, u32[]{:S(2)}) copy-start(bf16[768,192]{0,1:T(8,128)(2,1)} %param.18) | copy-start | bytes 884740
  6.0 20.0 %copy-start.2 = (bf16[512,256]{1,0:T(8,128)(2,1)S(1)}, bf16[512,256]{1,0:T(8,128)(2,1)}, u32[]{:S(2)}) copy-start(bf16[512,256]{1,0:T(8,128)(2,1)} %own.1) | copy-start | bytes 786436
  10.7 8.2 %collective-permute-start = (bf16[768,128]{1,0:T(8,128)(2,1)}, bf16[768,128]{1,0:T(8,128)(2,1)S(1)}, u32[]{:S(2)}, u32[]{:S(2)}) collective-permute-start(bf16[768,128]{1,0:T(8,128)(2,1)} %q_down.1.p0), channel_id=1, source_target_pairs={{0,2},{1,3},{2,4},{3,5},{4,6},{5,7},{6,0},{7,1},{8,10},{9,11},{10,... | collective-permute-start | bytes 589832 | tf_op jit(solution)/shard_map/ppermute | solution.py:47
  12.3 13.1 %collective-permute-start.1 = (bf16[768,128]{1,0:T(8,128)(2,1)}, bf16[768,128]{1,0:T(8,128)(2,1)S(1)}, u32[]{:S(2)}, u32[]{:S(2)}) collective-permute-start(bf16[768,128]{1,0:T(8,128)(2,1)} %q_down.1.p0), channel_id=1, source_target_pairs={{0,4},{1,5},{2,6},{3,7},{4,0},{5,1},{6,2},{7,3},{8,12},{9,13},{10,... | collective-permute-start | bytes 589832 | tf_op jit(solution)/shard_map/ppermute | solution.py:47
  15.2 10.8 %collective-permute-start.2 = (bf16[768,128]{1,0:T(8,128)(2,1)}, bf16[768,128]{1,0:T(8,128)(2,1)S(1)}, u32[]{:S(2)}, u32[]{:S(2)}) collective-permute-start(bf16[768,128]{1,0:T(8,128)(2,1)} %q_down.1.p0), channel_id=1, source_target_pairs={{0,6},{1,7},{2,0},{3,1},{4,2},{5,3},{6,4},{7,5},{8,14},{9,15},{10,... | collective-permute-start | bytes 589832 | tf_op jit(solution)/shard_map/ppermute | solution.py:47
  16.6 13.8 %collective-permute-start.10 = (bf16[544,128]{1,0:T(8,128)(2,1)S(1)}, bf16[544,128]{1,0:T(8,128)(2,1)S(1)}, u32[]{:S(2)}, u32[]{:S(2)}) collective-permute-start(bf16[544,128]{1,0:T(8,128)(2,1)S(1)} %copy-done.3), channel_id=1, source_target_pairs={{0,6},{1,7},{2,0},{3,1},{4,2},{5,3},{6,4},{7,5},{8,14},{9,15},{10,... | collective-permute-start | bytes 417800 | tf_op jit(solution)/shard_map/ppermute | solution.py:47
  16.6 9.8 %collective-permute-start.3 = (bf16[192,768]{1,0:T(8,128)(2,1)S(1)}, bf16[192,768]{1,0:T(8,128)(2,1)S(1)}, u32[]{:S(2)}, u32[]{:S(2)}) collective-permute-start(bf16[192,768]{1,0:T(8,128)(2,1)S(1)} %bitcast.17), channel_id=1, source_target_pairs={{0,1},{1,0},{2,3},{3,2},{4,5},{5,4},{6,7},{7,6},{8,9},{9,8},{10,11... | collective-permute-start | bytes 884744 | tf_op jit(solution)/shard_map/ppermute | solution.py:47
  18.9 11.5 %collective-permute-start.8 = (bf16[544,128]{1,0:T(8,128)(2,1)S(1)}, bf16[544,128]{1,0:T(8,128)(2,1)S(1)}, u32[]{:S(2)}, u32[]{:S(2)}) collective-permute-start(bf16[544,128]{1,0:T(8,128)(2,1)S(1)} %copy-done.3), channel_id=1, source_target_pairs={{0,2},{1,3},{2,4},{3,5},{4,6},{5,7},{6,0},{7,1},{8,10},{9,11},{10,... | collective-permute-start | bytes 417800 | tf_op jit(solution)/shard_map/ppermute | solution.py:47
  25.4 6.6 %collective-permute-start.9 = (bf16[544,128]{1,0:T(8,128)(2,1)S(1)}, bf16[544,128]{1,0:T(8,128)(2,1)S(1)}, u32[]{:S(2)}, u32[]{:S(2)}) collective-permute-start(bf16[544,128]{1,0:T(8,128)(2,1)S(1)} %copy-done.3), channel_id=1, source_target_pairs={{0,4},{1,5},{2,6},{3,7},{4,0},{5,1},{6,2},{7,3},{8,12},{9,13},{10,... | collective-permute-start | bytes 417800 | tf_op jit(solution)/shard_map/ppermute | solution.py:47
  26.1 5.9 %collective-permute-start.11 = (bf16[512,256]{1,0:T(8,128)(2,1)S(1)}, bf16[512,256]{1,0:T(8,128)(2,1)S(1)}, u32[]{:S(2)}, u32[]{:S(2)}) collective-permute-start(bf16[512,256]{1,0:T(8,128)(2,1)S(1)} %copy-done.2), channel_id=1, source_target_pairs={{0,1},{1,0},{2,3},{3,2},{4,5},{5,4},{6,7},{7,6},{8,9},{9,8},{10,11... | collective-permute-start | bytes 786440 | tf_op jit(solution)/shard_map/ppermute | solution.py:47
  26.4 0.9 copy-start
  28.4 11.7 %collective-permute-start.4 = (bf16[96,512]{1,0:T(8,128)(2,1)S(1)}, bf16[96,512]{1,0:T(8,128)(2,1)S(1)}, u32[]{:S(2)}, u32[]{:S(2)}) collective-permute-start(bf16[96,512]{1,0:T(8,128)(2,1)S(1)} %get-tuple-element.29), channel_id=1, source_target_pairs={{0,32},{1,33},{2,34},{3,35},{4,36},{5,37},{6,38},{7,39},{8,40},{9,... | collective-permute-start | bytes 294920 | tf_op jit(solution)/shard_map/ppermute | solution.py:47
  33.0 14.6 %collective-permute-start.12 = (bf16[160,512]{1,0:T(8,128)(2,1)S(1)}, bf16[160,512]{1,0:T(8,128)(2,1)S(1)}, u32[]{:S(2)}, u32[]{:S(2)}) collective-permute-start(bf16[160,512]{1,0:T(8,128)(2,1)S(1)} %get-tuple-element.34), channel_id=1, source_target_pairs={{0,32},{1,33},{2,34},{3,35},{4,36},{5,37},{6,38},{7,39},{8,40},{9,... | collective-permute-start | bytes 491528 | tf_op jit(solution)/shard_map/ppermute | solution.py:47
  35.0 12.6 %collective-permute-start.13 = (bf16[160,512]{1,0:T(8,128)(2,1)S(1)}, bf16[160,512]{1,0:T(8,128)(2,1)S(1)}, u32[]{:S(2)}, u32[]{:S(2)}) collective-permute-start(bf16[160,512]{1,0:T(8,128)(2,1)S(1)} %get-tuple-element.35), channel_id=1, source_target_pairs={{0,64},{1,65},{2,66},{3,67},{4,68},{5,69},{6,70},{7,71},{8,72},{9,... | collective-permute-start | bytes 491528 | tf_op jit(solution)/shard_map/ppermute | solution.py:47
  38.6 9.1 %collective-permute-start.14 = (bf16[160,512]{1,0:T(8,128)(2,1)S(1)}, bf16[160,512]{1,0:T(8,128)(2,1)S(1)}, u32[]{:S(2)}, u32[]{:S(2)}) collective-permute-start(bf16[160,512]{1,0:T(8,128)(2,1)S(1)} %get-tuple-element.36), channel_id=1, source_target_pairs={{0,96},{1,97},{2,98},{3,99},{4,100},{5,101},{6,102},{7,103},{8,104... | collective-permute-start | bytes 491528 | tf_op jit(solution)/shard_map/ppermute | solution.py:47
  39.6 6.8 %collective-permute-start.5 = (bf16[96,512]{1,0:T(8,128)(2,1)S(1)}, bf16[96,512]{1,0:T(8,128)(2,1)S(1)}, u32[]{:S(2)}, u32[]{:S(2)}) collective-permute-start(bf16[96,512]{1,0:T(8,128)(2,1)S(1)} %get-tuple-element.30), channel_id=1, source_target_pairs={{0,64},{1,65},{2,66},{3,67},{4,68},{5,69},{6,70},{7,71},{8,72},{9,... | collective-permute-start | bytes 294920 | tf_op jit(solution)/shard_map/ppermute | solution.py:47
  40.1 7.3 %collective-permute-start.6 = (bf16[96,512]{1,0:T(8,128)(2,1)S(1)}, bf16[96,512]{1,0:T(8,128)(2,1)S(1)}, u32[]{:S(2)}, u32[]{:S(2)}) collective-permute-start(bf16[96,512]{1,0:T(8,128)(2,1)S(1)} %get-tuple-element.31), channel_id=1, source_target_pairs={{0,96},{1,97},{2,98},{3,99},{4,100},{5,101},{6,102},{7,103},{8,104... | collective-permute-start | bytes 294920 | tf_op jit(solution)/shard_map/ppermute | solution.py:47
  47.5 6.0 %collective-permute-start.7 = (bf16[384,512]{1,0:T(8,128)(2,1)S(1)}, bf16[384,512]{1,0:T(8,128)(2,1)S(1)}, u32[]{:S(2)}, u32[]{:S(2)}) collective-permute-start(bf16[384,512]{1,0:T(8,128)(2,1)S(1)} %join.2.refs_0_), channel_id=1, source_target_pairs={{0,1},{1,0},{2,3},{3,2},{4,5},{5,4},{6,7},{7,6},{8,9},{9,8},{10,11... | collective-permute-start | bytes 1179656 | tf_op jit(solution)/shard_map/ppermute | solution.py:47
  47.7 29.2 %collective-permute-start.20 = (bf16[480,512]{1,0:T(8,128)(2,1)S(1)}, bf16[480,512]{1,0:T(8,128)(2,1)S(1)}, u32[]{:S(2)}, u32[]{:S(2)}) collective-permute-start(bf16[480,512]{1,0:T(8,128)(2,1)S(1)} %join.3.refs_3_), channel_id=1, source_target_pairs={{0,8},{1,9},{2,10},{3,11},{4,12},{5,13},{6,14},{7,15},{8,16},{9,17... | collective-permute-start | bytes 1474568 | tf_op jit(solution)/shard_map/ppermute | solution.py:47
  48.2 45.7 %collective-permute-start.18 = (bf16[480,512]{1,0:T(8,128)(2,1)S(1)}, bf16[480,512]{1,0:T(8,128)(2,1)S(1)}, u32[]{:S(2)}, u32[]{:S(2)}) collective-permute-start(bf16[480,512]{1,0:T(8,128)(2,1)S(1)} %join.3.refs_3_), channel_id=1, source_target_pairs={{0,24},{1,25},{2,26},{3,27},{4,28},{5,29},{6,30},{7,31},{8,0},{9,1... | collective-permute-start | bytes 1474568 | tf_op jit(solution)/shard_map/ppermute | solution.py:47
  49.8 61.5 %collective-permute-start.16 = (bf16[480,512]{1,0:T(8,128)(2,1)S(1)}, bf16[480,512]{1,0:T(8,128)(2,1)S(1)}, u32[]{:S(2)}, u32[]{:S(2)}) collective-permute-start(bf16[480,512]{1,0:T(8,128)(2,1)S(1)} %join.3.refs_3_), channel_id=1, source_target_pairs={{0,16},{1,17},{2,18},{3,19},{4,20},{5,21},{6,22},{7,23},{8,24},{9,... | collective-permute-start | bytes 1474568 | tf_op jit(solution)/shard_map/ppermute | solution.py:47
  51.2 24.2 %collective-permute-start.19 = (bf16[160,512]{1,0:T(8,128)(2,1)S(1)}, bf16[160,512]{1,0:T(8,128)(2,1)S(1)}, u32[]{:S(2)}, u32[]{:S(2)}) collective-permute-start(bf16[160,512]{1,0:T(8,128)(2,1)S(1)} %get-tuple-element.33.refs_2_), channel_id=1, source_target_pairs={{0,8},{1,9},{2,10},{3,11},{4,12},{5,13},{6,14},{7,15},{8,16},{9,17... | collective-permute-start | bytes 491528 | tf_op jit(solution)/shard_map/ppermute | solution.py:47
  53.5 40.4 %collective-permute-start.17 = (bf16[160,512]{1,0:T(8,128)(2,1)S(1)}, bf16[160,512]{1,0:T(8,128)(2,1)S(1)}, u32[]{:S(2)}, u32[]{:S(2)}) collective-permute-start(bf16[160,512]{1,0:T(8,128)(2,1)S(1)} %get-tuple-element.33.refs_2_), channel_id=1, source_target_pairs={{0,24},{1,25},{2,26},{3,27},{4,28},{5,29},{6,30},{7,31},{8,0},{9,1... | collective-permute-start | bytes 491528 | tf_op jit(solution)/shard_map/ppermute | solution.py:47
  75.4 35.8 %collective-permute-start.15 = (bf16[160,512]{1,0:T(8,128)(2,1)S(1)}, bf16[160,512]{1,0:T(8,128)(2,1)S(1)}, u32[]{:S(2)}, u32[]{:S(2)}) collective-permute-start(bf16[160,512]{1,0:T(8,128)(2,1)S(1)} %get-tuple-element.33.refs_2_), channel_id=1, source_target_pairs={{0,16},{1,17},{2,18},{3,19},{4,20},{5,21},{6,22},{7,23},{8,24},{9,... | collective-permute-start | bytes 491528 | tf_op jit(solution)/shard_map/ppermute | solution.py:47
  76.8 72.6 %slice-start = ((s8[8388608]{0:T(1024)(128)(4,1)}), s8[4194304]{0:T(1024)(128)(4,1)S(1)}, s32[]{:S(2)}) async-start(s8[8388608]{0:T(1024)(128)(4,1)} %bitcast.15), calls=%async_computation | async-start | bytes 8388608
  93.9 55.5 %slice-start.1 = ((s8[8388608]{0:T(1024)(128)(4,1)}), s8[4194304]{0:T(1024)(128)(4,1)S(1)}, s32[]{:S(2)}) async-start(s8[8388608]{0:T(1024)(128)(4,1)} %bitcast.15), calls=%async_computation.1 | async-start | bytes 8388608
  111.2 38.2 %copy-start.4 = (f32[4096]{0:T(1024)S(1)}, f32[4096]{0:T(1024)}, u32[]{:S(2)}) copy-start(f32[4096]{0:T(1024)} %param.21) | copy-start | bytes 49156
  128.4 2.3 %collective-permute-start.21 = (f32[4,88,512]{2,1,0:T(8,128)S(1)}, f32[4,88,512]{2,1,0:T(8,128)S(1)}, u32[]{:S(2)}, u32[]{:S(2)}) collective-permute-start(f32[4,88,512]{2,1,0:T(8,128)S(1)} %get-tuple-element.40), channel_id=1, source_target_pairs={{0,1},{1,0},{2,3},{3,2},{4,5},{5,4},{6,7},{7,6},{8,9},{9,8},{10,11... | collective-permute-start | bytes 2162696 | tf_op jit(solution)/shard_map/ppermute | solution.py:47
  130.8 6.6 %collective-permute-start.22 = (bf16[64,512]{1,0:T(8,128)(2,1)S(1)}, bf16[64,512]{1,0:T(8,128)(2,1)S(1)}, u32[]{:S(2)}, u32[]{:S(2)}) collective-permute-start(bf16[64,512]{1,0:T(8,128)(2,1)S(1)} %get-tuple-element.42), channel_id=1, source_target_pairs={{32,0},{33,1},{34,2},{35,3},{36,4},{37,5},{38,6},{39,7},{40,8},{41... | collective-permute-start | bytes 196616 | tf_op jit(solution)/shard_map/ppermute | solution.py:47
  134.2 6.1 %collective-permute-start.23 = (bf16[64,512]{1,0:T(8,128)(2,1)S(1)}, bf16[64,512]{1,0:T(8,128)(2,1)S(1)}, u32[]{:S(2)}, u32[]{:S(2)}) collective-permute-start(bf16[64,512]{1,0:T(8,128)(2,1)S(1)} %get-tuple-element.43), channel_id=1, source_target_pairs={{64,0},{65,1},{66,2},{67,3},{68,4},{69,5},{70,6},{71,7},{72,8},{73... | collective-permute-start | bytes 196616 | tf_op jit(solution)/shard_map/ppermute | solution.py:47
  134.7 6.2 %collective-permute-start.24 = (bf16[64,512]{1,0:T(8,128)(2,1)S(1)}, bf16[64,512]{1,0:T(8,128)(2,1)S(1)}, u32[]{:S(2)}, u32[]{:S(2)}) collective-permute-start(bf16[64,512]{1,0:T(8,128)(2,1)S(1)} %get-tuple-element.44), channel_id=1, source_target_pairs={{96,0},{97,1},{98,2},{99,3},{100,4},{101,5},{102,6},{103,7},{104,8... | collective-permute-start | bytes 196616 | tf_op jit(solution)/shard_map/ppermute | solution.py:47
  141.0 4.4 %collective-permute-start.25 = (bf16[256,128]{1,0:T(8,128)(2,1)S(1)}, bf16[256,128]{1,0:T(8,128)(2,1)S(1)}, u32[]{:S(2)}, u32[]{:S(2)}) collective-permute-start(bf16[256,128]{1,0:T(8,128)(2,1)S(1)} %get-tuple-element.46), channel_id=1, source_target_pairs={{2,0},{3,1},{4,2},{5,3},{6,4},{7,5},{0,6},{1,7},{10,8},{11,9},{12,... | collective-permute-start | bytes 196616 | tf_op jit(solution)/shard_map/ppermute | solution.py:47
  142.1 6.1 %collective-permute-start.26 = (bf16[256,128]{1,0:T(8,128)(2,1)S(1)}, bf16[256,128]{1,0:T(8,128)(2,1)S(1)}, u32[]{:S(2)}, u32[]{:S(2)}) collective-permute-start(bf16[256,128]{1,0:T(8,128)(2,1)S(1)} %get-tuple-element.47), channel_id=1, source_target_pairs={{4,0},{5,1},{6,2},{7,3},{0,4},{1,5},{2,6},{3,7},{12,8},{13,9},{14,... | collective-permute-start | bytes 196616 | tf_op jit(solution)/shard_map/ppermute | solution.py:47
  144.0 5.5 %collective-permute-start.27 = (bf16[256,128]{1,0:T(8,128)(2,1)S(1)}, bf16[256,128]{1,0:T(8,128)(2,1)S(1)}, u32[]{:S(2)}, u32[]{:S(2)}) collective-permute-start(bf16[256,128]{1,0:T(8,128)(2,1)S(1)} %get-tuple-element.48), channel_id=1, source_target_pairs={{6,0},{7,1},{0,2},{1,3},{2,4},{3,5},{4,6},{5,7},{14,8},{15,9},{8,1... | collective-permute-start | bytes 196616 | tf_op jit(solution)/shard_map/ppermute | solution.py:47

commit v4 on v3

--- a/solution.py
+++ b/solution.py
@@ -280,12 +280,12 @@
     def exact(kq, kk, free):
         m_old = m_ref[kq]
         s = jnp.dot(ks[kk], qs[kq], preferred_element_type=F32) * SCALE
-        kr = lax.broadcasted_iota(jnp.int32, (512, 1024), 0)
-        qr = lax.broadcasted_iota(jnp.int32, (512, 1024), 1)
+        kr = lax.broadcasted_iota(jnp.int32, (512, 1), 0)
+        qr = lax.broadcasted_iota(jnp.int32, (1, 1024), 1)
         kpos = ((y - (kr >> 7)) & 3) * 256 + c * 128 + (kr & 127)
         par = jnp.where(qr < 512, c, 1 - c)
-        qpos = ((y - (qr >> 7)) & 3) * 256 + par * 128 + (qr & 127)
-        s = jnp.where(kpos <= qpos + free, s, -1e30)
+        qpos = ((y - (qr >> 7)) & 3) * 256 + par * 128 + (qr & 127) + free
+        s = jnp.where(kpos <= qpos, s, -1e30)
         m_new = jnp.maximum(m_old, jnp.max(s, axis=0, keepdims=True))
         p = jnp.exp2(s - m_new).astype(BF)
         o = jnp.dot(vs[kk], p, preferred_element_type=F32)

time: 153 us -> 153 us (level)
  no operation moved by 1% of the time
where the time goes in v4:
time: 153 us
  Pallas kernels  85.9 us (56%)
  starting transfers between devices  36.6 us (24%)
  waiting for transfers between devices  27.5 us (18%)
    pallas_call x4, Pallas kernels, attention(): pl.pallas_call(functools.partial(attn_kernel, first, last), out_shape=out...  70.5 us
    ppermute x28, starting transfers between devices, send(): return lax.ppermute(a, AXES, perm)  36.6 us
    ppermute x28, waiting for transfers between devices, send(): return lax.ppermute(a, AXES, perm)  27.5 us
    pallas_call x1, Pallas kernels, kv_down_call(): pl.pallas_call(kv_down_kernel, out_shape=[jax.ShapeDtypeStruct((rows, d),...  5.26 us
    pallas_call x1, Pallas kernels, q_down_call(): pl.pallas_call(q_down_kernel, out_shape=jax.ShapeDtypeStruct((768, rows),...  4.6 us
    pallas_call x1, Pallas kernels, out_call(): pl.pallas_call(out_kernel, out_shape=jax.ShapeDtypeStruct((128, w.shape[1...  3.18 us
  transfers between devices with their start and end apart: 28, of which 13 were waited for; matrix products, arithmetic and copies ran while one was open for 0% of the time, Pallas kernels for 36%

profile of v4, /device:TPU:6, one launch (start us, length us, event | category | flops | bytes accessed | tf_op | source)
XLA Modules:
  0.0 152.6 jit_solution(1668065415067345933)
XLA Ops:
  0.0 0.7 multiply_sine_fusion.1
  0.7 5.3 %kv_down.1 = (bf16[128,4096]{1,0:T(8,128)(2,1)}, bf16[544,128]{1,0:T(8,128)(2,1)}) custom-call(bf16[128,4096]{1,0:T(8,128)(2,1)} %tok.1, f32[1,4096]{1,0:T(1,128)} %bitcast.21, bf16[4096,512]{1,0:T(8,128)(2,1)} %kvd.1, bf16[32,4096]{1,0:T(8,128)(2,1)} %bitcast.20, f32[1,512]{1,0:T(1,128)} %bitcast.23, f32[16,128]{1,0:T(8,128)} %get-tuple-element.52.cos, ...), custom_call_target="tpu_custom_call" | custom-call | tf_op jit(solution)/shard_map/kv_down/pallas_call | solution.py:107
  6.0 4.6 %q_down.1.p0 = bf16[768,128]{1,0:T(8,128)(2,1)} custom-call(bf16[128,4096]{1,0:T(8,128)(2,1)} %get-tuple-element.27.src, bf16[4096,768]{1,0:T(8,128)(2,1)} %qd.1, f32[6,128]{1,0:T(8,128)} %bitcast.22), custom_call_target="tpu_custom_call" | custom-call | tf_op jit(solution)/shard_map/q_down/pallas_call | solution.py:140
  10.7 1.6 %collective-permute-start = (bf16[768,128]{1,0:T(8,128)(2,1)}, bf16[768,128]{1,0:T(8,128)(2,1)S(1)}, u32[]{:S(2)}, u32[]{:S(2)}) collective-permute-start(bf16[768,128]{1,0:T(8,128)(2,1)} %q_down.1.p0), channel_id=1, source_target_pairs={{0,2},{1,3},{2,4},{3,5},{4,6},{5,7},{6,0},{7,1},{8,10},{9,11},{10,... | collective-permute-start | bytes 589832 | tf_op jit(solution)/shard_map/ppermute | solution.py:47
  12.3 2.9 %collective-permute-start.1 = (bf16[768,128]{1,0:T(8,128)(2,1)}, bf16[768,128]{1,0:T(8,128)(2,1)S(1)}, u32[]{:S(2)}, u32[]{:S(2)}) collective-permute-start(bf16[768,128]{1,0:T(8,128)(2,1)} %q_down.1.p0), channel_id=1, source_target_pairs={{0,4},{1,5},{2,6},{3,7},{4,0},{5,1},{6,2},{7,3},{8,12},{9,13},{10,... | collective-permute-start | bytes 589832 | tf_op jit(solution)/shard_map/ppermute | solution.py:47
  15.2 1.3 collective-permute-start.2
  16.8 2.1 %collective-permute-done.p1 = bf16[768,128]{1,0:T(8,128)(2,1)S(1)} collective-permute-done((bf16[768,128]{1,0:T(8,128)(2,1)}, bf16[768,128]{1,0:T(8,128)(2,1)S(1)}, u32[]{:S(2)}, u32[]{:S(2)}) %collective-permute-start) | collective-permute-done | bytes 196640 | tf_op jit(solution)/shard_map/ppermute | solution.py:47
  18.9 1.4 collective-permute-start.8
  20.3 5.1 %collective-permute-done.1.p2 = bf16[768,128]{1,0:T(8,128)(2,1)S(1)} collective-permute-done((bf16[768,128]{1,0:T(8,128)(2,1)}, bf16[768,128]{1,0:T(8,128)(2,1)S(1)}, u32[]{:S(2)}, u32[]{:S(2)}) %collective-permute-start.1) | collective-permute-done | bytes 196640 | tf_op jit(solution)/shard_map/ppermute | solution.py:47
  25.4 0.7 collective-permute-start.9
  26.1 0.2 multiply_sine_fusion
  26.4 0.9 copy-done
  27.3 1.1 q_up.1
  28.4 2.0 %collective-permute-start.4 = (bf16[96,512]{1,0:T(8,128)(2,1)S(1)}, bf16[96,512]{1,0:T(8,128)(2,1)S(1)}, u32[]{:S(2)}, u32[]{:S(2)}) collective-permute-start(bf16[96,512]{1,0:T(8,128)(2,1)S(1)} %get-tuple-element.29), channel_id=1, source_target_pairs={{0,32},{1,33},{2,34},{3,35},{4,36},{5,37},{6,38},{7,39},{8,40},{9,... | collective-permute-start | bytes 294920 | tf_op jit(solution)/shard_map/ppermute | solution.py:47
  30.4 1.5 %collective-permute-done.9.p2 = bf16[544,128]{1,0:T(8,128)(2,1)S(1)} collective-permute-done((bf16[544,128]{1,0:T(8,128)(2,1)S(1)}, bf16[544,128]{1,0:T(8,128)(2,1)S(1)}, u32[]{:S(2)}, u32[]{:S(2)}) %collective-permute-start.9) | collective-permute-done | bytes 139296 | tf_op jit(solution)/shard_map/ppermute | solution.py:47
  31.9 1.0 kv_up.1
  33.0 2.0 %collective-permute-start.12 = (bf16[160,512]{1,0:T(8,128)(2,1)S(1)}, bf16[160,512]{1,0:T(8,128)(2,1)S(1)}, u32[]{:S(2)}, u32[]{:S(2)}) collective-permute-start(bf16[160,512]{1,0:T(8,128)(2,1)S(1)} %get-tuple-element.34), channel_id=1, source_target_pairs={{0,32},{1,33},{2,34},{3,35},{4,36},{5,37},{6,38},{7,39},{8,40},{9,... | collective-permute-start | bytes 491528 | tf_op jit(solution)/shard_map/ppermute | solution.py:47
  35.0 3.6 %collective-permute-start.13 = (bf16[160,512]{1,0:T(8,128)(2,1)S(1)}, bf16[160,512]{1,0:T(8,128)(2,1)S(1)}, u32[]{:S(2)}, u32[]{:S(2)}) collective-permute-start(bf16[160,512]{1,0:T(8,128)(2,1)S(1)} %get-tuple-element.35), channel_id=1, source_target_pairs={{0,64},{1,65},{2,66},{3,67},{4,68},{5,69},{6,70},{7,71},{8,72},{9,... | collective-permute-start | bytes 491528 | tf_op jit(solution)/shard_map/ppermute | solution.py:47
  38.6 1.0 collective-permute-start.14
  39.6 0.5 collective-permute-start.5
  40.1 3.1 %collective-permute-start.6 = (bf16[96,512]{1,0:T(8,128)(2,1)S(1)}, bf16[96,512]{1,0:T(8,128)(2,1)S(1)}, u32[]{:S(2)}, u32[]{:S(2)}) collective-permute-start(bf16[96,512]{1,0:T(8,128)(2,1)S(1)} %get-tuple-element.31), channel_id=1, source_target_pairs={{0,96},{1,97},{2,98},{3,99},{4,100},{5,101},{6,102},{7,103},{8,104... | collective-permute-start | bytes 294920 | tf_op jit(solution)/shard_map/ppermute | solution.py:47
  43.3 3.1 %collective-permute-done.5.refs_2_ = bf16[96,512]{1,0:T(8,128)(2,1)S(1)} collective-permute-done((bf16[96,512]{1,0:T(8,128)(2,1)S(1)}, bf16[96,512]{1,0:T(8,128)(2,1)S(1)}, u32[]{:S(2)}, u32[]{:S(2)}) %collective-permute-start.5) | collective-permute-done | bytes 98336 | tf_op jit(solution)/shard_map/ppermute | solution.py:47
  46.3 1.1 collective-permute-done.6.refs_3_
  47.7 0.6 collective-permute-start.20
  48.2 1.5 %collective-permute-start.18 = (bf16[480,512]{1,0:T(8,128)(2,1)S(1)}, bf16[480,512]{1,0:T(8,128)(2,1)S(1)}, u32[]{:S(2)}, u32[]{:S(2)}) collective-permute-start(bf16[480,512]{1,0:T(8,128)(2,1)S(1)} %join.3.refs_3_), channel_id=1, source_target_pairs={{0,24},{1,25},{2,26},{3,27},{4,28},{5,29},{6,30},{7,31},{8,0},{9,1... | collective-permute-start | bytes 1474568 | tf_op jit(solution)/shard_map/ppermute | solution.py:47
  49.8 1.4 collective-permute-start.16
  51.2 2.1 %collective-permute-start.19 = (bf16[160,512]{1,0:T(8,128)(2,1)S(1)}, bf16[160,512]{1,0:T(8,128)(2,1)S(1)}, u32[]{:S(2)}, u32[]{:S(2)}) collective-permute-start(bf16[160,512]{1,0:T(8,128)(2,1)S(1)} %get-tuple-element.33.refs_2_), channel_id=1, source_target_pairs={{0,8},{1,9},{2,10},{3,11},{4,12},{5,13},{6,14},{7,15},{8,16},{9,17... | collective-permute-start | bytes 491528 | tf_op jit(solution)/shard_map/ppermute | solution.py:47
  53.5 0.2 collective-permute-start.17
  53.7 19.1 %attn.4 = (f32[4,88,1024]{2,1,0:T(8,128)S(1)}, bf16[4,96,1024]{2,1,0:T(8,128)(2,1)S(1)}) custom-call(s32[5]{0:T(128)S(1)} %stack.50.s.s_ref, bf16[384,512]{1,0:T(8,128)(2,1)S(1)} %join.2.refs_0_, bf16[384,512]{1,0:T(8,128)(2,1)S(1)} %collective-permute-done.7.refs_1_, bf16[160,512]{1,0:T(8,128)(2,1)S(1)} %get-tuple-element.33.refs_2_, ...), custom_call_target="tpu_custom_call" | custom-call | flops 1500000000 | bytes 1048576 | tf_op jit(solution)/shard_map/attn/pallas_call | solution.py:380
  72.8 2.6 %collective-permute-done.19.refs_1_ = bf16[160,512]{1,0:T(8,128)(2,1)S(1)} collective-permute-done((bf16[160,512]{1,0:T(8,128)(2,1)S(1)}, bf16[160,512]{1,0:T(8,128)(2,1)S(1)}, u32[]{:S(2)}, u32[]{:S(2)}) %collective-permute-start.19) | collective-permute-done | bytes 163872 | tf_op jit(solution)/shard_map/ppermute | solution.py:47
  75.4 1.4 collective-permute-start.15
  76.9 17.1 %attn.5.refs_3_ = f32[4,88,1024]{2,1,0:T(8,128)S(1)} custom-call(s32[5]{0:T(128)S(1)} %stack.56.s_ref, bf16[4,96,1024]{2,1,0:T(8,128)(2,1)S(1)} %get-tuple-element.37.refs_0_, bf16[160,512]{1,0:T(8,128)(2,1)S(1)} %collective-permute-done.19.refs_1_, bf16[480,512]{1,0:T(8,128)(2,1)S(1)} %collective-permute-done.20.refs_2_, ...), custom_call_target="tpu_custom_call" | custom-call | flops 1500000000 | bytes 1048576 | tf_op jit(solution)/shard_map/attn/pallas_call | solution.py:380
  94.0 17.2 %attn.6.refs_3_ = f32[4,88,1024]{2,1,0:T(8,128)S(1)} custom-call(s32[5]{0:T(128)S(1)} %stack.54.s_ref, bf16[4,96,1024]{2,1,0:T(8,128)(2,1)S(1)} %get-tuple-element.37.refs_0_, bf16[160,512]{1,0:T(8,128)(2,1)S(1)} %collective-permute-done.17.refs_1_, bf16[480,512]{1,0:T(8,128)(2,1)S(1)} %collective-permute-done.18.refs_2_, f32[4,88,1024]{2,1,0:T(8,128)S(1)} %attn.5.refs_3_), custom_call_target="tpu_custom_call" | custom-call | flops 1500000000 | bytes 1048576 | tf_op jit(solution)/shard_map/attn/pallas_call | solution.py:380
  111.2 17.1 %attn.7 = (f32[4,88,512]{2,1,0:T(8,128)S(1)}, f32[4,88,512]{2,1,0:T(8,128)S(1)}) custom-call(s32[5]{0:T(128)S(1)} %stack.52.s_ref, bf16[4,96,1024]{2,1,0:T(8,128)(2,1)S(1)} %get-tuple-element.37.refs_0_, bf16[160,512]{1,0:T(8,128)(2,1)S(1)} %collective-permute-done.15.refs_1_, bf16[480,512]{1,0:T(8,128)(2,1)S(1)} %collective-permute-done.16.refs_2_, ...), custom_call_target="tpu_custom_call" | custom-call | flops 1500000000 | bytes 1048576 | tf_op jit(solution)/shard_map/attn/pallas_call | solution.py:380
  128.5 2.2 %collective-permute-done.21.theirs = f32[4,88,512]{2,1,0:T(8,128)S(1)} collective-permute-done((f32[4,88,512]{2,1,0:T(8,128)S(1)}, f32[4,88,512]{2,1,0:T(8,128)S(1)}, u32[]{:S(2)}, u32[]{:S(2)}) %collective-permute-start.21) | collective-permute-done | bytes 720928 | tf_op jit(solution)/shard_map/ppermute | solution.py:47
  130.8 3.4 %collective-permute-start.22 = (bf16[64,512]{1,0:T(8,128)(2,1)S(1)}, bf16[64,512]{1,0:T(8,128)(2,1)S(1)}, u32[]{:S(2)}, u32[]{:S(2)}) collective-permute-start(bf16[64,512]{1,0:T(8,128)(2,1)S(1)} %get-tuple-element.42), channel_id=1, source_target_pairs={{32,0},{33,1},{34,2},{35,3},{36,4},{37,5},{38,6},{39,7},{40,8},{41... | collective-permute-start | bytes 196616 | tf_op jit(solution)/shard_map/ppermute | solution.py:47
  134.2 0.5 collective-permute-start.23
  134.7 1.2 collective-permute-start.24
  135.9 1.5 collective-permute-done.22.r1
  137.4 2.8 %collective-permute-done.23.r2 = bf16[64,512]{1,0:T(8,128)(2,1)S(1)} collective-permute-done((bf16[64,512]{1,0:T(8,128)(2,1)S(1)}, bf16[64,512]{1,0:T(8,128)(2,1)S(1)}, u32[]{:S(2)}, u32[]{:S(2)}) %collective-permute-start.23) | collective-permute-done | bytes 65568 | tf_op jit(solution)/shard_map/ppermute | solution.py:47
  140.2 0.7 collective-permute-done.24.r3
  141.0 1.1 collective-permute-start.25
  142.1 1.8 %collective-permute-start.26 = (bf16[256,128]{1,0:T(8,128)(2,1)S(1)}, bf16[256,128]{1,0:T(8,128)(2,1)S(1)}, u32[]{:S(2)}, u32[]{:S(2)}) collective-permute-start(bf16[256,128]{1,0:T(8,128)(2,1)S(1)} %get-tuple-element.47), channel_id=1, source_target_pairs={{4,0},{5,1},{6,2},{7,3},{0,4},{1,5},{2,6},{3,7},{12,8},{13,9},{14,... | collective-permute-start | bytes 196616 | tf_op jit(solution)/shard_map/ppermute | solution.py:47
  144.0 0.8 collective-permute-start.27
  144.8 0.7 collective-permute-done.25.t1
  145.4 2.8 %collective-permute-done.26.t2 = bf16[256,128]{1,0:T(8,128)(2,1)S(1)} collective-permute-done((bf16[256,128]{1,0:T(8,128)(2,1)S(1)}, bf16[256,128]{1,0:T(8,128)(2,1)S(1)}, u32[]{:S(2)}, u32[]{:S(2)}) %collective-permute-start.26) | collective-permute-done | bytes 65568 | tf_op jit(solution)/shard_map/ppermute | solution.py:47
  148.2 1.2 collective-permute-done.27.t3
  149.4 3.2 %out_proj.1 = bf16[128,4096]{1,0:T(8,128)(2,1)} custom-call(s32[5]{0:T(128)S(1)} %stack.50.s.s_ref, bf16[256,128]{1,0:T(8,128)(2,1)S(1)} %get-tuple-element.45.t0, bf16[256,128]{1,0:T(8,128)(2,1)S(1)} %collective-permute-done.25.t1, bf16[256,128]{1,0:T(8,128)(2,1)S(1)} %collective-permute-done.26.t2, bf16[256,128]{1,0:T(8,128)(2,1)S(1)} %collective-permute-done.27.t3, ...), custom_call_target="tpu_custom_call" | custom-call | tf_op jit(solution)/shard_map/out_proj/pallas_call | solution.py:423
  (46 shorter events, 1.0 us)
Async XLA Ops:
  6.0 10.5 %copy-start.3 = (bf16[544,128]{1,0:T(8,128)(2,1)S(1)}, bf16[544,128]{1,0:T(8,128)(2,1)}, u32[]{:S(2)}) copy-start(bf16[544,128]{1,0:T(8,128)(2,1)} %get-tuple-element.32.p0) | copy-start | bytes 417796
  6.0 10.6 %copy-start.1 = (bf16[768,192]{0,1:T(8,128)(2,1)S(1)}, bf16[768,192]{0,1:T(8,128)(2,1)}, u32[]{:S(2)}) copy-start(bf16[768,192]{0,1:T(8,128)(2,1)} %param.18) | copy-start | bytes 884740
  6.0 20.0 %copy-start.2 = (bf16[512,256]{1,0:T(8,128)(2,1)S(1)}, bf16[512,256]{1,0:T(8,128)(2,1)}, u32[]{:S(2)}) copy-start(bf16[512,256]{1,0:T(8,128)(2,1)} %own.1) | copy-start | bytes 786436
  10.7 8.2 %collective-permute-start = (bf16[768,128]{1,0:T(8,128)(2,1)}, bf16[768,128]{1,0:T(8,128)(2,1)S(1)}, u32[]{:S(2)}, u32[]{:S(2)}) collective-permute-start(bf16[768,128]{1,0:T(8,128)(2,1)} %q_down.1.p0), channel_id=1, source_target_pairs={{0,2},{1,3},{2,4},{3,5},{4,6},{5,7},{6,0},{7,1},{8,10},{9,11},{10,... | collective-permute-start | bytes 589832 | tf_op jit(solution)/shard_map/ppermute | solution.py:47
  12.3 13.1 %collective-permute-start.1 = (bf16[768,128]{1,0:T(8,128)(2,1)}, bf16[768,128]{1,0:T(8,128)(2,1)S(1)}, u32[]{:S(2)}, u32[]{:S(2)}) collective-permute-start(bf16[768,128]{1,0:T(8,128)(2,1)} %q_down.1.p0), channel_id=1, source_target_pairs={{0,4},{1,5},{2,6},{3,7},{4,0},{5,1},{6,2},{7,3},{8,12},{9,13},{10,... | collective-permute-start | bytes 589832 | tf_op jit(solution)/shard_map/ppermute | solution.py:47
  15.2 10.8 %collective-permute-start.2 = (bf16[768,128]{1,0:T(8,128)(2,1)}, bf16[768,128]{1,0:T(8,128)(2,1)S(1)}, u32[]{:S(2)}, u32[]{:S(2)}) collective-permute-start(bf16[768,128]{1,0:T(8,128)(2,1)} %q_down.1.p0), channel_id=1, source_target_pairs={{0,6},{1,7},{2,0},{3,1},{4,2},{5,3},{6,4},{7,5},{8,14},{9,15},{10,... | collective-permute-start | bytes 589832 | tf_op jit(solution)/shard_map/ppermute | solution.py:47
  16.6 13.8 %collective-permute-start.10 = (bf16[544,128]{1,0:T(8,128)(2,1)S(1)}, bf16[544,128]{1,0:T(8,128)(2,1)S(1)}, u32[]{:S(2)}, u32[]{:S(2)}) collective-permute-start(bf16[544,128]{1,0:T(8,128)(2,1)S(1)} %copy-done.3), channel_id=1, source_target_pairs={{0,6},{1,7},{2,0},{3,1},{4,2},{5,3},{6,4},{7,5},{8,14},{9,15},{10,... | collective-permute-start | bytes 417800 | tf_op jit(solution)/shard_map/ppermute | solution.py:47
  16.6 9.8 %collective-permute-start.3 = (bf16[192,768]{1,0:T(8,128)(2,1)S(1)}, bf16[192,768]{1,0:T(8,128)(2,1)S(1)}, u32[]{:S(2)}, u32[]{:S(2)}) collective-permute-start(bf16[192,768]{1,0:T(8,128)(2,1)S(1)} %bitcast.17), channel_id=1, source_target_pairs={{0,1},{1,0},{2,3},{3,2},{4,5},{5,4},{6,7},{7,6},{8,9},{9,8},{10,11... | collective-permute-start | bytes 884744 | tf_op jit(solution)/shard_map/ppermute | solution.py:47
  18.9 11.5 %collective-permute-start.8 = (bf16[544,128]{1,0:T(8,128)(2,1)S(1)}, bf16[544,128]{1,0:T(8,128)(2,1)S(1)}, u32[]{:S(2)}, u32[]{:S(2)}) collective-permute-start(bf16[544,128]{1,0:T(8,128)(2,1)S(1)} %copy-done.3), channel_id=1, source_target_pairs={{0,2},{1,3},{2,4},{3,5},{4,6},{5,7},{6,0},{7,1},{8,10},{9,11},{10,... | collective-permute-start | bytes 417800 | tf_op jit(solution)/shard_map/ppermute | solution.py:47
  25.4 6.6 %collective-permute-start.9 = (bf16[544,128]{1,0:T(8,128)(2,1)S(1)}, bf16[544,128]{1,0:T(8,128)(2,1)S(1)}, u32[]{:S(2)}, u32[]{:S(2)}) collective-permute-start(bf16[544,128]{1,0:T(8,128)(2,1)S(1)} %copy-done.3), channel_id=1, source_target_pairs={{0,4},{1,5},{2,6},{3,7},{4,0},{5,1},{6,2},{7,3},{8,12},{9,13},{10,... | collective-permute-start | bytes 417800 | tf_op jit(solution)/shard_map/ppermute | solution.py:47
  26.1 5.9 %collective-permute-start.11 = (bf16[512,256]{1,0:T(8,128)(2,1)S(1)}, bf16[512,256]{1,0:T(8,128)(2,1)S(1)}, u32[]{:S(2)}, u32[]{:S(2)}) collective-permute-start(bf16[512,256]{1,0:T(8,128)(2,1)S(1)} %copy-done.2), channel_id=1, source_target_pairs={{0,1},{1,0},{2,3},{3,2},{4,5},{5,4},{6,7},{7,6},{8,9},{9,8},{10,11... | collective-permute-start | bytes 786440 | tf_op jit(solution)/shard_map/ppermute | solution.py:47
  26.4 0.9 copy-start
  28.4 11.7 %collective-permute-start.4 = (bf16[96,512]{1,0:T(8,128)(2,1)S(1)}, bf16[96,512]{1,0:T(8,128)(2,1)S(1)}, u32[]{:S(2)}, u32[]{:S(2)}) collective-permute-start(bf16[96,512]{1,0:T(8,128)(2,1)S(1)} %get-tuple-element.29), channel_id=1, source_target_pairs={{0,32},{1,33},{2,34},{3,35},{4,36},{5,37},{6,38},{7,39},{8,40},{9,... | collective-permute-start | bytes 294920 | tf_op jit(solution)/shard_map/ppermute | solution.py:47
  33.0 14.6 %collective-permute-start.12 = (bf16[160,512]{1,0:T(8,128)(2,1)S(1)}, bf16[160,512]{1,0:T(8,128)(2,1)S(1)}, u32[]{:S(2)}, u32[]{:S(2)}) collective-permute-start(bf16[160,512]{1,0:T(8,128)(2,1)S(1)} %get-tuple-element.34), channel_id=1, source_target_pairs={{0,32},{1,33},{2,34},{3,35},{4,36},{5,37},{6,38},{7,39},{8,40},{9,... | collective-permute-start | bytes 491528 | tf_op jit(solution)/shard_map/ppermute | solution.py:47
  35.0 12.6 %collective-permute-start.13 = (bf16[160,512]{1,0:T(8,128)(2,1)S(1)}, bf16[160,512]{1,0:T(8,128)(2,1)S(1)}, u32[]{:S(2)}, u32[]{:S(2)}) collective-permute-start(bf16[160,512]{1,0:T(8,128)(2,1)S(1)} %get-tuple-element.35), channel_id=1, source_target_pairs={{0,64},{1,65},{2,66},{3,67},{4,68},{5,69},{6,70},{7,71},{8,72},{9,... | collective-permute-start | bytes 491528 | tf_op jit(solution)/shard_map/ppermute | solution.py:47
  38.6 9.1 %collective-permute-start.14 = (bf16[160,512]{1,0:T(8,128)(2,1)S(1)}, bf16[160,512]{1,0:T(8,128)(2,1)S(1)}, u32[]{:S(2)}, u32[]{:S(2)}) collective-permute-start(bf16[160,512]{1,0:T(8,128)(2,1)S(1)} %get-tuple-element.36), channel_id=1, source_target_pairs={{0,96},{1,97},{2,98},{3,99},{4,100},{5,101},{6,102},{7,103},{8,104... | collective-permute-start | bytes 491528 | tf_op jit(solution)/shard_map/ppermute | solution.py:47
  39.6 6.8 %collective-permute-start.5 = (bf16[96,512]{1,0:T(8,128)(2,1)S(1)}, bf16[96,512]{1,0:T(8,128)(2,1)S(1)}, u32[]{:S(2)}, u32[]{:S(2)}) collective-permute-start(bf16[96,512]{1,0:T(8,128)(2,1)S(1)} %get-tuple-element.30), channel_id=1, source_target_pairs={{0,64},{1,65},{2,66},{3,67},{4,68},{5,69},{6,70},{7,71},{8,72},{9,... | collective-permute-start | bytes 294920 | tf_op jit(solution)/shard_map/ppermute | solution.py:47
  40.1 7.3 %collective-permute-start.6 = (bf16[96,512]{1,0:T(8,128)(2,1)S(1)}, bf16[96,512]{1,0:T(8,128)(2,1)S(1)}, u32[]{:S(2)}, u32[]{:S(2)}) collective-permute-start(bf16[96,512]{1,0:T(8,128)(2,1)S(1)} %get-tuple-element.31), channel_id=1, source_target_pairs={{0,96},{1,97},{2,98},{3,99},{4,100},{5,101},{6,102},{7,103},{8,104... | collective-permute-start | bytes 294920 | tf_op jit(solution)/shard_map/ppermute | solution.py:47
  47.5 6.0 %collective-permute-start.7 = (bf16[384,512]{1,0:T(8,128)(2,1)S(1)}, bf16[384,512]{1,0:T(8,128)(2,1)S(1)}, u32[]{:S(2)}, u32[]{:S(2)}) collective-permute-start(bf16[384,512]{1,0:T(8,128)(2,1)S(1)} %join.2.refs_0_), channel_id=1, source_target_pairs={{0,1},{1,0},{2,3},{3,2},{4,5},{5,4},{6,7},{7,6},{8,9},{9,8},{10,11... | collective-permute-start | bytes 1179656 | tf_op jit(solution)/shard_map/ppermute | solution.py:47
  47.7 29.2 %collective-permute-start.20 = (bf16[480,512]{1,0:T(8,128)(2,1)S(1)}, bf16[480,512]{1,0:T(8,128)(2,1)S(1)}, u32[]{:S(2)}, u32[]{:S(2)}) collective-permute-start(bf16[480,512]{1,0:T(8,128)(2,1)S(1)} %join.3.refs_3_), channel_id=1, source_target_pairs={{0,8},{1,9},{2,10},{3,11},{4,12},{5,13},{6,14},{7,15},{8,16},{9,17... | collective-permute-start | bytes 1474568 | tf_op jit(solution)/shard_map/ppermute | solution.py:47
  48.2 45.7 %collective-permute-start.18 = (bf16[480,512]{1,0:T(8,128)(2,1)S(1)}, bf16[480,512]{1,0:T(8,128)(2,1)S(1)}, u32[]{:S(2)}, u32[]{:S(2)}) collective-permute-start(bf16[480,512]{1,0:T(8,128)(2,1)S(1)} %join.3.refs_3_), channel_id=1, source_target_pairs={{0,24},{1,25},{2,26},{3,27},{4,28},{5,29},{6,30},{7,31},{8,0},{9,1... | collective-permute-start | bytes 1474568 | tf_op jit(solution)/shard_map/ppermute | solution.py:47
  49.8 61.5 %collective-permute-start.16 = (bf16[480,512]{1,0:T(8,128)(2,1)S(1)}, bf16[480,512]{1,0:T(8,128)(2,1)S(1)}, u32[]{:S(2)}, u32[]{:S(2)}) collective-permute-start(bf16[480,512]{1,0:T(8,128)(2,1)S(1)} %join.3.refs_3_), channel_id=1, source_target_pairs={{0,16},{1,17},{2,18},{3,19},{4,20},{5,21},{6,22},{7,23},{8,24},{9,... | collective-permute-start | bytes 1474568 | tf_op jit(solution)/shard_map/ppermute | solution.py:47
  51.2 24.2 %collective-permute-start.19 = (bf16[160,512]{1,0:T(8,128)(2,1)S(1)}, bf16[160,512]{1,0:T(8,128)(2,1)S(1)}, u32[]{:S(2)}, u32[]{:S(2)}) collective-permute-start(bf16[160,512]{1,0:T(8,128)(2,1)S(1)} %get-tuple-element.33.refs_2_), channel_id=1, source_target_pairs={{0,8},{1,9},{2,10},{3,11},{4,12},{5,13},{6,14},{7,15},{8,16},{9,17... | collective-permute-start | bytes 491528 | tf_op jit(solution)/shard_map/ppermute | solution.py:47
  53.5 40.4 %collective-permute-start.17 = (bf16[160,512]{1,0:T(8,128)(2,1)S(1)}, bf16[160,512]{1,0:T(8,128)(2,1)S(1)}, u32[]{:S(2)}, u32[]{:S(2)}) collective-permute-start(bf16[160,512]{1,0:T(8,128)(2,1)S(1)} %get-tuple-element.33.refs_2_), channel_id=1, source_target_pairs={{0,24},{1,25},{2,26},{3,27},{4,28},{5,29},{6,30},{7,31},{8,0},{9,1... | collective-permute-start | bytes 491528 | tf_op jit(solution)/shard_map/ppermute | solution.py:47
  75.4 35.8 %collective-permute-start.15 = (bf16[160,512]{1,0:T(8,128)(2,1)S(1)}, bf16[160,512]{1,0:T(8,128)(2,1)S(1)}, u32[]{:S(2)}, u32[]{:S(2)}) collective-permute-start(bf16[160,512]{1,0:T(8,128)(2,1)S(1)} %get-tuple-element.33.refs_2_), channel_id=1, source_target_pairs={{0,16},{1,17},{2,18},{3,19},{4,20},{5,21},{6,22},{7,23},{8,24},{9,... | collective-permute-start | bytes 491528 | tf_op jit(solution)/shard_map/ppermute | solution.py:47
  76.8 72.6 %slice-start = ((s8[8388608]{0:T(1024)(128)(4,1)}), s8[4194304]{0:T(1024)(128)(4,1)S(1)}, s32[]{:S(2)}) async-start(s8[8388608]{0:T(1024)(128)(4,1)} %bitcast.15), calls=%async_computation | async-start | bytes 8388608
  93.9 55.5 %slice-start.1 = ((s8[8388608]{0:T(1024)(128)(4,1)}), s8[4194304]{0:T(1024)(128)(4,1)S(1)}, s32[]{:S(2)}) async-start(s8[8388608]{0:T(1024)(128)(4,1)} %bitcast.15), calls=%async_computation.1 | async-start | bytes 8388608
  111.2 38.2 %copy-start.4 = (f32[4096]{0:T(1024)S(1)}, f32[4096]{0:T(1024)}, u32[]{:S(2)}) copy-start(f32[4096]{0:T(1024)} %param.21) | copy-start | bytes 49156
  128.4 2.3 %collective-permute-start.21 = (f32[4,88,512]{2,1,0:T(8,128)S(1)}, f32[4,88,512]{2,1,0:T(8,128)S(1)}, u32[]{:S(2)}, u32[]{:S(2)}) collective-permute-start(f32[4,88,512]{2,1,0:T(8,128)S(1)} %get-tuple-element.40), channel_id=1, source_target_pairs={{0,1},{1,0},{2,3},{3,2},{4,5},{5,4},{6,7},{7,6},{8,9},{9,8},{10,11... | collective-permute-start | bytes 2162696 | tf_op jit(solution)/shard_map/ppermute | solution.py:47
  130.8 6.6 %collective-permute-start.22 = (bf16[64,512]{1,0:T(8,128)(2,1)S(1)}, bf16[64,512]{1,0:T(8,128)(2,1)S(1)}, u32[]{:S(2)}, u32[]{:S(2)}) collective-permute-start(bf16[64,512]{1,0:T(8,128)(2,1)S(1)} %get-tuple-element.42), channel_id=1, source_target_pairs={{32,0},{33,1},{34,2},{35,3},{36,4},{37,5},{38,6},{39,7},{40,8},{41... | collective-permute-start | bytes 196616 | tf_op jit(solution)/shard_map/ppermute | solution.py:47
  134.2 6.1 %collective-permute-start.23 = (bf16[64,512]{1,0:T(8,128)(2,1)S(1)}, bf16[64,512]{1,0:T(8,128)(2,1)S(1)}, u32[]{:S(2)}, u32[]{:S(2)}) collective-permute-start(bf16[64,512]{1,0:T(8,128)(2,1)S(1)} %get-tuple-element.43), channel_id=1, source_target_pairs={{64,0},{65,1},{66,2},{67,3},{68,4},{69,5},{70,6},{71,7},{72,8},{73... | collective-permute-start | bytes 196616 | tf_op jit(solution)/shard_map/ppermute | solution.py:47
  134.7 6.2 %collective-permute-start.24 = (bf16[64,512]{1,0:T(8,128)(2,1)S(1)}, bf16[64,512]{1,0:T(8,128)(2,1)S(1)}, u32[]{:S(2)}, u32[]{:S(2)}) collective-permute-start(bf16[64,512]{1,0:T(8,128)(2,1)S(1)} %get-tuple-element.44), channel_id=1, source_target_pairs={{96,0},{97,1},{98,2},{99,3},{100,4},{101,5},{102,6},{103,7},{104,8... | collective-permute-start | bytes 196616 | tf_op jit(solution)/shard_map/ppermute | solution.py:47
  141.0 4.4 %collective-permute-start.25 = (bf16[256,128]{1,0:T(8,128)(2,1)S(1)}, bf16[256,128]{1,0:T(8,128)(2,1)S(1)}, u32[]{:S(2)}, u32[]{:S(2)}) collective-permute-start(bf16[256,128]{1,0:T(8,128)(2,1)S(1)} %get-tuple-element.46), channel_id=1, source_target_pairs={{2,0},{3,1},{4,2},{5,3},{6,4},{7,5},{0,6},{1,7},{10,8},{11,9},{12,... | collective-permute-start | bytes 196616 | tf_op jit(solution)/shard_map/ppermute | solution.py:47
  142.1 6.1 %collective-permute-start.26 = (bf16[256,128]{1,0:T(8,128)(2,1)S(1)}, bf16[256,128]{1,0:T(8,128)(2,1)S(1)}, u32[]{:S(2)}, u32[]{:S(2)}) collective-permute-start(bf16[256,128]{1,0:T(8,128)(2,1)S(1)} %get-tuple-element.47), channel_id=1, source_target_pairs={{4,0},{5,1},{6,2},{7,3},{0,4},{1,5},{2,6},{3,7},{12,8},{13,9},{14,... | collective-permute-start | bytes 196616 | tf_op jit(solution)/shard_map/ppermute | solution.py:47
  144.0 5.5 %collective-permute-start.27 = (bf16[256,128]{1,0:T(8,128)(2,1)S(1)}, bf16[256,128]{1,0:T(8,128)(2,1)S(1)}, u32[]{:S(2)}, u32[]{:S(2)}) collective-permute-start(bf16[256,128]{1,0:T(8,128)(2,1)S(1)} %get-tuple-element.48), channel_id=1, source_target_pairs={{6,0},{7,1},{0,2},{1,3},{2,4},{3,5},{4,6},{5,7},{14,8},{15,9},{8,1... | collective-permute-start | bytes 196616 | tf_op jit(solution)/shard_map/ppermute | solution.py:47
